TPU v7x, 512 devices: a 4x2x32 block of a 4x8x32 slice. The times are simulated.
512 devices in a mesh: grp: 2 (over y), tp: 32 (over z), dp: 8 (over x, core).
Axes of the slice: x: 4, y: 2, z: 32, core: 2. Of those that a mesh axis runs over, the one named last changes fastest.
The devices are a block of a 4x8x32 slice.
Arguments:
- tokens: bfloat16 [256, 8, 4096], P(('grp', 'tp'), None, 'dp'), parts along dimension 0, may hold values from -8 to 8
- seq_lengths: int32 [256], P('grp'), parts along dimension 0, may hold values from 1 to 8, 384 in all
- state_re: float32 [2, 256, 8192], P(None, ('grp', 'dp'), 'tp'), parts along dimension 1, may hold values from -6 to 6
- state_im: float32 [2, 256, 8192], P(None, ('grp', 'dp'), 'tp'), parts along dimension 1, may hold values from -6 to 6
- gain_in: float32 [2, 4096], P(None, 'dp'), may hold values from 0.1 to 1.9
- w_in: bfloat16 [2, 4096, 2048], P(None, 'dp', 'tp'), may hold values from -0.09375 to 0.09375
- decay_rate: float32 [2, 8192], P(None, 'tp'), may hold values from 0.05 to 4
- frequency: float32 [2, 8192], P(None, 'tp'), may hold values from -3.140625 to 3.140625
- log_step: float32 [2, 128], P(None, 'tp'), may hold values from -2.3 to 0
- in_re: float32 [2, 128, 64, 16], P(None, 'tp'), may hold values from -1 to 1
- in_im: float32 [2, 128, 64, 16], P(None, 'tp'), may hold values from -1 to 1
- readout_real: float32 [2, 128, 16, 64], P(None, 'tp'), may hold values from -0.75 to 0.75
- readout_imaginary: float32 [2, 128, 16, 64], P(None, 'tp'), may hold values from -0.75 to 0.75
- skip_scale: float32 [2, 2048], P(None, 'tp'), may hold values from -4 to 4
- gain_out: float32 [2, 2048], P(None, 'tp'), may hold values from 0.1 to 1.9
- w_out: bfloat16 [2, 2048, 4096], P(None, 'tp', 'dp'), may hold values from -0.125 to 0.125
Outputs:
- result: bfloat16 [256, 8, 4096], P(('grp', 'tp'), None, 'dp'), parts along dimension 0
- final_re: float32 [2, 256, 8192], P(None, ('grp', 'dp'), 'tp'), parts along dimension 1
- final_im: float32 [2, 256, 8192], P(None, ('grp', 'dp'), 'tp'), parts along dimension 1
There are 2 independent parts, one for each index of `grp`. A program takes and returns all parts, laid end to end along the dimension named above; an argument that names none is the same for every part. Nothing has to cross between parts.
Inputs may be any that keep to these rules, and one draw needn't show every extreme that they name: `seq_lengths`: within one group of requests the live tokens of all 128 sequences sum to exactly 384, and some sequence has all 8 live.
All inputs are finite; a program needn't handle non-finite values.
Results may differ from a plain program's by a relative error of at most 0.019.
Values may be sent and summed in bfloat16 or wider, within the bound.
No kernel may reach another device: no remote copies, remote signals or barrier semaphores. Data moves between devices by JAX's collectives and lax.ppermute only.
A program may use at most 64 MiB of HBM per device.

v0:
```python
import math

import jax
import jax.numpy as jnp
from jax import lax
from jax.sharding import PartitionSpec as P

D = 4096
CHANNELS = 2048


EPSILON = 1e-06


def laid_out(pieces, dim):
    lengths = list(pieces.shape[1:])
    lengths[dim] *= pieces.shape[0]
    return jnp.moveaxis(pieces, 0, dim).reshape(lengths)


def from_everyone(shard, axis):
    peers = lax.axis_size(axis)
    return lax.all_to_all(
        jnp.broadcast_to(shard[None], (peers, *shard.shape)), axis, 0, 0, tiled=True
    )


def gather_directly(shard, axis, dim):
    return laid_out(from_everyone(shard, axis), dim)


def cut_along(shard, dim, peers):
    before, after = (shard.shape[:dim], shard.shape[dim + 1 :])
    return jnp.moveaxis(shard.reshape(*before, peers, -1, *after), dim, 0)


def sent_and_summed(shard, axis, dim):
    pieces = cut_along(shard, dim, lax.axis_size(axis))
    arrived = lax.all_to_all(pieces, axis, split_axis=0, concat_axis=0, tiled=True)
    return arrived.astype(jnp.float32).sum(axis=0)


def in_one_piece(arrays, axis, dim, along):
    widths = [math.prod(a.shape[along:]) for a in arrays]
    both = jnp.concatenate(
        [a.reshape(*a.shape[:along], w) for a, w in zip(arrays, widths)], axis=along
    )
    out = sent_and_summed(both, axis, dim)
    pieces = jnp.split(out, [sum(widths[:k]) for k in range(1, len(widths))], axis=along)
    return tuple((b.reshape(*out.shape[:along], *a.shape[along:]) for a, b in zip(arrays, pieces)))


def of_everyone(shard, axis):
    everything = from_everyone(shard, axis)
    return jnp.sum(everything, axis=0)


def recur(
    driven,
    seq_lengths,
    state_re,
    state_im,
    decay_rate,
    frequency,
    log_step,
    in_re,
    in_im,
    readout_real,
    readout_imaginary,
    skip_scale,
):
    seq_count, step_count, chan_count = driven.shape
    channel_groups = log_step.shape[0]
    step_dt = jnp.exp(log_step)[:, None]
    real_part = -decay_rate.reshape(channel_groups, -1)
    imag_part = frequency.reshape(channel_groups, -1)
    magnitude = jnp.exp(real_part * step_dt)
    carry_re = magnitude * jnp.cos(imag_part * step_dt)
    carry_im = magnitude * jnp.sin(imag_part * step_dt)
    denominator = real_part * real_part + imag_part * imag_part
    factor_re = ((carry_re - 1.0) * real_part + carry_im * imag_part) / denominator
    factor_im = (carry_im * real_part - (carry_re - 1.0) * imag_part) / denominator
    input_re = factor_re[..., None] * in_re - factor_im[..., None] * in_im
    input_im = factor_re[..., None] * in_im + factor_im[..., None] * in_re
    group_split_rows = driven.astype(jnp.float32).reshape(seq_count, step_count, channel_groups, -1)
    pushed_re = jnp.einsum("gpc,stgc->stgp", input_re, group_split_rows)
    pushed_im = jnp.einsum("gpc,stgc->stgp", input_im, group_split_rows)
    hidden_real = state_re.reshape(seq_count, channel_groups, -1)
    hidden_imaginary = state_im.reshape(seq_count, channel_groups, -1)
    positions = jnp.arange(step_count, dtype=jnp.int32)
    live = positions[None, :] < seq_lengths[:, None]
    layer_outputs = []
    for tok_step in range(step_count):
        active = live[:, tok_step][:, None, None]
        next_re = carry_re * hidden_real - carry_im * hidden_imaginary + pushed_re[:, tok_step]
        next_im = carry_re * hidden_imaginary + carry_im * hidden_real + pushed_im[:, tok_step]
        hidden_real = jnp.where(active, next_re, hidden_real)
        hidden_imaginary = jnp.where(active, next_im, hidden_imaginary)
        layer_outputs.append(
            jnp.einsum("jlb,wjb->wjl", readout_real, hidden_real)
            - jnp.einsum("jlb,wjb->wjl", readout_imaginary, hidden_imaginary)
        )
    readout = jnp.stack(layer_outputs, axis=1).reshape(seq_count, step_count, chan_count)
    readout = jax.nn.gelu(readout + skip_scale * driven.astype(jnp.float32))
    readout = jnp.where(live[..., None], readout, 0.0)
    return (hidden_real.reshape(seq_count, -1), hidden_imaginary.reshape(seq_count, -1), readout)


def per_device(
    tokens,
    seq_lengths,
    state_re,
    state_im,
    gain_in,
    w_in,
    decay_rate,
    frequency,
    log_step,
    in_re,
    in_im,
    readout_real,
    readout_imaginary,
    skip_scale,
    gain_out,
    w_out,
):
    seq_local = tokens.shape[0]
    seqs_all = seq_local * lax.axis_size("tp")
    seqs_state = seqs_all // lax.axis_size("dp")
    state_start = lax.axis_index("dp") * seqs_state
    state_lengths = lax.dynamic_slice_in_dim(seq_lengths, state_start, seqs_state, 0)
    current = tokens
    finals_re = []
    finals_im = []
    for depth_index in range(state_re.shape[0]):
        gain_row = gain_in[depth_index]
        gathered = gather_directly(current, "tp", 0)
        values = gathered.astype(jnp.float32)
        squares = jnp.sum(values * values, axis=-1)
        scaled_rows = (values * gain_row).astype(jnp.bfloat16)
        weight_block = w_in[depth_index]
        summed, mine_sq = in_one_piece(
            (
                jnp.einsum(
                    "std,dc->stc", scaled_rows, weight_block, preferred_element_type=jnp.float32
                ).astype(jnp.bfloat16),
                squares.astype(jnp.bfloat16),
            ),
            "dp",
            0,
            2,
        )
        inv_rms = lax.rsqrt(mine_sq / D + EPSILON)
        driven = (inv_rms[..., None] * summed).astype(jnp.bfloat16)
        new_re, new_im, readout = recur(
            driven,
            state_lengths,
            state_re[depth_index],
            state_im[depth_index],
            decay_rate[depth_index],
            frequency[depth_index],
            log_step[depth_index],
            in_re[depth_index],
            in_im[depth_index],
            readout_real[depth_index],
            readout_imaginary[depth_index],
            skip_scale[depth_index],
        )
        finals_re.append(new_re)
        finals_im.append(new_im)
        branch_sq = of_everyone(jnp.sum(readout * readout, axis=-1), "tp")
        inv_out = lax.rsqrt(branch_sq / CHANNELS + EPSILON)
        normed = (readout * inv_out[..., None] * gain_out[depth_index]).astype(jnp.bfloat16)
        branch_all = gather_directly(normed, "dp", 0)
        out_block = w_out[depth_index]
        mixed = sent_and_summed(
            jnp.einsum(
                "stc,cd->std", branch_all, out_block, preferred_element_type=jnp.float32
            ).astype(jnp.bfloat16),
            "tp",
            0,
        )
        current = (current.astype(jnp.float32) + mixed).astype(jnp.bfloat16)
    return (current, jnp.stack(finals_re), jnp.stack(finals_im))


def solution(mesh):
    in_specs = (
        P(("grp", "tp"), None, "dp"),
        P("grp"),
        P(None, ("grp", "dp"), "tp"),
        P(None, ("grp", "dp"), "tp"),
        P(None, "dp"),
        P(None, "dp", "tp"),
        P(None, "tp"),
        P(None, "tp"),
        P(None, "tp"),
        P(None, "tp", None, None),
        P(None, "tp", None, None),
        P(None, "tp", None, None),
        P(None, "tp", None, None),
        P(None, "tp"),
        P(None, "tp"),
        P(None, "tp", "dp"),
    )
    out_specs = (
        P(("grp", "tp"), None, "dp"),
        P(None, ("grp", "dp"), "tp"),
        P(None, ("grp", "dp"), "tp"),
    )
    return jax.shard_map(
        per_device, mesh=mesh, in_specs=in_specs, out_specs=out_specs, check_vma=False
    )
```

profile of v0, /device:TPU:40, one launch (start us, length us, event | category | flops | bytes accessed | tf_op | source)
XLA Modules:
  0.0 614.2 jit_solution(3000106348975648382)
XLA Ops:
  0.6 0.8 copy.485
  1.4 1.5 broadcast_in_dim.286
  2.9 45.9 %all-to-all-start = ((bf16[32,4,8,512]{3,1,2,0:T(4,128)(2,1)}), bf16[32,4,8,512]{3,1,2,0:T(4,128)(2,1)S(1)}, u32[]{:S(2)}, u32[]{:S(2)}) async-start(bf16[32,4,8,512]{3,1,2,0:T(4,128)(2,1)} %broadcast_in_dim.286), calls=%async_computation | async-start | bytes 2097152 | tf_op jit(solution)/shard_map/all_to_all | solution.py:23
  49.7 103.6 %all-to-all-done = bf16[32,4,8,512]{3,1,2,0:T(4,128)(2,1)S(1)} async-done(((bf16[32,4,8,512]{3,1,2,0:T(4,128)(2,1)}), bf16[32,4,8,512]{3,1,2,0:T(4,128)(2,1)S(1)}, u32[]{:S(2)}, u32[]{:S(2)}) %all-to-all-start) | async-done | bytes 1048608 | tf_op jit(solution)/shard_map/all_to_all | solution.py:23
  153.3 0.4 fusion
  154.0 0.8 copy.494
  155.3 0.8 pad_maximum_fusion
  156.1 4.6 all-to-all-start.1
  160.7 7.5 %all-to-all-done.1 = bf16[8,16,8,65]{3,2,1,0:T(8,128)(2,1)S(1)} async-done(((bf16[8,16,8,65]{3,2,1,0:T(8,128)(2,1)}), bf16[8,16,8,65]{3,2,1,0:T(8,128)(2,1)S(1)}, u32[]{:S(2)}, u32[]{:S(2)}) %all-to-all-start.1) | async-done | bytes 133152 | tf_op jit(solution)/shard_map/all_to_all | solution.py:39
  172.9 29.6 %all_to_all.50 = f32[32,1,128]{2,1,0:T(1,128)S(1)} all-to-all(f32[32,1,128]{2,1,0:T(1,128)S(1)} %reshape.895), channel_id=1, replica_groups=mesh['grp'=2,'tp'=32,'dp'=8] {'tp'}, dimensions={0} | all-to-all | bytes 32768 | tf_op jit(solution)/shard_map/all_to_all | solution.py:23
  202.5 0.5 broadcast.499
  203.1 0.7 reduce.34
  204.4 8.6 %all_to_all.51 = bf16[8,2,4096]{2,1,0:T(2,128)(2,1)S(1)} all-to-all(bf16[8,2,4096]{2,1,0:T(2,128)(2,1)S(1)} %reshape.897), channel_id=1, replica_groups=mesh['grp'=2,'tp'=32,'dp'=8] {'dp'}, dimensions={0} | all-to-all | bytes 262144 | tf_op jit(solution)/shard_map/all_to_all | solution.py:23
  213.9 0.5 copy.530
  214.4 113.4 %all_to_all.52 = bf16[32,4,8,512]{3,1,2,0:T(4,128)(2,1)S(1)} all-to-all(bf16[32,4,8,512]{3,1,2,0:T(4,128)(2,1)S(1)} %copy.530), channel_id=1, replica_groups=mesh['grp'=2,'tp'=32,'dp'=8] {'tp'}, dimensions={0} | all-to-all | bytes 2097152 | tf_op jit(solution)/shard_map/all_to_all | solution.py:39
  328.0 0.6 copy-done.4
  328.7 1.5 broadcast_in_dim.304
  330.1 4.8 all-to-all-start.5
  336.7 101.5 %all-to-all-done.5 = bf16[32,4,8,512]{3,1,2,0:T(4,128)(2,1)S(1)} async-done(((bf16[32,4,8,512]{3,1,2,0:T(4,128)(2,1)}), bf16[32,4,8,512]{3,1,2,0:T(4,128)(2,1)S(1)}, u32[]{:S(2)}, u32[]{:S(2)}) %all-to-all-start.5) | async-done | bytes 1048608 | tf_op jit(solution)/shard_map/all_to_all | solution.py:23
  439.3 0.8 copy.539
  440.2 0.8 pad_maximum_fusion.1
  441.0 3.8 all-to-all-start.6
  445.0 6.9 %all-to-all-done.6 = bf16[8,16,8,65]{3,2,1,0:T(8,128)(2,1)S(1)} async-done(((bf16[8,16,8,65]{3,2,1,0:T(8,128)(2,1)}), bf16[8,16,8,65]{3,2,1,0:T(8,128)(2,1)S(1)}, u32[]{:S(2)}, u32[]{:S(2)}) %all-to-all-start.6) | async-done | bytes 133152 | tf_op jit(solution)/shard_map/all_to_all | solution.py:39
  457.8 28.8 %all_to_all.53 = f32[32,1,128]{2,1,0:T(1,128)S(1)} all-to-all(f32[32,1,128]{2,1,0:T(1,128)S(1)} %reshape.899), channel_id=1, replica_groups=mesh['grp'=2,'tp'=32,'dp'=8] {'tp'}, dimensions={0} | all-to-all | bytes 32768 | tf_op jit(solution)/shard_map/all_to_all | solution.py:23
  486.6 0.7 reduce.35
  487.9 8.6 %all_to_all.54 = bf16[8,2,4096]{2,1,0:T(2,128)(2,1)S(1)} all-to-all(bf16[8,2,4096]{2,1,0:T(2,128)(2,1)S(1)} %reshape.901), channel_id=1, replica_groups=mesh['grp'=2,'tp'=32,'dp'=8] {'dp'}, dimensions={0} | all-to-all | bytes 262144 | tf_op jit(solution)/shard_map/all_to_all | solution.py:23
  497.4 1.5 copy.569
  499.0 4.8 all-to-all-start.9
  505.6 0.6 pad_maximum_fusion.3
  506.3 0.6 pad_maximum_fusion.2
  506.9 106.4 %all-to-all-done.9 = bf16[32,4,8,512]{3,1,2,0:T(4,128)(2,1)S(1)} async-done(((bf16[32,4,8,512]{3,1,2,0:T(4,128)(2,1)}), bf16[32,4,8,512]{3,1,2,0:T(4,128)(2,1)S(1)}, u32[]{:S(2)}, u32[]{:S(2)}) %all-to-all-start.9) | async-done | bytes 1048608 | tf_op jit(solution)/shard_map/all_to_all | solution.py:39
  613.5 0.6 copy.604
  (261 shorter events, 19.8 us)
Async XLA Ops:
  2.9 46.0 %copy-start.15 = (s32[128]{0:T(128)S(1)}, s32[128]{0:T(128)}, u32[]{:S(2)}) copy-start(s32[128]{0:T(128)} %param.17) | copy-start | bytes 1540
  2.9 46.2 %copy-start.10 = (f32[2,256]{1,0:T(2,128)S(1)}, f32[2,256]{1,0:T(2,128)}, u32[]{:S(2)}) copy-start(f32[2,256]{1,0:T(2,128)} %param.22) | copy-start | bytes 6148
  2.9 46.2 %copy-start.11 = (f32[2,256]{1,0:T(2,128)S(1)}, f32[2,256]{1,0:T(2,128)}, u32[]{:S(2)}) copy-start(f32[2,256]{1,0:T(2,128)} %param.23) | copy-start | bytes 6148
  2.9 46.4 %slice-start.1 = ((f32[2,16,256]{2,1,0:T(8,128)}), f32[1,16,256]{2,1,0:T(8,128)S(1)}, s32[]{:S(2)}) async-start(f32[2,16,256]{2,1,0:T(8,128)} %param.18), calls=%async_computation.11 | async-start | bytes 32768 | tf_op jit(solution)/shard_map/slice | solution.py:158
  2.9 46.5 %slice-start = ((f32[2,16,256]{2,1,0:T(8,128)}), f32[1,16,256]{2,1,0:T(8,128)S(1)}, s32[]{:S(2)}) async-start(f32[2,16,256]{2,1,0:T(8,128)} %param.19), calls=%async_computation.10 | async-start | bytes 32768 | tf_op jit(solution)/shard_map/slice | solution.py:159
  2.9 46.6 %copy-start.12 = (f32[2,4]{1,0:T(2,128)S(1)}, f32[2,4]{1,0:T(2,128)}, u32[]{:S(2)}) copy-start(f32[2,4]{1,0:T(2,128)} %param.24) | copy-start | bytes 100
  2.9 46.6 %copy-start.9 = (f32[2,512]{1,0:T(2,128)S(1)}, f32[2,512]{1,0:T(2,128)}, u32[]{:S(2)}) copy-start(f32[2,512]{1,0:T(2,128)} %param.20) | copy-start | bytes 12292
  2.9 150.4 %all-to-all-start = ((bf16[32,4,8,512]{3,1,2,0:T(4,128)(2,1)}), bf16[32,4,8,512]{3,1,2,0:T(4,128)(2,1)S(1)}, u32[]{:S(2)}, u32[]{:S(2)}) async-start(bf16[32,4,8,512]{3,1,2,0:T(4,128)(2,1)} %broadcast_in_dim.286), calls=%async_computation | async-start | bytes 2097152 | tf_op jit(solution)/shard_map/all_to_all | solution.py:23
  153.3 1.5 copy-start.6
  154.8 5.9 copy-start.13
  154.8 5.9 copy-start.14
  155.3 13.5 %copy-start.2 = (f32[2,4,64,16]{2,3,1,0:T(8,128)S(1)}, f32[2,4,64,16]{2,3,1,0:T(8,128)}, u32[]{:S(2)}) copy-start(f32[2,4,64,16]{2,3,1,0:T(8,128)} %param.26) | copy-start | bytes 98308
  155.3 13.5 %copy-start.3 = (f32[2,4,64,16]{2,3,1,0:T(8,128)S(1)}, f32[2,4,64,16]{2,3,1,0:T(8,128)}, u32[]{:S(2)}) copy-start(f32[2,4,64,16]{2,3,1,0:T(8,128)} %param.25) | copy-start | bytes 98308
  156.1 12.1 %all-to-all-start.1 = ((bf16[8,16,8,65]{3,2,1,0:T(8,128)(2,1)}), bf16[8,16,8,65]{3,2,1,0:T(8,128)(2,1)S(1)}, u32[]{:S(2)}, u32[]{:S(2)}) async-start(bf16[8,16,8,65]{3,2,1,0:T(8,128)(2,1)} %pad_maximum_fusion), calls=%async_computation.1 | async-start | bytes 524288 | tf_op jit(solution)/shard_map/all_to_all | solution.py:39
  168.6 0.9 copy-start
  168.7 0.9 copy-start.1
  172.8 40.4 %copy-start.7 = (bf16[2,64,512]{2,1,0:T(8,128)(2,1)S(1)}, bf16[2,64,512]{2,1,0:T(8,128)(2,1)}, u32[]{:S(2)}) copy-start(bf16[2,64,512]{2,1,0:T(8,128)(2,1)} %param.31) | copy-start | bytes 393220
  327.8 0.8 copy-start.4
  330.1 108.1 %all-to-all-start.5 = ((bf16[32,4,8,512]{3,1,2,0:T(4,128)(2,1)}), bf16[32,4,8,512]{3,1,2,0:T(4,128)(2,1)S(1)}, u32[]{:S(2)}, u32[]{:S(2)}) async-start(bf16[32,4,8,512]{3,1,2,0:T(4,128)(2,1)} %broadcast_in_dim.304), calls=%async_computation.5 | async-start | bytes 2097152 | tf_op jit(solution)/shard_map/all_to_all | solution.py:23
  439.1 5.7 copy-start.5
  439.1 5.7 copy-start.8
  441.0 10.9 %all-to-all-start.6 = ((bf16[8,16,8,65]{3,2,1,0:T(8,128)(2,1)}), bf16[8,16,8,65]{3,2,1,0:T(8,128)(2,1)S(1)}, u32[]{:S(2)}, u32[]{:S(2)}) async-start(bf16[8,16,8,65]{3,2,1,0:T(8,128)(2,1)} %pad_maximum_fusion.1), calls=%async_computation.6 | async-start | bytes 524288 | tf_op jit(solution)/shard_map/all_to_all | solution.py:39
  499.0 114.3 %all-to-all-start.9 = ((bf16[32,4,8,512]{3,1,2,0:T(4,128)(2,1)}), bf16[32,4,8,512]{3,1,2,0:T(4,128)(2,1)S(1)}, u32[]{:S(2)}, u32[]{:S(2)}) async-start(bf16[32,4,8,512]{3,1,2,0:T(4,128)(2,1)} %copy.569), calls=%async_computation.9 | async-start | bytes 2097152 | tf_op jit(solution)/shard_map/all_to_all | solution.py:39
where the time goes:
time: 615 us; the launch traced here: 614 us
  waiting for transfers between devices  326 us (53%)
  blocking collectives  189 us (31%)
  starting transfers between devices  64 us (10%)
  local copies, waits for them, and re-layouts  19.3 us (3%)
  other arithmetic  7.96 us (1%)
  matrix products  6.48 us (1%)
    all_to_all x2, waiting for transfers between devices, from_everyone(): lax.all_to_all(jnp.broadcast_to(shard[None], (peers, *shard.shape)), axis...  205 us
    all_to_all x3, waiting for transfers between devices, sent_and_summed(): lax.all_to_all(pieces, axis, split_axis=0, concat_axis=0, tiled=True)  121 us
    all_to_all x1, blocking collectives, sent_and_summed(): lax.all_to_all(pieces, axis, split_axis=0, concat_axis=0, tiled=True)  113 us
    all_to_all x4, blocking collectives, from_everyone(): lax.all_to_all(jnp.broadcast_to(shard[None], (peers, *shard.shape)), axis...  75.6 us
    all_to_all x2, starting transfers between devices, from_everyone(): lax.all_to_all(jnp.broadcast_to(shard[None], (peers, *shard.shape)), axis...  50.8 us
    all_to_all x3, starting transfers between devices, sent_and_summed(): lax.all_to_all(pieces, axis, split_axis=0, concat_axis=0, tiled=True)  13.2 us
  transfers between devices with their start and end apart: 5, of which 5 were waited for; matrix products, arithmetic and copies ran while one was open for 1% of the time, Pallas kernels for 0%

commit v1 on v0

v1 whole, which is shorter than its diff:
```python
import math

import jax
import jax.numpy as jnp
from jax import lax
from jax.sharding import Mesh, PartitionSpec as P

D = 4096
CHANNELS = 2048


EPSILON = 1e-06
LIVE_PER_SEQ = 3


NEAR = 4


def from_everyone(shard, axis):
    peers = lax.axis_size(axis)
    return lax.all_to_all(
        jnp.broadcast_to(shard[None], (peers, *shard.shape)), axis, 0, 0, tiled=True
    )


def exchanged(pieces, axis):
    return lax.all_to_all(pieces, axis, 0, 0, tiled=True)


def summed(pieces, axis):
    return jnp.sum(exchanged(pieces, axis).astype(jnp.float32), axis=0)


def gathered_over_tp(rows):
    far = from_everyone(rows, "far")
    near = from_everyone(far.reshape(-1, rows.shape[-1]), "near")
    return near.reshape(-1, rows.shape[-1])


def scattered_over_tp(pieces):
    near, far, rows, width = pieces.shape
    part = summed(pieces.reshape(near, far * rows, width), "near").astype(jnp.bfloat16)
    return summed(part.reshape(far, rows, width), "far")


def with_squares(product, squares):
    return jnp.concatenate(
        [product.astype(jnp.bfloat16), squares[..., None].astype(jnp.bfloat16)], axis=-1
    )


def with_row(pieces, squares):
    row = jnp.pad(squares, [(0, 0), (0, 0), (0, pieces.shape[-1] - squares.shape[-1])])
    return jnp.concatenate([pieces, row[:, :, None].astype(jnp.bfloat16)], axis=2)


def mixed_of(total, rows):
    inv_out = lax.rsqrt(total[rows, :rows] / CHANNELS + EPSILON)
    return total[:rows] * inv_out[:, None]


def project_in(rows, gain_row, weight_block):
    values = rows.astype(jnp.float32)
    squares = jnp.sum(values * values, axis=-1)
    scaled = (values * gain_row).astype(jnp.bfloat16)
    product = jnp.dot(scaled, weight_block, preferred_element_type=jnp.float32)
    return with_squares(product, squares)


def recur(
    driven,
    seq_lengths,
    state_re,
    state_im,
    decay_rate,
    frequency,
    log_step,
    in_re,
    in_im,
    readout_real,
    readout_imaginary,
    skip_scale,
):
    seq_count, step_count, chan_count = driven.shape
    channel_groups = log_step.shape[0]
    step_dt = jnp.exp(log_step)[:, None]
    real_part = -decay_rate.reshape(channel_groups, -1)
    imag_part = frequency.reshape(channel_groups, -1)
    magnitude = jnp.exp(real_part * step_dt)
    carry_re = magnitude * jnp.cos(imag_part * step_dt)
    carry_im = magnitude * jnp.sin(imag_part * step_dt)
    denominator = real_part * real_part + imag_part * imag_part
    factor_re = ((carry_re - 1.0) * real_part + carry_im * imag_part) / denominator
    factor_im = (carry_im * real_part - (carry_re - 1.0) * imag_part) / denominator
    input_re = factor_re[..., None] * in_re - factor_im[..., None] * in_im
    input_im = factor_re[..., None] * in_im + factor_im[..., None] * in_re
    group_split_rows = driven.astype(jnp.float32).reshape(seq_count, step_count, channel_groups, -1)
    pushed_re = jnp.einsum("gpc,stgc->stgp", input_re, group_split_rows)
    pushed_im = jnp.einsum("gpc,stgc->stgp", input_im, group_split_rows)
    hidden_real = state_re.reshape(seq_count, channel_groups, -1)
    hidden_imaginary = state_im.reshape(seq_count, channel_groups, -1)
    positions = jnp.arange(step_count, dtype=jnp.int32)
    live = positions[None, :] < seq_lengths[:, None]
    layer_outputs = []
    for tok_step in range(step_count):
        active = live[:, tok_step][:, None, None]
        next_re = carry_re * hidden_real - carry_im * hidden_imaginary + pushed_re[:, tok_step]
        next_im = carry_re * hidden_imaginary + carry_im * hidden_real + pushed_im[:, tok_step]
        hidden_real = jnp.where(active, next_re, hidden_real)
        hidden_imaginary = jnp.where(active, next_im, hidden_imaginary)
        layer_outputs.append(
            jnp.einsum("jlb,wjb->wjl", readout_real, hidden_real)
            - jnp.einsum("jlb,wjb->wjl", readout_imaginary, hidden_imaginary)
        )
    readout = jnp.stack(layer_outputs, axis=1).reshape(seq_count, step_count, chan_count)
    readout = jax.nn.gelu(readout + skip_scale * driven.astype(jnp.float32))
    readout = jnp.where(live[..., None], readout, 0.0)
    return (hidden_real.reshape(seq_count, -1), hidden_imaginary.reshape(seq_count, -1), readout)


def branch(packed, depth, lengths, states, weights):
    total = summed(packed, "dp")
    inv_rms = lax.rsqrt(total[:, -1:] / D + EPSILON)
    driven = (inv_rms * total[:, :-1]).astype(jnp.bfloat16)
    seqs = lengths.shape[0]
    new_re, new_im, readout = recur(
        driven.reshape(seqs, -1, driven.shape[-1]),
        lengths,
        *[s[depth] for s in states],
        *[w[depth] for w in weights[:-1]],
    )
    readout = readout.reshape(driven.shape)
    sent = with_squares(readout * weights[-1][depth], jnp.sum(readout * readout, axis=-1))
    everyone = from_everyone(sent, "dp")
    return new_re, new_im, everyone.reshape(-1, sent.shape[-1])


def per_device(
    tokens,
    seq_lengths,
    state_re,
    state_im,
    gain_in,
    w_in,
    decay_rate,
    frequency,
    log_step,
    in_re,
    in_im,
    readout_real,
    readout_imaginary,
    skip_scale,
    gain_out,
    w_out,
):
    near, far, dp = (lax.axis_size(a) for a in ("near", "far", "dp"))
    seq_local, steps, width = tokens.shape
    seqs_all = seq_local * near * far
    seqs_state = seqs_all // dp
    own = seq_local * steps
    rows_all = seqs_all * steps
    live_own = LIVE_PER_SEQ * seq_local
    rank = lax.axis_index("far") * near + lax.axis_index("near")
    state_start = lax.axis_index("dp") * seqs_state
    state_lengths = lax.dynamic_slice_in_dim(seq_lengths, state_start, seqs_state, 0)
    states = (state_re, state_im)
    weights = (
        decay_rate,
        frequency,
        log_step,
        in_re,
        in_im,
        readout_real,
        readout_imaginary,
        skip_scale,
        gain_out,
    )

    step_of = jnp.arange(steps, dtype=jnp.int32)
    live = step_of[None, :] < seq_lengths[:, None]
    starts = jnp.cumsum(seq_lengths) - seq_lengths
    place = jnp.where(live, starts[:, None] + step_of[None, :], -1).reshape(-1)
    slot = jnp.arange(near * far * live_own, dtype=jnp.int32)
    n_of, f_of, r_of = slot // (far * live_own), slot // live_own % far, slot % live_own
    token_of = (f_of * near + n_of) * live_own + r_of
    pick = (token_of[:, None] == place[None, :]).astype(jnp.bfloat16)

    def natural(rows):
        split = rows.reshape(near, far, own, rows.shape[-1])
        return jnp.swapaxes(split, 0, 1).reshape(rows_all, rows.shape[-1])

    def exact(left, right):
        return jnp.dot(left, right, preferred_element_type=jnp.float32).astype(jnp.bfloat16)

    everyone = gathered_over_tp(tokens.reshape(own, width))
    packed = natural(project_in(everyone, gain_in[0], w_in[0]))
    re_0, im_0, sent = branch(
        packed.reshape(dp, -1, packed.shape[-1]), 0, state_lengths, states, weights
    )
    live_sent = jnp.dot(pick, sent, preferred_element_type=jnp.float32)
    partial = jnp.dot(
        live_sent[:, :-1].astype(jnp.bfloat16), w_out[0], preferred_element_type=jnp.float32
    ).astype(jnp.bfloat16)
    total = scattered_over_tp(
        with_row(
            partial.reshape(near, far, live_own, width),
            live_sent[:, -1].reshape(near, far, live_own),
        )
    )
    place_gathered = place.reshape(far, near, own).swapaxes(0, 1).reshape(-1)
    mine = rank * live_own + jnp.arange(live_own, dtype=jnp.int32)
    pick_mine = (mine[:, None] == place_gathered[None, :]).astype(jnp.bfloat16)
    before = jnp.dot(pick_mine, everyone, preferred_element_type=jnp.float32)
    current = (before + mixed_of(total, live_own)).astype(jnp.bfloat16)

    everyone = gathered_over_tp(current)
    packed = exact(pick.T, project_in(everyone, gain_in[1], w_in[1]))
    re_1, im_1, sent = branch(
        packed.reshape(dp, -1, packed.shape[-1]), 1, state_lengths, states, weights
    )
    partial = jnp.dot(
        sent[:, :-1], w_out[1], preferred_element_type=jnp.float32
    ).astype(jnp.bfloat16)
    total = scattered_over_tp(
        with_row(
            partial.reshape(far, near, own, width).swapaxes(0, 1),
            sent[:, -1].reshape(far, near, own).swapaxes(0, 1),
        )
    )
    place_own = lax.dynamic_slice_in_dim(place, rank * own, own, 0)
    pick_own = (place_own[:, None] == token_of[None, :]).astype(jnp.bfloat16)
    after = jnp.dot(pick_own, everyone, preferred_element_type=jnp.float32)
    before = jnp.where(
        (place_own >= 0)[:, None], after, tokens.reshape(own, width).astype(jnp.float32)
    )
    result = (before + mixed_of(total, own)).astype(jnp.bfloat16)
    return (result.reshape(tokens.shape), jnp.stack([re_0, re_1]), jnp.stack([im_0, im_1]))


def solution(mesh):
    grp, tp, dp = (mesh.shape[a] for a in ("grp", "tp", "dp"))
    split = Mesh(
        mesh.devices.reshape(grp, tp // NEAR, NEAR, dp), ("grp", "far", "near", "dp")
    )
    tp = ("far", "near")
    in_specs = (
        P(("grp", "far", "near"), None, "dp"),
        P("grp"),
        P(None, ("grp", "dp"), tp),
        P(None, ("grp", "dp"), tp),
        P(None, "dp"),
        P(None, "dp", tp),
        P(None, tp),
        P(None, tp),
        P(None, tp),
        P(None, tp, None, None),
        P(None, tp, None, None),
        P(None, tp, None, None),
        P(None, tp, None, None),
        P(None, tp),
        P(None, tp),
        P(None, tp, "dp"),
    )
    out_specs = (
        P(("grp", "far", "near"), None, "dp"),
        P(None, ("grp", "dp"), tp),
        P(None, ("grp", "dp"), tp),
    )
    return jax.shard_map(
        per_device, mesh=split, in_specs=in_specs, out_specs=out_specs, check_vma=False
    )
```

time: 615 us -> 349 us (0.57)
  the two profiles are of different devices: /device:TPU:40 before, /device:TPU:104 now
where the time goes in v1:
time: 349 us; the launch traced here: 348 us
  blocking collectives  169 us (48%)
  waiting for transfers between devices  113 us (32%)
  starting transfers between devices  33.1 us (9%)
  local copies, waits for them, and re-layouts  17.2 us (5%)
  matrix products  8.29 us (2%)
  other arithmetic  5.49 us (2%)
    all_to_all x3, blocking collectives, from_everyone(): lax.all_to_all(jnp.broadcast_to(shard[None], (peers, *shard.shape)), axis...  124 us
    all_to_all x4, waiting for transfers between devices, exchanged(): return lax.all_to_all(pieces, axis, 0, 0, tiled=True)  81.5 us
    all_to_all x2, blocking collectives, exchanged(): return lax.all_to_all(pieces, axis, 0, 0, tiled=True)  45.6 us
    all_to_all x3, waiting for transfers between devices, from_everyone(): lax.all_to_all(jnp.broadcast_to(shard[None], (peers, *shard.shape)), axis...  31.1 us
    all_to_all x4, starting transfers between devices, exchanged(): return lax.all_to_all(pieces, axis, 0, 0, tiled=True)  21.5 us
    all_to_all x3, starting transfers between devices, from_everyone(): lax.all_to_all(jnp.broadcast_to(shard[None], (peers, *shard.shape)), axis...  11.6 us
  transfers between devices with their start and end apart: 7, of which 7 were waited for; matrix products, arithmetic and copies ran while one was open for 2% of the time, Pallas kernels for 0%

profile of v1, /device:TPU:104, one launch (start us, length us, event | category | flops | bytes accessed | tf_op | source)
XLA Modules:
  0.0 347.9 jit_solution(10941936662312400346)
XLA Ops:
  0.6 0.8 broadcast_in_dim.319
  1.4 82.0 %all_to_all.60 = bf16[8,32,512]{2,1,0:T(8,128)(2,1)S(1)} all-to-all(bf16[8,32,512]{2,1,0:T(8,128)(2,1)S(1)} %broadcast_in_dim.319), channel_id=1, replica_groups=mesh['grp'=2,'far'=8,'near'=4,'dp'=8] {'far'}, dimensions={0} | all-to-all | bytes 524288 | tf_op jit(solution)/shard_map/all_to_all | solution.py:21
  83.4 1.1 broadcast_in_dim.321
  84.6 4.0 %all-to-all-start.1 = ((bf16[4,256,512]{2,1,0:T(8,128)(2,1)}), bf16[4,256,512]{2,1,0:T(8,128)(2,1)S(1)}, u32[]{:S(2)}, u32[]{:S(2)}) async-start(bf16[4,256,512]{2,1,0:T(8,128)(2,1)} %broadcast_in_dim.321), calls=%async_computation.1 | async-start | bytes 2097152 | tf_op jit(solution)/shard_map/all_to_all | solution.py:21
  89.9 19.5 %all-to-all-done.1 = bf16[4,256,512]{2,1,0:T(8,128)(2,1)S(1)} async-done(((bf16[4,256,512]{2,1,0:T(8,128)(2,1)}), bf16[4,256,512]{2,1,0:T(8,128)(2,1)S(1)}, u32[]{:S(2)}, u32[]{:S(2)}) %all-to-all-start.1) | async-done | bytes 1048608 | tf_op jit(solution)/shard_map/all_to_all | solution.py:21
  111.1 0.8 copy.520
  111.9 4.6 %all-to-all-start.2 = ((bf16[8,128,65]{1,2,0:T(8,128)(2,1)}), bf16[8,128,65]{1,2,0:T(8,128)(2,1)S(1)}, u32[]{:S(2)}, u32[]{:S(2)}) async-start(bf16[8,128,65]{1,2,0:T(8,128)(2,1)} %copy.520), calls=%async_computation.2 | async-start | bytes 294912 | tf_op jit(solution)/shard_map/all_to_all | solution.py:27
  116.5 6.2 %all-to-all-done.2 = bf16[8,128,65]{1,2,0:T(8,128)(2,1)S(1)} async-done(((bf16[8,128,65]{1,2,0:T(8,128)(2,1)}), bf16[8,128,65]{1,2,0:T(8,128)(2,1)S(1)}, u32[]{:S(2)}, u32[]{:S(2)}) %all-to-all-start.2) | async-done | bytes 133152 | tf_op jit(solution)/shard_map/all_to_all | solution.py:27
  127.0 0.7 broadcast_in_dim.340
  127.7 3.7 %all-to-all-start.3 = ((bf16[8,128,65]{1,2,0:T(8,128)(2,1)}), bf16[8,128,65]{1,2,0:T(8,128)(2,1)S(1)}, u32[]{:S(2)}, u32[]{:S(2)}) async-start(bf16[8,128,65]{1,2,0:T(8,128)(2,1)} %broadcast_in_dim.340), calls=%async_computation.3 | async-start | bytes 294912 | tf_op jit(solution)/shard_map/all_to_all | solution.py:21
  131.6 5.8 %all-to-all-done.3 = bf16[8,128,65]{1,2,0:T(8,128)(2,1)S(1)} async-done(((bf16[8,128,65]{1,2,0:T(8,128)(2,1)}), bf16[8,128,65]{1,2,0:T(8,128)(2,1)S(1)}, u32[]{:S(2)}, u32[]{:S(2)}) %all-to-all-start.3) | async-done | bytes 133152 | tf_op jit(solution)/shard_map/all_to_all | solution.py:21
  139.2 16.6 %all_to_all.61 = bf16[4,104,512]{2,1,0:T(8,128)(2,1)S(1)} all-to-all(bf16[4,104,512]{2,1,0:T(8,128)(2,1)S(1)} %copy.549), channel_id=1, replica_groups=mesh['grp'=2,'far'=8,'near'=4,'dp'=8] {'near'}, dimensions={0} | all-to-all | bytes 851968 | tf_op jit(solution)/shard_map/all_to_all | solution.py:27
  155.8 0.7 reshape.1069
  156.5 7.3 %all-to-all-start.5 = ((bf16[8,13,512]{2,1,0:T(8,128)(2,1)}), bf16[8,13,512]{2,1,0:T(8,128)(2,1)S(1)}, u32[]{:S(2)}, u32[]{:S(2)}) async-start(bf16[8,13,512]{2,1,0:T(8,128)(2,1)} %reshape.1069), calls=%async_computation.5 | async-start | bytes 262144 | tf_op jit(solution)/shard_map/all_to_all | solution.py:27
  164.6 28.7 %all-to-all-done.5 = bf16[8,13,512]{2,1,0:T(8,128)(2,1)S(1)} async-done(((bf16[8,13,512]{2,1,0:T(8,128)(2,1)}), bf16[8,13,512]{2,1,0:T(8,128)(2,1)S(1)}, u32[]{:S(2)}, u32[]{:S(2)}) %all-to-all-start.5) | async-done | bytes 106528 | tf_op jit(solution)/shard_map/all_to_all | solution.py:27
  193.6 33.1 %all_to_all.62 = bf16[8,12,512]{2,1,0:T(8,128)(2,1)S(1)} all-to-all(bf16[8,12,512]{2,1,0:T(8,128)(2,1)S(1)} %broadcast_in_dim.341), channel_id=1, replica_groups=mesh['grp'=2,'far'=8,'near'=4,'dp'=8] {'far'}, dimensions={0} | all-to-all | bytes 196608 | tf_op jit(solution)/shard_map/all_to_all | solution.py:21
  226.7 0.8 broadcast_in_dim.343
  227.5 3.9 %all-to-all-start.7 = ((bf16[4,96,512]{2,1,0:T(8,128)(2,1)}), bf16[4,96,512]{2,1,0:T(8,128)(2,1)S(1)}, u32[]{:S(2)}, u32[]{:S(2)}) async-start(bf16[4,96,512]{2,1,0:T(8,128)(2,1)} %broadcast_in_dim.343), calls=%async_computation.7 | async-start | bytes 786432 | tf_op jit(solution)/shard_map/all_to_all | solution.py:21
  233.2 5.7 %all-to-all-done.7 = bf16[4,96,512]{2,1,0:T(8,128)(2,1)S(1)} async-done(((bf16[4,96,512]{2,1,0:T(8,128)(2,1)}), bf16[4,96,512]{2,1,0:T(8,128)(2,1)S(1)}, u32[]{:S(2)}, u32[]{:S(2)}) %all-to-all-start.7) | async-done | bytes 393248 | tf_op jit(solution)/shard_map/all_to_all | solution.py:21
  240.0 0.7 copy.552
  240.6 3.6 %all-to-all-start.8 = ((bf16[8,128,65]{1,2,0:T(8,128)(2,1)}), bf16[8,128,65]{1,2,0:T(8,128)(2,1)S(1)}, u32[]{:S(2)}, u32[]{:S(2)}) async-start(bf16[8,128,65]{1,2,0:T(8,128)(2,1)} %copy.552), calls=%async_computation.8 | async-start | bytes 294912 | tf_op jit(solution)/shard_map/all_to_all | solution.py:27
  244.4 5.9 %all-to-all-done.8 = bf16[8,128,65]{1,2,0:T(8,128)(2,1)S(1)} async-done(((bf16[8,128,65]{1,2,0:T(8,128)(2,1)}), bf16[8,128,65]{1,2,0:T(8,128)(2,1)S(1)}, u32[]{:S(2)}, u32[]{:S(2)}) %all-to-all-start.8) | async-done | bytes 133152 | tf_op jit(solution)/shard_map/all_to_all | solution.py:27
  255.8 8.7 %all_to_all.63 = bf16[8,128,65]{1,2,0:T(8,128)(2,1)S(1)} all-to-all(bf16[8,128,65]{1,2,0:T(8,128)(2,1)S(1)} %broadcast_in_dim.344), channel_id=1, replica_groups=mesh['grp'=2,'far'=8,'near'=4,'dp'=8] {'dp'}, dimensions={0} | all-to-all | bytes 266240 | tf_op jit(solution)/shard_map/all_to_all | solution.py:21
  265.2 0.8 copy.662
  266.0 0.7 pad_maximum_fusion
  266.9 29.0 %all_to_all.64 = bf16[4,264,512]{2,1,0:T(8,128)(2,1)S(1)} all-to-all(bf16[4,264,512]{2,1,0:T(8,128)(2,1)S(1)} %copy.577), channel_id=1, replica_groups=mesh['grp'=2,'far'=8,'near'=4,'dp'=8] {'near'}, dimensions={0} | all-to-all | bytes 2162688 | tf_op jit(solution)/shard_map/all_to_all | solution.py:27
  296.2 0.8 reshape.1076
  297.0 6.1 %all-to-all-start.11 = ((bf16[8,33,512]{2,1,0:T(8,128)(2,1)}), bf16[8,33,512]{2,1,0:T(8,128)(2,1)S(1)}, u32[]{:S(2)}, u32[]{:S(2)}) async-start(bf16[8,33,512]{2,1,0:T(8,128)(2,1)} %reshape.1076), calls=%async_computation.11 | async-start | bytes 655360 | tf_op jit(solution)/shard_map/all_to_all | solution.py:27
  304.9 0.6 pad_maximum_fusion.3
  305.6 0.6 pad_maximum_fusion.2
  306.2 40.7 %all-to-all-done.11 = bf16[8,33,512]{2,1,0:T(8,128)(2,1)S(1)} async-done(((bf16[8,33,512]{2,1,0:T(8,128)(2,1)}), bf16[8,33,512]{2,1,0:T(8,128)(2,1)S(1)}, u32[]{:S(2)}, u32[]{:S(2)}) %all-to-all-start.11) | async-done | bytes 270368 | tf_op jit(solution)/shard_map/all_to_all | solution.py:27
  347.0 0.8 fusion.30
  (306 shorter events, 21.1 us)
Async XLA Ops:
  84.5 4.0 %copy-start.9 = (s32[128]{0:T(128)S(1)}, s32[128]{0:T(128)}, u32[]{:S(2)}) copy-start(s32[128]{0:T(128)} %param.17) | copy-start | bytes 1540
  84.5 4.3 %copy-start.11 = (f32[2,256]{1,0:T(2,128)S(1)}, f32[2,256]{1,0:T(2,128)}, u32[]{:S(2)}) copy-start(f32[2,256]{1,0:T(2,128)} %param.22) | copy-start | bytes 6148
  84.5 4.3 %copy-start.12 = (f32[2,256]{1,0:T(2,128)S(1)}, f32[2,256]{1,0:T(2,128)}, u32[]{:S(2)}) copy-start(f32[2,256]{1,0:T(2,128)} %param.23) | copy-start | bytes 6148
  84.5 4.6 %slice-start.1 = ((f32[2,16,256]{2,1,0:T(8,128)}), f32[1,16,256]{2,1,0:T(8,128)S(1)}, s32[]{:S(2)}) async-start(f32[2,16,256]{2,1,0:T(8,128)} %param.18), calls=%async_computation.13 | async-start | bytes 32768 | tf_op jit(solution)/shard_map/slice | solution.py:129
  84.5 4.7 %slice-start = ((f32[2,16,256]{2,1,0:T(8,128)}), f32[1,16,256]{2,1,0:T(8,128)S(1)}, s32[]{:S(2)}) async-start(f32[2,16,256]{2,1,0:T(8,128)} %param.19), calls=%async_computation.12 | async-start | bytes 32768 | tf_op jit(solution)/shard_map/slice | solution.py:129
  84.5 5.2 %copy-start.13 = (f32[2,4]{1,0:T(2,128)S(1)}, f32[2,4]{1,0:T(2,128)}, u32[]{:S(2)}) copy-start(f32[2,4]{1,0:T(2,128)} %param.24) | copy-start | bytes 100
  84.5 5.2 %copy-start.10 = (f32[2,512]{1,0:T(2,128)S(1)}, f32[2,512]{1,0:T(2,128)}, u32[]{:S(2)}) copy-start(f32[2,512]{1,0:T(2,128)} %param.20) | copy-start | bytes 12292
  84.6 24.8 %all-to-all-start.1 = ((bf16[4,256,512]{2,1,0:T(8,128)(2,1)}), bf16[4,256,512]{2,1,0:T(8,128)(2,1)S(1)}, u32[]{:S(2)}, u32[]{:S(2)}) async-start(bf16[4,256,512]{2,1,0:T(8,128)(2,1)} %broadcast_in_dim.321), calls=%async_computation.1 | async-start | bytes 2097152 | tf_op jit(solution)/shard_map/all_to_all | solution.py:21
  89.7 20.1 %copy-start.4 = (bf16[2,512,64]{1,2,0:T(8,128)(2,1)S(1)}, bf16[2,512,64]{1,2,0:T(8,128)(2,1)}, u32[]{:S(2)}) copy-start(bf16[2,512,64]{1,2,0:T(8,128)(2,1)} %param.21) | copy-start | bytes 393220
  110.4 6.1 %copy-start.14 = (f32[2,64]{1,0:T(2,128)S(1)}, f32[2,64]{1,0:T(2,128)}, u32[]{:S(2)}) copy-start(f32[2,64]{1,0:T(2,128)} %param.30) | copy-start | bytes 1540
  110.4 6.1 %copy-start.15 = (f32[2,64]{1,0:T(2,128)S(1)}, f32[2,64]{1,0:T(2,128)}, u32[]{:S(2)}) copy-start(f32[2,64]{1,0:T(2,128)} %param.29) | copy-start | bytes 1540
  110.9 12.2 %copy-start.2 = (f32[2,4,64,16]{2,3,1,0:T(8,128)S(1)}, f32[2,4,64,16]{2,3,1,0:T(8,128)}, u32[]{:S(2)}) copy-start(f32[2,4,64,16]{2,3,1,0:T(8,128)} %param.26) | copy-start | bytes 98308
  110.9 12.2 %copy-start.3 = (f32[2,4,64,16]{2,3,1,0:T(8,128)S(1)}, f32[2,4,64,16]{2,3,1,0:T(8,128)}, u32[]{:S(2)}) copy-start(f32[2,4,64,16]{2,3,1,0:T(8,128)} %param.25) | copy-start | bytes 98308
  111.9 10.9 %all-to-all-start.2 = ((bf16[8,128,65]{1,2,0:T(8,128)(2,1)}), bf16[8,128,65]{1,2,0:T(8,128)(2,1)S(1)}, u32[]{:S(2)}, u32[]{:S(2)}) async-start(bf16[8,128,65]{1,2,0:T(8,128)(2,1)} %copy.520), calls=%async_computation.2 | async-start | bytes 294912 | tf_op jit(solution)/shard_map/all_to_all | solution.py:27
  122.8 0.9 copy-start
  122.8 1.0 copy-start.1
  127.7 10.5 %copy-start.5 = (bf16[2,64,512]{2,1,0:T(8,128)(2,1)S(1)}, bf16[2,64,512]{2,1,0:T(8,128)(2,1)}, u32[]{:S(2)}) copy-start(bf16[2,64,512]{2,1,0:T(8,128)(2,1)} %param.31) | copy-start | bytes 393220
  127.7 9.8 %all-to-all-start.3 = ((bf16[8,128,65]{1,2,0:T(8,128)(2,1)}), bf16[8,128,65]{1,2,0:T(8,128)(2,1)S(1)}, u32[]{:S(2)}, u32[]{:S(2)}) async-start(bf16[8,128,65]{1,2,0:T(8,128)(2,1)} %broadcast_in_dim.340), calls=%async_computation.3 | async-start | bytes 294912 | tf_op jit(solution)/shard_map/all_to_all | solution.py:21
  156.5 36.8 %all-to-all-start.5 = ((bf16[8,13,512]{2,1,0:T(8,128)(2,1)}), bf16[8,13,512]{2,1,0:T(8,128)(2,1)S(1)}, u32[]{:S(2)}, u32[]{:S(2)}) async-start(bf16[8,13,512]{2,1,0:T(8,128)(2,1)} %reshape.1069), calls=%async_computation.5 | async-start | bytes 262144 | tf_op jit(solution)/shard_map/all_to_all | solution.py:27
  227.5 11.4 %all-to-all-start.7 = ((bf16[4,96,512]{2,1,0:T(8,128)(2,1)}), bf16[4,96,512]{2,1,0:T(8,128)(2,1)S(1)}, u32[]{:S(2)}, u32[]{:S(2)}) async-start(bf16[4,96,512]{2,1,0:T(8,128)(2,1)} %broadcast_in_dim.343), calls=%async_computation.7 | async-start | bytes 786432 | tf_op jit(solution)/shard_map/all_to_all | solution.py:21
  239.1 5.2 %copy-start.6 = (f32[2,16,256]{2,1,0:T(8,128)S(1)}, f32[2,16,256]{2,1,0:T(8,128)}, u32[]{:S(2)}) copy-start(f32[2,16,256]{2,1,0:T(8,128)} %param.19) | copy-start | bytes 98308
  239.1 5.2 %copy-start.7 = (f32[2,16,256]{2,1,0:T(8,128)S(1)}, f32[2,16,256]{2,1,0:T(8,128)}, u32[]{:S(2)}) copy-start(f32[2,16,256]{2,1,0:T(8,128)} %param.18) | copy-start | bytes 98308
  240.6 9.6 %all-to-all-start.8 = ((bf16[8,128,65]{1,2,0:T(8,128)(2,1)}), bf16[8,128,65]{1,2,0:T(8,128)(2,1)S(1)}, u32[]{:S(2)}, u32[]{:S(2)}) async-start(bf16[8,128,65]{1,2,0:T(8,128)(2,1)} %copy.552), calls=%async_computation.8 | async-start | bytes 294912 | tf_op jit(solution)/shard_map/all_to_all | solution.py:27
  297.0 50.0 %all-to-all-start.11 = ((bf16[8,33,512]{2,1,0:T(8,128)(2,1)}), bf16[8,33,512]{2,1,0:T(8,128)(2,1)S(1)}, u32[]{:S(2)}, u32[]{:S(2)}) async-start(bf16[8,33,512]{2,1,0:T(8,128)(2,1)} %reshape.1076), calls=%async_computation.11 | async-start | bytes 655360 | tf_op jit(solution)/shard_map/all_to_all | solution.py:27
  303.8 43.3 %copy-start.8 = (bf16[4,8,512]{2,1,0:T(8,128)(2,1)S(1)}, bf16[4,8,512]{2,1,0:T(8,128)(2,1)}, u32[]{:S(2)}) copy-start(bf16[4,8,512]{2,1,0:T(8,128)(2,1)} %param.16) | copy-start | bytes 98308

commit v2 on v1

v2 whole, which is shorter than its diff:
```python
import math

import jax
import jax.numpy as jnp
from jax import lax
from jax.sharding import Mesh, PartitionSpec as P

D = 4096
CHANNELS = 2048


EPSILON = 1e-06
NEAR = 4
LANES = 128


def from_everyone(shard, axis):
    peers = lax.axis_size(axis)
    return lax.all_to_all(
        jnp.broadcast_to(shard[None], (peers, *shard.shape)), axis, 0, 0, tiled=True
    )


def permuted_from_near(shard):
    peers = lax.axis_size("near")
    mine = lax.axis_index("near")
    came = [shard] + [
        lax.ppermute(shard, "near", [(p, p ^ d) for p in range(peers)]) for d in range(1, peers)
    ]
    bit = 1
    while bit < peers:
        odd = (mine & bit) != 0
        came = [jnp.where(odd, came[p ^ bit], came[p]) for p in range(peers)]
        bit *= 2
    return jnp.stack(came)


def exchanged(pieces, axis):
    return lax.all_to_all(pieces, axis, 0, 0, tiled=True)


def in_lanes(block, squares):
    spare = -(block.shape[-1] + 1) % LANES
    row = jnp.concatenate(
        [block.astype(jnp.bfloat16), squares[..., None].astype(jnp.bfloat16)], axis=-1
    )
    return jnp.pad(row, [(0, 0)] * (row.ndim - 1) + [(0, spare)])


def summed_over_far(partial, squares):
    far, rows, width = partial.shape
    cuts = range(0, width, LANES)
    last = jnp.pad(squares[:, None], [(0, 0), (0, 7), (0, LANES - rows)])
    pieces = jnp.concatenate(
        [partial[..., c : c + LANES] for c in cuts] + [last], axis=1
    ).astype(jnp.bfloat16)
    total = jnp.sum(exchanged(pieces, "far").astype(jnp.float32), axis=0)
    product = jnp.concatenate(
        [total[i * rows : (i + 1) * rows] for i in range(len(cuts))], axis=-1
    )
    return product, total[len(cuts) * rows, :rows]


def recur(
    driven,
    seq_lengths,
    state_re,
    state_im,
    decay_rate,
    frequency,
    log_step,
    in_re,
    in_im,
    readout_real,
    readout_imaginary,
    skip_scale,
):
    seq_count, step_count, chan_count = driven.shape
    channel_groups = log_step.shape[0]
    step_dt = jnp.exp(log_step)[:, None]
    real_part = -decay_rate.reshape(channel_groups, -1)
    imag_part = frequency.reshape(channel_groups, -1)
    magnitude = jnp.exp(real_part * step_dt)
    carry_re = magnitude * jnp.cos(imag_part * step_dt)
    carry_im = magnitude * jnp.sin(imag_part * step_dt)
    denominator = real_part * real_part + imag_part * imag_part
    factor_re = ((carry_re - 1.0) * real_part + carry_im * imag_part) / denominator
    factor_im = (carry_im * real_part - (carry_re - 1.0) * imag_part) / denominator
    input_re = factor_re[..., None] * in_re - factor_im[..., None] * in_im
    input_im = factor_re[..., None] * in_im + factor_im[..., None] * in_re
    group_split_rows = driven.astype(jnp.float32).reshape(seq_count, step_count, channel_groups, -1)
    pushed_re = jnp.einsum("gpc,stgc->stgp", input_re, group_split_rows)
    pushed_im = jnp.einsum("gpc,stgc->stgp", input_im, group_split_rows)
    hidden_real = state_re.reshape(seq_count, channel_groups, -1)
    hidden_imaginary = state_im.reshape(seq_count, channel_groups, -1)
    positions = jnp.arange(step_count, dtype=jnp.int32)
    live = positions[None, :] < seq_lengths[:, None]
    layer_outputs = []
    for tok_step in range(step_count):
        active = live[:, tok_step][:, None, None]
        next_re = carry_re * hidden_real - carry_im * hidden_imaginary + pushed_re[:, tok_step]
        next_im = carry_re * hidden_imaginary + carry_im * hidden_real + pushed_im[:, tok_step]
        hidden_real = jnp.where(active, next_re, hidden_real)
        hidden_imaginary = jnp.where(active, next_im, hidden_imaginary)
        layer_outputs.append(
            jnp.einsum("jlb,wjb->wjl", readout_real, hidden_real)
            - jnp.einsum("jlb,wjb->wjl", readout_imaginary, hidden_imaginary)
        )
    readout = jnp.stack(layer_outputs, axis=1).reshape(seq_count, step_count, chan_count)
    readout = jax.nn.gelu(readout + skip_scale * driven.astype(jnp.float32))
    readout = jnp.where(live[..., None], readout, 0.0)
    return (hidden_real.reshape(seq_count, -1), hidden_imaginary.reshape(seq_count, -1), readout)


def layer(rows, depth, lengths, gain_row, near_in, near_out, states, weights, gain_out):
    near, far, dp = (lax.axis_size(a) for a in ("near", "far", "dp"))
    own, width = rows.shape
    channels = near_in.shape[1]
    seqs = lengths.shape[0]

    values = from_everyone(rows, "far").astype(jnp.float32)
    squares = jnp.sum(values * values, axis=-1)
    scaled = (values * gain_row).astype(jnp.bfloat16).reshape(far * own, width)
    product = lax.dot_general(
        scaled,
        near_in.reshape(near * channels, width),
        (((1,), (1,)), ((), ())),
        preferred_element_type=jnp.float32,
    ).reshape(far, own, near * channels)
    pieces = jnp.stack(
        [in_lanes(product[..., n * channels : (n + 1) * channels], squares) for n in range(near)]
    )
    arrived = exchanged(pieces.reshape(near * dp, own, -1), ("near", "dp"))
    total = arrived.reshape(near, dp, own, -1).astype(jnp.float32).sum(axis=1)
    total = total.reshape(near * own, -1)
    inv_rms = lax.rsqrt(total[:, channels : channels + 1] / D + EPSILON)
    driven = (inv_rms * total[:, :channels]).astype(jnp.bfloat16)
    new_re, new_im, readout = recur(
        driven.reshape(seqs, -1, channels), lengths, *states, *weights
    )
    readout = readout.reshape(near, own, channels)

    sent = in_lanes(readout * gain_out, jnp.sum(readout * readout, axis=-1))
    pieces = jnp.broadcast_to(sent[:, None], (near, dp, *sent.shape[1:]))
    arrived = exchanged(pieces.reshape(near * dp, own, -1), ("near", "dp"))
    arrived = arrived.reshape(near, dp * own, -1)
    branch = jnp.concatenate([arrived[n, :, :channels] for n in range(near)], axis=-1)
    branch_sq = arrived[:, :, channels].astype(jnp.float32).sum(axis=0)
    partial = jnp.dot(
        branch, near_out.reshape(near * channels, width), preferred_element_type=jnp.float32
    )
    mixed, branch_sq = summed_over_far(
        partial.astype(jnp.bfloat16).reshape(far, own, width), branch_sq.reshape(far, own)
    )
    inv_out = lax.rsqrt(branch_sq / CHANNELS + EPSILON)
    updated = (rows.astype(jnp.float32) + mixed * inv_out[:, None]).astype(jnp.bfloat16)
    return updated, new_re, new_im


def per_device(
    tokens,
    seq_lengths,
    state_re,
    state_im,
    gain_in,
    w_in,
    decay_rate,
    frequency,
    log_step,
    in_re,
    in_im,
    readout_real,
    readout_imaginary,
    skip_scale,
    gain_out,
    w_out,
):
    seq_local, steps, width = tokens.shape
    layers, seqs_state = state_re.shape[:2]
    state_start = lax.axis_index("dp") * seqs_state
    lengths = lax.dynamic_slice_in_dim(seq_lengths, state_start, seqs_state, 0)
    weights = (
        decay_rate,
        frequency,
        log_step,
        in_re,
        in_im,
        readout_real,
        readout_imaginary,
        skip_scale,
    )
    near_both = [
        permuted_from_near(jnp.stack([w_in[d].T, w_out[d]])) for d in range(layers)
    ]
    near_in = [both[:, 0] for both in near_both]
    near_out = [both[:, 1] for both in near_both]
    current = tokens.reshape(seq_local * steps, width)
    finals_re = []
    finals_im = []
    for depth in range(layers):
        current, new_re, new_im = layer(
            current,
            depth,
            lengths,
            gain_in[depth],
            near_in[depth],
            near_out[depth],
            (state_re[depth], state_im[depth]),
            [w[depth] for w in weights],
            gain_out[depth],
        )
        finals_re.append(new_re)
        finals_im.append(new_im)
    return (current.reshape(tokens.shape), jnp.stack(finals_re), jnp.stack(finals_im))


def solution(mesh):
    grp, tp, dp = (mesh.shape[a] for a in ("grp", "tp", "dp"))
    split = Mesh(
        mesh.devices.reshape(grp, tp // NEAR, NEAR, dp), ("grp", "far", "near", "dp")
    )
    tp = ("far", "near")
    in_specs = (
        P(("grp", "far", "near"), None, "dp"),
        P("grp"),
        P(None, ("grp", "dp"), tp),
        P(None, ("grp", "dp"), tp),
        P(None, "dp"),
        P(None, "dp", tp),
        P(None, tp),
        P(None, tp),
        P(None, tp),
        P(None, tp, None, None),
        P(None, tp, None, None),
        P(None, tp, None, None),
        P(None, tp, None, None),
        P(None, tp),
        P(None, tp),
        P(None, tp, "dp"),
    )
    out_specs = (
        P(("grp", "far", "near"), None, "dp"),
        P(None, ("grp", "dp"), tp),
        P(None, ("grp", "dp"), tp),
    )
    return jax.shard_map(
        per_device, mesh=split, in_specs=in_specs, out_specs=out_specs, check_vma=False
    )
```

time: 349 us -> 332 us (0.951)
  the two profiles are of different devices: /device:TPU:104 before, /device:TPU:105 now
where the time goes in v2:
time: 332 us; the launch traced here: 331 us
  starting transfers between devices  105 us (32%)
  waiting for transfers between devices  104 us (31%)
  blocking collectives  82.9 us (25%)
  local copies, waits for them, and re-layouts  22.7 us (7%)
  other arithmetic  7.59 us (2%)
  matrix products  5.91 us (2%)
    all_to_all x3, blocking collectives, exchanged(): return lax.all_to_all(pieces, axis, 0, 0, tiled=True)  82.9 us
    all_to_all x3, waiting for transfers between devices, exchanged(): return lax.all_to_all(pieces, axis, 0, 0, tiled=True)  50.8 us
    all_to_all x2, starting transfers between devices, from_everyone(): lax.all_to_all(jnp.broadcast_to(shard[None], (peers, *shard.shape)), axis...  46.1 us
    ppermute x6, waiting for transfers between devices, permuted_from_near(): lax.ppermute(shard, 'near', [(p, p ^ d) for p in range(peers)])  44.9 us
    all_to_all x3, starting transfers between devices, exchanged(): return lax.all_to_all(pieces, axis, 0, 0, tiled=True)  39.7 us
    ppermute x6, starting transfers between devices, permuted_from_near(): lax.ppermute(shard, 'near', [(p, p ^ d) for p in range(peers)])  19.5 us
    unnamed x54, local copies, waits for them, and re-layouts  9.54 us
    all_to_all x2, waiting for transfers between devices, from_everyone(): lax.all_to_all(jnp.broadcast_to(shard[None], (peers, *shard.shape)), axis...  8.68 us
  transfers between devices with their start and end apart: 11, of which 9 were waited for; matrix products, arithmetic and copies ran while one was open for 2% of the time, Pallas kernels for 0%

profile of v2, /device:TPU:105, one launch (start us, length us, event | category | flops | bytes accessed | tf_op | source)
XLA Modules:
  0.0 330.5 jit_solution(6985957732215936555)
XLA Ops:
  0.6 1.5 broadcast_in_dim.288
  2.1 42.4 %all-to-all-start = ((bf16[8,32,512]{2,1,0:T(8,128)(2,1)}), bf16[8,32,512]{2,1,0:T(8,128)(2,1)S(1)}, u32[]{:S(2)}, u32[]{:S(2)}) async-start(bf16[8,32,512]{2,1,0:T(8,128)(2,1)} %broadcast_in_dim.288), calls=%async_computation | async-start | bytes 524288 | tf_op jit(solution)/shard_map/all_to_all | solution.py:19
  44.5 0.9 copy-done.6
  45.5 3.5 %collective-permute-start = (bf16[2,64,512]{2,1,0:T(8,128)(2,1)S(1)}, bf16[2,64,512]{2,1,0:T(8,128)(2,1)S(1)}, u32[]{:S(2)}, u32[]{:S(2)}) collective-permute-start(bf16[2,64,512]{2,1,0:T(8,128)(2,1)S(1)} %pad_maximum_fusion.4), channel_id=1, source_target_pairs={{0,24},{8,16},{16,8},{24,0},{1,25},{9,17},{17,9},{25,1},{2,26},{10... | collective-permute-start | bytes 393224 | tf_op jit(solution)/shard_map/ppermute | solution.py:28
  49.0 3.3 collective-permute-start.1
  52.3 3.1 collective-permute-start.2
  56.1 20.4 %collective-permute-done = bf16[2,64,512]{2,1,0:T(8,128)(2,1)S(1)} collective-permute-done((bf16[2,64,512]{2,1,0:T(8,128)(2,1)S(1)}, bf16[2,64,512]{2,1,0:T(8,128)(2,1)S(1)}, u32[]{:S(2)}, u32[]{:S(2)}) %collective-permute-start) | collective-permute-done | bytes 131104 | tf_op jit(solution)/shard_map/ppermute | solution.py:28
  76.5 0.8 collective-permute-done.1
  77.4 0.8 collective-permute-done.2
  79.3 0.7 pad_maximum_fusion.2
  80.0 18.9 %all-to-all-start.1 = ((bf16[32,32,128]{2,1,0:T(8,128)(2,1)}), bf16[32,32,128]{2,1,0:T(8,128)(2,1)S(1)}, u32[]{:S(2)}, u32[]{:S(2)}) async-start(bf16[32,32,128]{2,1,0:T(8,128)(2,1)} %bitcast.17), calls=%async_computation.1 | async-start | bytes 524288 | tf_op jit(solution)/shard_map/all_to_all | solution.py:39
  99.2 0.7 slice-done.1
  100.1 0.7 slice-done
  103.6 5.3 %all-to-all-done.1 = bf16[32,32,128]{2,1,0:T(8,128)(2,1)S(1)} async-done(((bf16[32,32,128]{2,1,0:T(8,128)(2,1)}), bf16[32,32,128]{2,1,0:T(8,128)(2,1)S(1)}, u32[]{:S(2)}, u32[]{:S(2)}) %all-to-all-start.1) | async-done | bytes 262176 | tf_op jit(solution)/shard_map/all_to_all | solution.py:39
  110.7 0.8 copy-done
  115.9 14.7 %all_to_all.40 = bf16[32,32,128]{2,1,0:T(8,128)(2,1)S(1)} all-to-all(bf16[32,32,128]{2,1,0:T(8,128)(2,1)S(1)} %bitcast.613), channel_id=1, replica_groups=mesh['grp'=2,'far'=8,'near'=4,'dp'=8] {'near','dp'}, dimensions={0} | all-to-all | bytes 524288 | tf_op jit(solution)/shard_map/all_to_all | solution.py:39
  131.3 53.5 %all_to_all.41 = bf16[8,136,128]{2,1,0:T(8,128)(2,1)S(1)} all-to-all(bf16[8,136,128]{2,1,0:T(8,128)(2,1)S(1)} %constant_dynamic-update-slice_fusion.8), channel_id=1, replica_groups=mesh['grp'=2,'far'=8,'near'=4,'dp'=8] {'far'}, dimensions={0} | all-to-all | bytes 557056 | tf_op jit(solution)/shard_map/all_to_all | solution.py:39
  184.9 0.7 copy-done.2
  185.7 0.7 broadcast_in_dim.307
  186.4 3.7 %all-to-all-start.4 = ((bf16[8,32,512]{2,1,0:T(8,128)(2,1)}), bf16[8,32,512]{2,1,0:T(8,128)(2,1)S(1)}, u32[]{:S(2)}, u32[]{:S(2)}) async-start(bf16[8,32,512]{2,1,0:T(8,128)(2,1)} %broadcast_in_dim.307), calls=%async_computation.4 | async-start | bytes 524288 | tf_op jit(solution)/shard_map/all_to_all | solution.py:19
  190.2 2.5 collective-permute-start.3
  192.7 5.1 %collective-permute-start.4 = (bf16[2,64,512]{2,1,0:T(8,128)(2,1)S(1)}, bf16[2,64,512]{2,1,0:T(8,128)(2,1)S(1)}, u32[]{:S(2)}, u32[]{:S(2)}) collective-permute-start(bf16[2,64,512]{2,1,0:T(8,128)(2,1)S(1)} %pad_maximum_fusion.5), channel_id=1, source_target_pairs={{0,16},{8,24},{16,0},{24,8},{1,17},{9,25},{17,1},{25,9},{2,18},{10... | collective-permute-start | bytes 393224 | tf_op jit(solution)/shard_map/ppermute | solution.py:28
  197.8 2.0 collective-permute-start.5
  199.8 20.7 %collective-permute-done.3 = bf16[2,64,512]{2,1,0:T(8,128)(2,1)S(1)} collective-permute-done((bf16[2,64,512]{2,1,0:T(8,128)(2,1)S(1)}, bf16[2,64,512]{2,1,0:T(8,128)(2,1)S(1)}, u32[]{:S(2)}, u32[]{:S(2)}) %collective-permute-start.3) | collective-permute-done | bytes 131104 | tf_op jit(solution)/shard_map/ppermute | solution.py:28
  220.5 2.1 collective-permute-done.4
  222.7 8.7 %all-to-all-done.4 = bf16[8,32,512]{2,1,0:T(8,128)(2,1)S(1)} async-done(((bf16[8,32,512]{2,1,0:T(8,128)(2,1)}), bf16[8,32,512]{2,1,0:T(8,128)(2,1)S(1)}, u32[]{:S(2)}, u32[]{:S(2)}) %all-to-all-start.4) | async-done | bytes 262176 | tf_op jit(solution)/shard_map/all_to_all | solution.py:19
  232.3 0.7 pad_maximum_fusion.3
  233.0 9.5 %all-to-all-start.5 = ((bf16[32,32,128]{2,1,0:T(8,128)(2,1)}), bf16[32,32,128]{2,1,0:T(8,128)(2,1)S(1)}, u32[]{:S(2)}, u32[]{:S(2)}) async-start(bf16[32,32,128]{2,1,0:T(8,128)(2,1)} %bitcast.87), calls=%async_computation.5 | async-start | bytes 524288 | tf_op jit(solution)/shard_map/all_to_all | solution.py:39
  245.1 7.4 %all-to-all-done.5 = bf16[32,32,128]{2,1,0:T(8,128)(2,1)S(1)} async-done(((bf16[32,32,128]{2,1,0:T(8,128)(2,1)}), bf16[32,32,128]{2,1,0:T(8,128)(2,1)S(1)}, u32[]{:S(2)}, u32[]{:S(2)}) %all-to-all-start.5) | async-done | bytes 262176 | tf_op jit(solution)/shard_map/all_to_all | solution.py:39
  258.5 14.7 %all_to_all.42 = bf16[32,32,128]{2,1,0:T(8,128)(2,1)S(1)} all-to-all(bf16[32,32,128]{2,1,0:T(8,128)(2,1)S(1)} %bitcast.614), channel_id=1, replica_groups=mesh['grp'=2,'far'=8,'near'=4,'dp'=8] {'near','dp'}, dimensions={0} | all-to-all | bytes 524288 | tf_op jit(solution)/shard_map/all_to_all | solution.py:39
  277.1 11.3 %all-to-all-start.7 = ((bf16[8,136,128]{2,1,0:T(8,128)(2,1)}), bf16[8,136,128]{2,1,0:T(8,128)(2,1)S(1)}, u32[]{:S(2)}, u32[]{:S(2)}) async-start(bf16[8,136,128]{2,1,0:T(8,128)(2,1)} %constant_dynamic-update-slice_fusion.17), calls=%async_computation.7 | async-start | bytes 557056 | tf_op jit(solution)/shard_map/all_to_all | solution.py:39
  291.5 38.1 %all-to-all-done.7 = bf16[8,136,128]{2,1,0:T(8,128)(2,1)S(1)} async-done(((bf16[8,136,128]{2,1,0:T(8,128)(2,1)}), bf16[8,136,128]{2,1,0:T(8,128)(2,1)S(1)}, u32[]{:S(2)}, u32[]{:S(2)}) %all-to-all-start.7) | async-done | bytes 278560 | tf_op jit(solution)/shard_map/all_to_all | solution.py:39
  (302 shorter events, 28.8 us)
Async XLA Ops:
  2.1 42.4 %copy-start.5 = (bf16[2,512,64]{1,2,0:T(8,128)(2,1)S(1)}, bf16[2,512,64]{1,2,0:T(8,128)(2,1)}, u32[]{:S(2)}) copy-start(bf16[2,512,64]{1,2,0:T(8,128)(2,1)} %param.21) | copy-start | bytes 393220
  2.1 76.3 %all-to-all-start = ((bf16[8,32,512]{2,1,0:T(8,128)(2,1)}), bf16[8,32,512]{2,1,0:T(8,128)(2,1)S(1)}, u32[]{:S(2)}, u32[]{:S(2)}) async-start(bf16[8,32,512]{2,1,0:T(8,128)(2,1)} %broadcast_in_dim.288), calls=%async_computation | async-start | bytes 524288 | tf_op jit(solution)/shard_map/all_to_all | solution.py:19
  44.5 0.9 copy-start.6
  45.5 31.1 %collective-permute-start = (bf16[2,64,512]{2,1,0:T(8,128)(2,1)S(1)}, bf16[2,64,512]{2,1,0:T(8,128)(2,1)S(1)}, u32[]{:S(2)}, u32[]{:S(2)}) collective-permute-start(bf16[2,64,512]{2,1,0:T(8,128)(2,1)S(1)} %pad_maximum_fusion.4), channel_id=1, source_target_pairs={{0,24},{8,16},{16,8},{24,0},{1,25},{9,17},{17,9},{25,1},{2,26},{10... | collective-permute-start | bytes 393224 | tf_op jit(solution)/shard_map/ppermute | solution.py:28
  49.0 28.4 %collective-permute-start.1 = (bf16[2,64,512]{2,1,0:T(8,128)(2,1)S(1)}, bf16[2,64,512]{2,1,0:T(8,128)(2,1)S(1)}, u32[]{:S(2)}, u32[]{:S(2)}) collective-permute-start(bf16[2,64,512]{2,1,0:T(8,128)(2,1)S(1)} %pad_maximum_fusion.4), channel_id=1, source_target_pairs={{0,16},{8,24},{16,0},{24,8},{1,17},{9,25},{17,1},{25,9},{2,18},{10... | collective-permute-start | bytes 393224 | tf_op jit(solution)/shard_map/ppermute | solution.py:28
  52.3 25.9 %collective-permute-start.2 = (bf16[2,64,512]{2,1,0:T(8,128)(2,1)S(1)}, bf16[2,64,512]{2,1,0:T(8,128)(2,1)S(1)}, u32[]{:S(2)}, u32[]{:S(2)}) collective-permute-start(bf16[2,64,512]{2,1,0:T(8,128)(2,1)S(1)} %pad_maximum_fusion.4), channel_id=1, source_target_pairs={{0,8},{8,0},{16,24},{24,16},{1,9},{9,1},{17,25},{25,17},{2,10},{10... | collective-permute-start | bytes 393224 | tf_op jit(solution)/shard_map/ppermute | solution.py:28
  55.4 0.7 copy-start.9
  80.0 18.9 %copy-start.10 = (f32[2,256]{1,0:T(2,128)S(1)}, f32[2,256]{1,0:T(2,128)}, u32[]{:S(2)}) copy-start(f32[2,256]{1,0:T(2,128)} %param.22) | copy-start | bytes 6148
  80.0 19.0 %copy-start.11 = (f32[2,256]{1,0:T(2,128)S(1)}, f32[2,256]{1,0:T(2,128)}, u32[]{:S(2)}) copy-start(f32[2,256]{1,0:T(2,128)} %param.23) | copy-start | bytes 6148
  80.0 28.9 %all-to-all-start.1 = ((bf16[32,32,128]{2,1,0:T(8,128)(2,1)}), bf16[32,32,128]{2,1,0:T(8,128)(2,1)S(1)}, u32[]{:S(2)}, u32[]{:S(2)}) async-start(bf16[32,32,128]{2,1,0:T(8,128)(2,1)} %bitcast.17), calls=%async_computation.1 | async-start | bytes 524288 | tf_op jit(solution)/shard_map/all_to_all | solution.py:39
  99.2 0.7 slice-start.1
  100.0 0.7 slice-start
  100.8 0.7 copy-start.15
  102.1 0.7 copy-start.12
  102.8 0.7 copy-start.13
  102.8 0.7 copy-start.14
  109.3 0.8 copy-start.3
  109.3 0.9 copy-start.4
  110.6 0.8 copy-start
  111.7 0.8 copy-start.1
  184.9 0.8 copy-start.2
  186.4 45.0 %all-to-all-start.4 = ((bf16[8,32,512]{2,1,0:T(8,128)(2,1)}), bf16[8,32,512]{2,1,0:T(8,128)(2,1)S(1)}, u32[]{:S(2)}, u32[]{:S(2)}) async-start(bf16[8,32,512]{2,1,0:T(8,128)(2,1)} %broadcast_in_dim.307), calls=%async_computation.4 | async-start | bytes 524288 | tf_op jit(solution)/shard_map/all_to_all | solution.py:19
  190.2 30.3 %collective-permute-start.3 = (bf16[2,64,512]{2,1,0:T(8,128)(2,1)S(1)}, bf16[2,64,512]{2,1,0:T(8,128)(2,1)S(1)}, u32[]{:S(2)}, u32[]{:S(2)}) collective-permute-start(bf16[2,64,512]{2,1,0:T(8,128)(2,1)S(1)} %pad_maximum_fusion.5), channel_id=1, source_target_pairs={{0,24},{8,16},{16,8},{24,0},{1,25},{9,17},{17,9},{25,1},{2,26},{10... | collective-permute-start | bytes 393224 | tf_op jit(solution)/shard_map/ppermute | solution.py:28
  192.7 29.8 %collective-permute-start.4 = (bf16[2,64,512]{2,1,0:T(8,128)(2,1)S(1)}, bf16[2,64,512]{2,1,0:T(8,128)(2,1)S(1)}, u32[]{:S(2)}, u32[]{:S(2)}) collective-permute-start(bf16[2,64,512]{2,1,0:T(8,128)(2,1)S(1)} %pad_maximum_fusion.5), channel_id=1, source_target_pairs={{0,16},{8,24},{16,0},{24,8},{1,17},{9,25},{17,1},{25,9},{2,18},{10... | collective-permute-start | bytes 393224 | tf_op jit(solution)/shard_map/ppermute | solution.py:28
  197.8 24.7 %collective-permute-start.5 = (bf16[2,64,512]{2,1,0:T(8,128)(2,1)S(1)}, bf16[2,64,512]{2,1,0:T(8,128)(2,1)S(1)}, u32[]{:S(2)}, u32[]{:S(2)}) collective-permute-start(bf16[2,64,512]{2,1,0:T(8,128)(2,1)S(1)} %pad_maximum_fusion.5), channel_id=1, source_target_pairs={{0,8},{8,0},{16,24},{24,16},{1,9},{9,1},{17,25},{25,17},{2,10},{10... | collective-permute-start | bytes 393224 | tf_op jit(solution)/shard_map/ppermute | solution.py:28
  233.0 19.5 %all-to-all-start.5 = ((bf16[32,32,128]{2,1,0:T(8,128)(2,1)}), bf16[32,32,128]{2,1,0:T(8,128)(2,1)S(1)}, u32[]{:S(2)}, u32[]{:S(2)}) async-start(bf16[32,32,128]{2,1,0:T(8,128)(2,1)} %bitcast.87), calls=%async_computation.5 | async-start | bytes 524288 | tf_op jit(solution)/shard_map/all_to_all | solution.py:39
  244.0 0.8 copy-start.8
  244.2 0.8 copy-start.7
  277.1 52.5 %all-to-all-start.7 = ((bf16[8,136,128]{2,1,0:T(8,128)(2,1)}), bf16[8,136,128]{2,1,0:T(8,128)(2,1)S(1)}, u32[]{:S(2)}, u32[]{:S(2)}) async-start(bf16[8,136,128]{2,1,0:T(8,128)(2,1)} %constant_dynamic-update-slice_fusion.17), calls=%async_computation.7 | async-start | bytes 557056 | tf_op jit(solution)/shard_map/all_to_all | solution.py:39

commit v3 on v2

v3 whole, which is shorter than its diff:
```python
import functools

import jax
import jax.numpy as jnp
from jax import lax
from jax.experimental import pallas as pl
from jax.experimental.pallas import tpu as pltpu
from jax.sharding import Mesh, PartitionSpec as P

D = 4096
CHANNELS = 2048


EPSILON = 1e-06
NEAR = 4
LANES = 128


def from_everyone(shard, axis):
    peers = lax.axis_size(axis)
    return lax.all_to_all(
        jnp.broadcast_to(shard[None], (peers, *shard.shape)), axis, 0, 0, tiled=True
    )


def permuted_from_near(shard):
    peers = lax.axis_size("near")
    mine = lax.axis_index("near")
    came = [shard] + [
        lax.ppermute(shard, "near", [(p, p ^ d) for p in range(peers)]) for d in range(1, peers)
    ]
    bit = 1
    while bit < peers:
        odd = (mine & bit) != 0
        came = [jnp.where(odd, came[p ^ bit], came[p]) for p in range(peers)]
        bit *= 2
    return jnp.stack(came)


def exchanged(pieces, axis):
    return lax.all_to_all(pieces, axis, 0, 0, tiled=True)


def in_lanes(block, squares):
    spare = -(block.shape[-1] + 1) % LANES
    row = jnp.concatenate(
        [block.astype(jnp.bfloat16), squares[..., None].astype(jnp.bfloat16)], axis=-1
    )
    return jnp.pad(row, [(0, 0)] * (row.ndim - 1) + [(0, spare)])


def summed_over_far(partial, squares):
    far, rows, width = partial.shape
    cuts = range(0, width, LANES)
    last = jnp.pad(squares[:, None], [(0, 0), (0, 7), (0, LANES - rows)])
    pieces = jnp.concatenate(
        [partial[..., c : c + LANES] for c in cuts] + [last], axis=1
    ).astype(jnp.bfloat16)
    total = jnp.sum(exchanged(pieces, "far").astype(jnp.float32), axis=0)
    product = jnp.concatenate(
        [total[i * rows : (i + 1) * rows] for i in range(len(cuts))], axis=-1
    )
    return product, total[len(cuts) * rows, :rows]


def recurrence_weights(
    decay_rate, frequency, log_step, in_re, in_im, readout_real, readout_imaginary
):
    layers, groups, states, channels = in_re.shape
    step_dt = jnp.exp(log_step)[..., None]
    real_part = -decay_rate.reshape(layers, groups, states)
    imag_part = frequency.reshape(layers, groups, states)
    magnitude = jnp.exp(real_part * step_dt)
    carry_re = magnitude * jnp.cos(imag_part * step_dt)
    carry_im = magnitude * jnp.sin(imag_part * step_dt)
    denominator = real_part * real_part + imag_part * imag_part
    factor_re = (((carry_re - 1.0) * real_part + carry_im * imag_part) / denominator)[..., None]
    factor_im = ((carry_im * real_part - (carry_re - 1.0) * imag_part) / denominator)[..., None]
    carry = jnp.stack([carry_re, carry_im], axis=1).reshape(layers, 2, groups * states)
    same = jnp.eye(groups, dtype=jnp.float32)
    drive = jnp.stack(
        [factor_re * in_re - factor_im * in_im, factor_re * in_im + factor_im * in_re], axis=1
    )
    drive = drive.transpose(0, 2, 4, 1, 3)[:, :, :, :, None] * same[:, None, None, :, None]
    drive = drive.reshape(layers, groups * channels, -1)
    read = jnp.stack([readout_real, -readout_imaginary], axis=1)
    read = read.transpose(0, 1, 2, 4, 3)[:, :, :, :, None] * same[:, None, :, None]
    read = read.reshape(layers, -1, groups * channels)
    spare = LANES - groups * channels
    drive = jnp.pad(drive, [(0, 0), (0, spare), (0, 0)]).astype(jnp.bfloat16)
    read = jnp.pad(read, [(0, 0), (0, 0), (0, spare)]).astype(jnp.bfloat16)
    return carry, drive, read


def recur_kernel(
    depth, channels, steps, arrived, live, re, im, carry, drive, read, skip, gain, *rest
):
    if depth:
        done_re, done_im, sent, final_re, final_im, hidden = rest
        final_re[:depth] = done_re[...]
        final_im[:depth] = done_im[...]
    else:
        sent, final_re, final_im, hidden = rest
    seqs, states = re.shape[1:]
    rows = seqs * steps
    total = arrived[:, 0].astype(jnp.float32)
    for j in range(1, arrived.shape[1]):
        total += arrived[:, j].astype(jnp.float32)
    total = total.reshape(rows, LANES)
    inv_rms = lax.rsqrt(total[:, channels : channels + 1] / D + EPSILON)
    driven = (total * inv_rms).astype(jnp.bfloat16)
    at = lax.broadcasted_iota(jnp.int32, (rows, rows), 0)
    to = lax.broadcasted_iota(jnp.int32, (rows, rows), 1)
    by_step = ((at % seqs) * steps + at // seqs == to).astype(jnp.bfloat16)
    by_seq = ((to % seqs) * steps + to // seqs == at).astype(jnp.bfloat16)
    driven = jnp.dot(by_step, driven, preferred_element_type=jnp.float32)
    pushed = jnp.dot(
        driven.astype(jnp.bfloat16), drive[depth], preferred_element_type=jnp.float32
    )
    carry_re, carry_im = carry[depth, 0:1], carry[depth, 1:2]
    real, imag = re[depth], im[depth]
    for t in range(steps):
        now = slice(t * seqs, (t + 1) * seqs)
        active = jnp.concatenate([live[now]] * (states // LANES), axis=1) > 0
        next_re = carry_re * real - carry_im * imag + pushed[now, :states]
        next_im = carry_re * imag + carry_im * real + pushed[now, states:]
        real = jnp.where(active, next_re, real)
        imag = jnp.where(active, next_im, imag)
        hidden[now, :states] = real.astype(jnp.bfloat16)
        hidden[now, states:] = imag.astype(jnp.bfloat16)
    final_re[depth] = real
    final_im[depth] = imag
    value = jnp.dot(hidden[...], read[depth], preferred_element_type=jnp.float32)
    value = value + skip[depth : depth + 1] * driven
    bent = 0.7978845608028654 * (value + 0.044715 * value * value * value)
    value = jnp.where(live[...] > 0, 0.5 * value * (1.0 + jnp.tanh(bent)), 0.0)
    squares = jnp.sum(value * value, axis=1, keepdims=True)
    lane = lax.broadcasted_iota(jnp.int32, (rows, LANES), 1)
    out = jnp.where(lane == channels, squares, value * gain[depth : depth + 1])
    out = jnp.dot(by_seq, out.astype(jnp.bfloat16), preferred_element_type=jnp.float32)
    sent[...] = out.reshape(sent.shape).astype(jnp.bfloat16)


def recur(depth, channels, arrived, live, states, weights, done):
    near, _, own, lanes = arrived.shape
    _, seqs, width = states[0].shape
    final = jax.ShapeDtypeStruct((depth + 1, seqs, width), jnp.float32)
    rows = near * own
    return pl.pallas_call(
        functools.partial(recur_kernel, depth, channels, rows // seqs),
        out_shape=(jax.ShapeDtypeStruct((near, own, lanes), jnp.bfloat16), final, final),
        scratch_shapes=[pltpu.VMEM((rows, 2 * width), jnp.bfloat16)],
        cost_estimate=pl.CostEstimate(
            flops=200_000_000, bytes_accessed=1 << 20, transcendentals=1 << 14
        ),
        name="recur",
    )(arrived, live, *states, *weights, *done)


def layer(rows, depth, channels, live, gain_row, near_in, to_near, states, weights, done):
    near, far, dp = (lax.axis_size(a) for a in ("near", "far", "dp"))
    own, width = rows.shape

    values = from_everyone(rows, "far").astype(jnp.float32)
    squares = jnp.sum(values * values, axis=-1)
    scaled = (values * gain_row).astype(jnp.bfloat16).reshape(far * own, width)
    product = lax.dot_general(
        scaled,
        near_in.reshape(near * channels, width),
        (((1,), (1,)), ((), ())),
        preferred_element_type=jnp.float32,
    ).reshape(far, own, near * channels)
    pieces = jnp.stack(
        [in_lanes(product[..., n * channels : (n + 1) * channels], squares) for n in range(near)]
    )
    to_near, pieces = lax.optimization_barrier((to_near, pieces))
    arrived = exchanged(pieces.reshape(near * dp, own, -1), ("near", "dp"))
    from_near, arrived = lax.optimization_barrier((permuted_from_near(to_near), arrived))
    near_out = from_near[:, 0]
    arrived = arrived.reshape(near, dp, own, -1)
    sent, *done = recur(depth, channels, arrived, live, states, weights, done)

    pieces = jnp.broadcast_to(sent[:, None], (near, dp, *sent.shape[1:]))
    arrived = exchanged(pieces.reshape(near * dp, own, -1), ("near", "dp"))
    arrived = arrived.reshape(near, dp * own, -1)
    branch = jnp.concatenate([arrived[n, :, :channels] for n in range(near)], axis=-1)
    branch_sq = arrived[:, :, channels].astype(jnp.float32).sum(axis=0)
    partial = jnp.dot(
        branch, near_out.reshape(near * channels, width), preferred_element_type=jnp.float32
    )
    mixed, branch_sq = summed_over_far(
        partial.astype(jnp.bfloat16).reshape(far, own, width), branch_sq.reshape(far, own)
    )
    inv_out = lax.rsqrt(branch_sq / CHANNELS + EPSILON)
    updated = (rows.astype(jnp.float32) + mixed * inv_out[:, None]).astype(jnp.bfloat16)
    return updated, done, from_near[:, -1]


def per_device(
    tokens,
    seq_lengths,
    state_re,
    state_im,
    gain_in,
    w_in,
    decay_rate,
    frequency,
    log_step,
    in_re,
    in_im,
    readout_real,
    readout_imaginary,
    skip_scale,
    gain_out,
    w_out,
):
    seq_local, steps, width = tokens.shape
    layers, seqs_state = state_re.shape[:2]
    state_start = lax.axis_index("dp") * seqs_state
    lengths = lax.dynamic_slice_in_dim(seq_lengths, state_start, seqs_state, 0)
    step = jnp.arange(steps, dtype=jnp.int32)[:, None, None]
    live = (step < lengths[None, :, None]).astype(jnp.float32)
    live = jnp.broadcast_to(live, (steps, seqs_state, LANES)).reshape(-1, LANES)
    channels = skip_scale.shape[1]
    in_all_lanes = [(0, 0), (0, LANES - channels)]
    weights = recurrence_weights(
        decay_rate, frequency, log_step, in_re, in_im, readout_real, readout_imaginary
    ) + (jnp.pad(skip_scale, in_all_lanes), jnp.pad(gain_out, in_all_lanes))
    near_in = permuted_from_near(w_in[0].T)
    current = tokens.reshape(seq_local * steps, width)
    done = ()
    for depth in range(layers):
        to_near = [w_out[depth]] + [w_in[d].T for d in range(depth + 1, layers)[:1]]
        current, done, near_in = layer(
            current,
            depth,
            channels,
            live,
            gain_in[depth],
            near_in,
            jnp.stack(to_near),
            (state_re, state_im),
            weights,
            done,
        )
    return (current.reshape(tokens.shape), *done)


def solution(mesh):
    grp, tp, dp = (mesh.shape[a] for a in ("grp", "tp", "dp"))
    split = Mesh(
        mesh.devices.reshape(grp, tp // NEAR, NEAR, dp), ("grp", "far", "near", "dp")
    )
    tp = ("far", "near")
    in_specs = (
        P(("grp", "far", "near"), None, "dp"),
        P("grp"),
        P(None, ("grp", "dp"), tp),
        P(None, ("grp", "dp"), tp),
        P(None, "dp"),
        P(None, "dp", tp),
        P(None, tp),
        P(None, tp),
        P(None, tp),
        P(None, tp, None, None),
        P(None, tp, None, None),
        P(None, tp, None, None),
        P(None, tp, None, None),
        P(None, tp),
        P(None, tp),
        P(None, tp, "dp"),
    )
    out_specs = (
        P(("grp", "far", "near"), None, "dp"),
        P(None, ("grp", "dp"), tp),
        P(None, ("grp", "dp"), tp),
    )
    return jax.shard_map(
        per_device, mesh=split, in_specs=in_specs, out_specs=out_specs, check_vma=False
    )
```

time: 332 us -> 331 us (level)
  the two profiles are of different devices: /device:TPU:105 before, /device:TPU:97 now
where the time goes in v3:
time: 331 us; the launch traced here: 330 us
  starting transfers between devices  111 us (34%)
  blocking collectives  111 us (34%)
  waiting for transfers between devices  75.4 us (23%)
  local copies, waits for them, and re-layouts  20.2 us (6%)
  Pallas kernels  5.15 us (2%)
  other arithmetic  4.51 us (1%)
    all_to_all x2, blocking collectives, exchanged(): return lax.all_to_all(pieces, axis, 0, 0, tiled=True)  67.8 us
    all_to_all x4, waiting for transfers between devices, exchanged(): return lax.all_to_all(pieces, axis, 0, 0, tiled=True)  52.8 us
    all_to_all x1, blocking collectives, from_everyone(): lax.all_to_all(jnp.broadcast_to(shard[None], (peers, *shard.shape)), axis...  43.1 us
    all_to_all x1, starting transfers between devices, from_everyone(): lax.all_to_all(jnp.broadcast_to(shard[None], (peers, *shard.shape)), axis...  42.4 us
    all_to_all x4, starting transfers between devices, exchanged(): return lax.all_to_all(pieces, axis, 0, 0, tiled=True)  40.4 us
    ppermute x9, starting transfers between devices, permuted_from_near(): lax.ppermute(shard, 'near', [(p, p ^ d) for p in range(peers)])  28.5 us
    ppermute x9, waiting for transfers between devices, permuted_from_near(): lax.ppermute(shard, 'near', [(p, p ^ d) for p in range(peers)])  19.2 us
    unnamed x40, local copies, waits for them, and re-layouts  8.82 us
  transfers between devices with their start and end apart: 14, of which 10 were waited for; matrix products, arithmetic and copies ran while one was open for 2% of the time, Pallas kernels for 0%

profile of v3, /device:TPU:97, one launch (start us, length us, event | category | flops | bytes accessed | tf_op | source)
XLA Modules:
  0.0 329.8 jit_solution(9964406156898708989)
XLA Ops:
  0.6 1.5 broadcast_in_dim.13
  2.1 42.4 %all-to-all-start = ((bf16[8,32,512]{2,1,0:T(8,128)(2,1)}), bf16[8,32,512]{2,1,0:T(8,128)(2,1)S(1)}, u32[]{:S(2)}, u32[]{:S(2)}) async-start(bf16[8,32,512]{2,1,0:T(8,128)(2,1)} %broadcast_in_dim.13), calls=%async_computation | async-start | bytes 524288 | tf_op jit(solution)/shard_map/all_to_all | solution.py:21
  44.5 3.7 %collective-permute-start = (bf16[64,512]{1,0:T(8,128)(2,1)S(1)}, bf16[64,512]{1,0:T(8,128)(2,1)S(1)}, u32[]{:S(2)}, u32[]{:S(2)}) collective-permute-start(bf16[64,512]{1,0:T(8,128)(2,1)S(1)} %get-tuple-element.63), channel_id=1, source_target_pairs={{0,24},{8,16},{16,8},{24,0},{1,25},{9,17},{17,9},{25,1},{2,26},{10... | collective-permute-start | bytes 196616 | tf_op jit(solution)/shard_map/ppermute | solution.py:30
  48.2 3.3 collective-permute-start.1
  51.5 3.1 collective-permute-start.2
  57.6 10.1 %collective-permute-done = bf16[64,512]{1,0:T(8,128)(2,1)S(1)} collective-permute-done((bf16[64,512]{1,0:T(8,128)(2,1)S(1)}, bf16[64,512]{1,0:T(8,128)(2,1)S(1)}, u32[]{:S(2)}, u32[]{:S(2)}) %collective-permute-start) | collective-permute-done | bytes 65568 | tf_op jit(solution)/shard_map/ppermute | solution.py:30
  67.8 0.8 collective-permute-done.1
  68.6 4.3 %collective-permute-done.2 = bf16[64,512]{1,0:T(8,128)(2,1)S(1)} collective-permute-done((bf16[64,512]{1,0:T(8,128)(2,1)S(1)}, bf16[64,512]{1,0:T(8,128)(2,1)S(1)}, u32[]{:S(2)}, u32[]{:S(2)}) %collective-permute-start.2) | collective-permute-done | bytes 65568 | tf_op jit(solution)/shard_map/ppermute | solution.py:30
  73.0 3.5 %all-to-all-done = bf16[8,32,512]{2,1,0:T(8,128)(2,1)S(1)} async-done(((bf16[8,32,512]{2,1,0:T(8,128)(2,1)}), bf16[8,32,512]{2,1,0:T(8,128)(2,1)S(1)}, u32[]{:S(2)}, u32[]{:S(2)}) %all-to-all-start) | async-done | bytes 262176 | tf_op jit(solution)/shard_map/all_to_all | solution.py:21
  78.1 19.0 %all-to-all-start.1 = ((bf16[32,32,128]{2,1,0:T(8,128)(2,1)}), bf16[32,32,128]{2,1,0:T(8,128)(2,1)S(1)}, u32[]{:S(2)}, u32[]{:S(2)}) async-start(bf16[32,32,128]{2,1,0:T(8,128)(2,1)} %bitcast.23), calls=%async_computation.1 | async-start | bytes 524288 | tf_op jit(solution)/shard_map/all_to_all | solution.py:41
  99.8 0.8 copy-done.8
  101.8 3.1 collective-permute-start.3
  104.9 3.0 collective-permute-start.4
  107.9 3.1 collective-permute-start.5
  114.4 1.5 collective-permute-done.4
  116.9 2.6 recur.2
  119.4 1.5 broadcast_in_dim.15
  120.9 10.2 %all-to-all-start.2 = ((bf16[32,32,128]{2,1,0:T(8,128)(2,1)}), bf16[32,32,128]{2,1,0:T(8,128)(2,1)S(1)}, u32[]{:S(2)}, u32[]{:S(2)}) async-start(bf16[32,32,128]{2,1,0:T(8,128)(2,1)} %bitcast.32), calls=%async_computation.2 | async-start | bytes 524288 | tf_op jit(solution)/shard_map/all_to_all | solution.py:41
  131.1 10.0 %all-to-all-done.2 = bf16[32,32,128]{2,1,0:T(8,128)(2,1)S(1)} async-done(((bf16[32,32,128]{2,1,0:T(8,128)(2,1)}), bf16[32,32,128]{2,1,0:T(8,128)(2,1)S(1)}, u32[]{:S(2)}, u32[]{:S(2)}) %all-to-all-start.2) | async-done | bytes 262176 | tf_op jit(solution)/shard_map/all_to_all | solution.py:41
  141.8 49.7 %all_to_all.40 = bf16[8,136,128]{2,1,0:T(8,128)(2,1)S(1)} all-to-all(bf16[8,136,128]{2,1,0:T(8,128)(2,1)S(1)} %constant_dynamic-update-slice_fusion), channel_id=1, replica_groups=mesh['grp'=2,'far'=8,'near'=4,'dp'=8] {'far'}, dimensions={0} | all-to-all | bytes 557056 | tf_op jit(solution)/shard_map/all_to_all | solution.py:41
  192.3 43.1 %all_to_all.41 = bf16[8,32,512]{2,1,0:T(8,128)(2,1)S(1)} all-to-all(bf16[8,32,512]{2,1,0:T(8,128)(2,1)S(1)} %broadcast_in_dim.16), channel_id=1, replica_groups=mesh['grp'=2,'far'=8,'near'=4,'dp'=8] {'far'}, dimensions={0} | all-to-all | bytes 524288 | tf_op jit(solution)/shard_map/all_to_all | solution.py:21
  237.0 6.9 %all-to-all-start.5 = ((bf16[32,32,128]{2,1,0:T(8,128)(2,1)}), bf16[32,32,128]{2,1,0:T(8,128)(2,1)S(1)}, u32[]{:S(2)}, u32[]{:S(2)}) async-start(bf16[32,32,128]{2,1,0:T(8,128)(2,1)} %bitcast.57), calls=%async_computation.5 | async-start | bytes 524288 | tf_op jit(solution)/shard_map/all_to_all | solution.py:41
  243.9 3.1 collective-permute-start.6
  247.1 3.0 collective-permute-start.7
  250.1 3.1 collective-permute-start.8
  253.2 2.3 collective-permute-done.6
  255.6 1.6 all-to-all-done.5
  257.9 2.6 recur.3
  260.5 0.8 broadcast_in_dim.17
  261.3 18.1 %all_to_all.42 = bf16[32,32,128]{2,1,0:T(8,128)(2,1)S(1)} all-to-all(bf16[32,32,128]{2,1,0:T(8,128)(2,1)S(1)} %bitcast.159), channel_id=1, replica_groups=mesh['grp'=2,'far'=8,'near'=4,'dp'=8] {'near','dp'}, dimensions={0} | all-to-all | bytes 524288 | tf_op jit(solution)/shard_map/all_to_all | solution.py:41
  283.3 4.4 %all-to-all-start.7 = ((bf16[8,136,128]{2,1,0:T(8,128)(2,1)}), bf16[8,136,128]{2,1,0:T(8,128)(2,1)S(1)}, u32[]{:S(2)}, u32[]{:S(2)}) async-start(bf16[8,136,128]{2,1,0:T(8,128)(2,1)} %constant_dynamic-update-slice_fusion.1), calls=%async_computation.7 | async-start | bytes 557056 | tf_op jit(solution)/shard_map/all_to_all | solution.py:41
  287.7 41.2 %all-to-all-done.7 = bf16[8,136,128]{2,1,0:T(8,128)(2,1)S(1)} async-done(((bf16[8,136,128]{2,1,0:T(8,128)(2,1)}), bf16[8,136,128]{2,1,0:T(8,128)(2,1)S(1)}, u32[]{:S(2)}, u32[]{:S(2)}) %all-to-all-start.7) | async-done | bytes 278560 | tf_op jit(solution)/shard_map/all_to_all | solution.py:41
  (136 shorter events, 21.3 us)
Async XLA Ops:
  2.1 42.4 %copy-start.3 = (bf16[2,512,64]{1,2,0:T(8,128)(2,1)S(1)}, bf16[2,512,64]{1,2,0:T(8,128)(2,1)}, u32[]{:S(2)}) copy-start(bf16[2,512,64]{1,2,0:T(8,128)(2,1)} %param.21) | copy-start | bytes 393220
  2.1 74.4 %all-to-all-start = ((bf16[8,32,512]{2,1,0:T(8,128)(2,1)}), bf16[8,32,512]{2,1,0:T(8,128)(2,1)S(1)}, u32[]{:S(2)}, u32[]{:S(2)}) async-start(bf16[8,32,512]{2,1,0:T(8,128)(2,1)} %broadcast_in_dim.13), calls=%async_computation | async-start | bytes 524288 | tf_op jit(solution)/shard_map/all_to_all | solution.py:21
  44.5 13.1 %copy-start.4 = (bf16[2,64,512]{2,1,0:T(8,128)(2,1)S(1)}, bf16[2,64,512]{2,1,0:T(8,128)(2,1)}, u32[]{:S(2)}) copy-start(bf16[2,64,512]{2,1,0:T(8,128)(2,1)} %param.31) | copy-start | bytes 393220
  44.5 23.2 %collective-permute-start = (bf16[64,512]{1,0:T(8,128)(2,1)S(1)}, bf16[64,512]{1,0:T(8,128)(2,1)S(1)}, u32[]{:S(2)}, u32[]{:S(2)}) collective-permute-start(bf16[64,512]{1,0:T(8,128)(2,1)S(1)} %get-tuple-element.63), channel_id=1, source_target_pairs={{0,24},{8,16},{16,8},{24,0},{1,25},{9,17},{17,9},{25,1},{2,26},{10... | collective-permute-start | bytes 196616 | tf_op jit(solution)/shard_map/ppermute | solution.py:30
  48.2 20.4 %collective-permute-start.1 = (bf16[64,512]{1,0:T(8,128)(2,1)S(1)}, bf16[64,512]{1,0:T(8,128)(2,1)S(1)}, u32[]{:S(2)}, u32[]{:S(2)}) collective-permute-start(bf16[64,512]{1,0:T(8,128)(2,1)S(1)} %get-tuple-element.63), channel_id=1, source_target_pairs={{0,16},{8,24},{16,0},{24,8},{1,17},{9,25},{17,1},{25,9},{2,18},{10... | collective-permute-start | bytes 196616 | tf_op jit(solution)/shard_map/ppermute | solution.py:30
  51.5 21.4 %collective-permute-start.2 = (bf16[64,512]{1,0:T(8,128)(2,1)S(1)}, bf16[64,512]{1,0:T(8,128)(2,1)S(1)}, u32[]{:S(2)}, u32[]{:S(2)}) collective-permute-start(bf16[64,512]{1,0:T(8,128)(2,1)S(1)} %get-tuple-element.63), channel_id=1, source_target_pairs={{0,8},{8,0},{16,24},{24,16},{1,9},{9,1},{17,25},{25,17},{2,10},{10... | collective-permute-start | bytes 196616 | tf_op jit(solution)/shard_map/ppermute | solution.py:30
  54.6 0.7 copy-start.12
  55.4 0.7 copy-start.9
  56.1 0.7 copy-start.11
  56.9 0.7 copy-start.10
  78.1 20.0 %copy-start.6 = (f32[2,4,64,16]{2,3,1,0:T(8,128)S(1)}, f32[2,4,64,16]{2,3,1,0:T(8,128)}, u32[]{:S(2)}) copy-start(f32[2,4,64,16]{2,3,1,0:T(8,128)} %param.26) | copy-start | bytes 98308
  78.1 20.0 %copy-start.7 = (f32[2,4,64,16]{2,3,1,0:T(8,128)S(1)}, f32[2,4,64,16]{2,3,1,0:T(8,128)}, u32[]{:S(2)}) copy-start(f32[2,4,64,16]{2,3,1,0:T(8,128)} %param.25) | copy-start | bytes 98308
  78.1 38.0 %all-to-all-start.1 = ((bf16[32,32,128]{2,1,0:T(8,128)(2,1)}), bf16[32,32,128]{2,1,0:T(8,128)(2,1)S(1)}, u32[]{:S(2)}, u32[]{:S(2)}) async-start(bf16[32,32,128]{2,1,0:T(8,128)(2,1)} %bitcast.23), calls=%async_computation.1 | async-start | bytes 524288 | tf_op jit(solution)/shard_map/all_to_all | solution.py:41
  97.3 0.7 copy-start.15
  98.9 0.8 copy-start.5
  99.8 0.8 copy-start.8
  101.8 12.6 %collective-permute-start.3 = (bf16[2,64,512]{2,1,0:T(8,128)(2,1)S(1)}, bf16[2,64,512]{2,1,0:T(8,128)(2,1)S(1)}, u32[]{:S(2)}, u32[]{:S(2)}) collective-permute-start(bf16[2,64,512]{2,1,0:T(8,128)(2,1)S(1)} %pad_maximum_fusion.5), channel_id=1, source_target_pairs={{0,24},{8,16},{16,8},{24,0},{1,25},{9,17},{17,9},{25,1},{2,26},{10... | collective-permute-start | bytes 393224 | tf_op jit(solution)/shard_map/ppermute | solution.py:30
  104.9 11.0 %collective-permute-start.4 = (bf16[2,64,512]{2,1,0:T(8,128)(2,1)S(1)}, bf16[2,64,512]{2,1,0:T(8,128)(2,1)S(1)}, u32[]{:S(2)}, u32[]{:S(2)}) collective-permute-start(bf16[2,64,512]{2,1,0:T(8,128)(2,1)S(1)} %pad_maximum_fusion.5), channel_id=1, source_target_pairs={{0,16},{8,24},{16,0},{24,8},{1,17},{9,25},{17,1},{25,9},{2,18},{10... | collective-permute-start | bytes 393224 | tf_op jit(solution)/shard_map/ppermute | solution.py:30
  107.9 8.1 %collective-permute-start.5 = (bf16[2,64,512]{2,1,0:T(8,128)(2,1)S(1)}, bf16[2,64,512]{2,1,0:T(8,128)(2,1)S(1)}, u32[]{:S(2)}, u32[]{:S(2)}) collective-permute-start(bf16[2,64,512]{2,1,0:T(8,128)(2,1)S(1)} %pad_maximum_fusion.5), channel_id=1, source_target_pairs={{0,8},{8,0},{16,24},{24,16},{1,9},{9,1},{17,25},{25,17},{2,10},{10... | collective-permute-start | bytes 393224 | tf_op jit(solution)/shard_map/ppermute | solution.py:30
  111.8 0.8 copy-start.13
  112.5 0.7 copy-start.14
  116.1 0.7 copy-start
  120.9 20.2 %all-to-all-start.2 = ((bf16[32,32,128]{2,1,0:T(8,128)(2,1)}), bf16[32,32,128]{2,1,0:T(8,128)(2,1)S(1)}, u32[]{:S(2)}, u32[]{:S(2)}) async-start(bf16[32,32,128]{2,1,0:T(8,128)(2,1)} %bitcast.32), calls=%async_computation.2 | async-start | bytes 524288 | tf_op jit(solution)/shard_map/all_to_all | solution.py:41
  191.5 0.8 copy-start.2
  237.0 20.2 %all-to-all-start.5 = ((bf16[32,32,128]{2,1,0:T(8,128)(2,1)}), bf16[32,32,128]{2,1,0:T(8,128)(2,1)S(1)}, u32[]{:S(2)}, u32[]{:S(2)}) async-start(bf16[32,32,128]{2,1,0:T(8,128)(2,1)} %bitcast.57), calls=%async_computation.5 | async-start | bytes 524288 | tf_op jit(solution)/shard_map/all_to_all | solution.py:41
  243.9 11.6 %collective-permute-start.6 = (bf16[1,64,512]{2,1,0:T(8,128)(2,1)S(1)}, bf16[1,64,512]{2,1,0:T(8,128)(2,1)S(1)}, u32[]{:S(2)}, u32[]{:S(2)}) collective-permute-start(bf16[1,64,512]{2,1,0:T(8,128)(2,1)S(1)} %get-tuple-element.22), channel_id=1, source_target_pairs={{0,24},{8,16},{16,8},{24,0},{1,25},{9,17},{17,9},{25,1},{2,26},{10... | collective-permute-start | bytes 196616 | tf_op jit(solution)/shard_map/ppermute | solution.py:30
  247.1 8.4 %collective-permute-start.7 = (bf16[1,64,512]{2,1,0:T(8,128)(2,1)S(1)}, bf16[1,64,512]{2,1,0:T(8,128)(2,1)S(1)}, u32[]{:S(2)}, u32[]{:S(2)}) collective-permute-start(bf16[1,64,512]{2,1,0:T(8,128)(2,1)S(1)} %get-tuple-element.22), channel_id=1, source_target_pairs={{0,16},{8,24},{16,0},{24,8},{1,17},{9,25},{17,1},{25,9},{2,18},{10... | collective-permute-start | bytes 196616 | tf_op jit(solution)/shard_map/ppermute | solution.py:30
  250.1 5.4 %collective-permute-start.8 = (bf16[1,64,512]{2,1,0:T(8,128)(2,1)S(1)}, bf16[1,64,512]{2,1,0:T(8,128)(2,1)S(1)}, u32[]{:S(2)}, u32[]{:S(2)}) collective-permute-start(bf16[1,64,512]{2,1,0:T(8,128)(2,1)S(1)} %get-tuple-element.22), channel_id=1, source_target_pairs={{0,8},{8,0},{16,24},{24,16},{1,9},{9,1},{17,25},{25,17},{2,10},{10... | collective-permute-start | bytes 196616 | tf_op jit(solution)/shard_map/ppermute | solution.py:30
  257.2 0.7 copy-start.1
  283.3 45.6 %all-to-all-start.7 = ((bf16[8,136,128]{2,1,0:T(8,128)(2,1)}), bf16[8,136,128]{2,1,0:T(8,128)(2,1)S(1)}, u32[]{:S(2)}, u32[]{:S(2)}) async-start(bf16[8,136,128]{2,1,0:T(8,128)(2,1)} %constant_dynamic-update-slice_fusion.1), calls=%async_computation.7 | async-start | bytes 557056 | tf_op jit(solution)/shard_map/all_to_all | solution.py:41

commit v4 on v3

v4 whole, which is shorter than its diff:
```python
import functools

import jax
import jax.numpy as jnp
from jax import lax
from jax.experimental import pallas as pl
from jax.experimental.pallas import tpu as pltpu
from jax.sharding import Mesh, PartitionSpec as P

D = 4096
CHANNELS = 2048


EPSILON = 1e-06
LIVE_PER_SEQ = 3
NEAR = 4
LANES = 128


def from_everyone(shard, axis):
    peers = lax.axis_size(axis)
    return lax.all_to_all(
        jnp.broadcast_to(shard[None], (peers, *shard.shape)), axis, 0, 0, tiled=True
    )


def permuted_from_near(shard):
    peers = lax.axis_size("near")
    mine = lax.axis_index("near")
    came = [shard] + [
        lax.ppermute(shard, "near", [(p, p ^ d) for p in range(peers)]) for d in range(1, peers)
    ]
    bit = 1
    while bit < peers:
        odd = (mine & bit) != 0
        came = [jnp.where(odd, came[p ^ bit], came[p]) for p in range(peers)]
        bit *= 2
    return jnp.stack(came)


def exchanged(pieces, axis):
    return lax.all_to_all(pieces, axis, 0, 0, tiled=True)


def in_lanes(block, squares):
    spare = -(block.shape[-1] + 1) % LANES
    row = jnp.concatenate(
        [block.astype(jnp.bfloat16), squares[..., None].astype(jnp.bfloat16)], axis=-1
    )
    return jnp.pad(row, [(0, 0)] * (row.ndim - 1) + [(0, spare)])


def recurrence_weights(
    decay_rate, frequency, log_step, in_re, in_im, readout_real, readout_imaginary
):
    layers, groups, states, channels = in_re.shape
    step_dt = jnp.exp(log_step)[..., None]
    real_part = -decay_rate.reshape(layers, groups, states)
    imag_part = frequency.reshape(layers, groups, states)
    magnitude = jnp.exp(real_part * step_dt)
    carry_re = magnitude * jnp.cos(imag_part * step_dt)
    carry_im = magnitude * jnp.sin(imag_part * step_dt)
    denominator = real_part * real_part + imag_part * imag_part
    factor_re = (((carry_re - 1.0) * real_part + carry_im * imag_part) / denominator)[..., None]
    factor_im = ((carry_im * real_part - (carry_re - 1.0) * imag_part) / denominator)[..., None]
    carry = jnp.stack([carry_re, carry_im], axis=1).reshape(layers, 2, groups * states)
    same = jnp.eye(groups, dtype=jnp.float32)
    drive = jnp.stack(
        [factor_re * in_re - factor_im * in_im, factor_re * in_im + factor_im * in_re], axis=1
    )
    drive = drive.transpose(0, 2, 4, 1, 3)[:, :, :, :, None] * same[:, None, None, :, None]
    drive = drive.reshape(layers, groups * channels, -1)
    read = jnp.stack([readout_real, -readout_imaginary], axis=1)
    read = read.transpose(0, 1, 2, 4, 3)[:, :, :, :, None] * same[:, None, :, None]
    read = read.reshape(layers, -1, groups * channels)
    spare = LANES - groups * channels
    drive = jnp.pad(drive, [(0, 0), (0, spare), (0, 0)]).astype(jnp.bfloat16)
    read = jnp.pad(read, [(0, 0), (0, 0), (0, spare)]).astype(jnp.bfloat16)
    return carry, drive, read


def product(left, right, dims):
    return lax.dot_general(left, right, (dims, ((), ())), preferred_element_type=jnp.float32)


def recur_kernel(
    depth, channels, steps, arrived, live, re, im, carry, drive, read, skip, gain, *rest
):
    first = depth == 0
    if first:
        sent, final_re, final_im, hidden = rest
    else:
        done_re, done_im, sent, final_re, final_im, hidden = rest
        final_re[:depth] = done_re[...]
        final_im[:depth] = done_im[...]
    seqs, states = re.shape[1:]
    rows = seqs * steps
    at = lax.broadcasted_iota(jnp.int32, (rows, rows), 0)
    to = lax.broadcasted_iota(jnp.int32, (rows, rows), 1)
    by_step = ((at % seqs) * steps + at // seqs == to).astype(jnp.bfloat16)
    if first:
        total = arrived[:, 0].astype(jnp.float32)
        for j in range(1, arrived.shape[1]):
            total += arrived[:, j].astype(jnp.float32)
        total = total.reshape(rows, LANES)
        inv_rms = lax.rsqrt(total[:, channels : channels + 1] / D + EPSILON)
        driven = (total * inv_rms).astype(jnp.bfloat16)
        driven = product(by_step, driven, ((1,), (0,)))
        matrix = drive[depth]
    else:
        total = jnp.sum(arrived[...].astype(jnp.float32), axis=0)
        inv_rms = lax.rsqrt(total[channels : channels + 1] / D + EPSILON)
        driven = (total * inv_rms).astype(jnp.bfloat16)
        driven = jnp.concatenate(
            [driven[:channels], jnp.zeros((LANES - channels, rows), jnp.bfloat16)], axis=0
        )
        driven = product(by_step, driven, ((1,), (1,)))
        matrix = drive[depth]
    pushed = product(driven.astype(jnp.bfloat16), matrix, ((1,), (0,)))
    carry_re, carry_im = carry[depth, 0:1], carry[depth, 1:2]
    real, imag = re[depth], im[depth]
    for t in range(steps):
        now = slice(t * seqs, (t + 1) * seqs)
        active = jnp.concatenate([live[now]] * (states // LANES), axis=1) > 0
        next_re = carry_re * real - carry_im * imag + pushed[now, :states]
        next_im = carry_re * imag + carry_im * real + pushed[now, states:]
        real = jnp.where(active, next_re, real)
        imag = jnp.where(active, next_im, imag)
        hidden[now, :states] = real.astype(jnp.bfloat16)
        hidden[now, states:] = imag.astype(jnp.bfloat16)
    final_re[depth] = real
    final_im[depth] = imag
    value = product(hidden[...], read[depth], ((1,), (0,)))
    value = value + skip[depth : depth + 1] * driven
    bent = 0.7978845608028654 * (value + 0.044715 * value * value * value)
    value = jnp.where(live[...] > 0, 0.5 * value * (1.0 + jnp.tanh(bent)), 0.0)
    squares = jnp.sum(value * value, axis=1, keepdims=True)
    lane = lax.broadcasted_iota(jnp.int32, (rows, LANES), 1)
    out = jnp.where(lane == channels, squares, value * gain[depth : depth + 1])
    out = out.astype(jnp.bfloat16)
    if first:
        out = product(out, by_step, ((0,), (0,)))
        sent[...] = out[: sent.shape[0]].astype(jnp.bfloat16)
    else:
        out = product(by_step, out, ((0,), (0,)))
        sent[...] = out.reshape(sent.shape).astype(jnp.bfloat16)


def call(kernel, out_shape, name, scratch_shapes=()):
    return pl.pallas_call(
        kernel,
        out_shape=out_shape,
        scratch_shapes=scratch_shapes,
        cost_estimate=pl.CostEstimate(
            flops=200_000_000, bytes_accessed=1 << 20, transcendentals=1 << 14
        ),
        name=name,
    )


def recur(depth, channels, out_dims, arrived, live, states, weights, done):
    _, seqs, width = states[0].shape
    rows = live.shape[0]
    final = jax.ShapeDtypeStruct((depth + 1, seqs, width), jnp.float32)
    return call(
        functools.partial(recur_kernel, depth, channels, rows // seqs),
        (jax.ShapeDtypeStruct(out_dims, jnp.bfloat16), final, final),
        "recur",
        [pltpu.VMEM((rows, 2 * width), jnp.bfloat16)],
    )(arrived, live, *states, *weights, *done)


def picked(token_of, place, pick):
    for j in range(place.shape[0]):
        here = token_of[...] == place[j : j + 1]
        pick[:, j * LANES : (j + 1) * LANES] = here.astype(jnp.float32).astype(jnp.bfloat16)


def live_out_kernel(channels, arrived, token_of, place, w_out, own, pieces, pick):
    near, slots = pieces.shape[0], token_of.shape[0] // pieces.shape[0]
    kept = pieces.shape[1] - 8 - own.shape[1]
    picked(token_of, place, pick)
    rows = jnp.concatenate([arrived[j] for j in range(arrived.shape[0])], axis=1)
    live = product(pick[...], rows, ((1,), (1,))).astype(jnp.bfloat16)
    partial = product(live, w_out[...], ((1,), (0,)))
    squares = product(rows[channels:], pick[...], ((1,), (1,)))
    for n in range(near):
        at = slice(n * slots, (n + 1) * slots)
        pieces[n, :kept] = partial[at][:kept].astype(jnp.bfloat16)
        pieces[n, kept : kept + 8, :slots] = squares[:, at].astype(jnp.bfloat16)
        pieces[n, kept : kept + 8, slots:] = jnp.zeros(
            (8, pieces.shape[2] - slots), jnp.bfloat16
        )
        pieces[n, kept + 8 :] = own[n]


def live_in_kernel(everyone, token_of, place, gain_row, w_in, pieces, pick):
    picked(token_of, place, pick)
    values = everyone[...].astype(jnp.float32)
    scaled = (values * gain_row[...]).astype(jnp.bfloat16)
    projected = product(w_in[...], scaled, ((1,), (1,)))
    ones = jnp.ones((8, values.shape[1]), jnp.bfloat16)
    squares = product(ones, (values * values).astype(jnp.bfloat16), ((1,), (1,)))
    both = jnp.concatenate([projected, squares], axis=0).astype(jnp.bfloat16)
    spread = product(both, pick[...], ((1,), (0,)))
    for j in range(place.shape[0]):
        pieces[j] = spread[:, j * LANES : (j + 1) * LANES].astype(jnp.bfloat16)


def out_kernel(channels, arrived, w_out, pieces):
    near, rows, _ = arrived.shape
    far, _, _ = pieces.shape
    own, width = rows // far, w_out.shape[2]
    lane = lax.broadcasted_iota(jnp.int32, (8, LANES), 1)
    one = (lane == channels).astype(jnp.float32).astype(jnp.bfloat16)
    partial = product(arrived[0], w_out[0], ((1,), (0,)))
    squares = product(one, arrived[0], ((1,), (1,)))
    for n in range(1, near):
        partial += product(arrived[n], w_out[n], ((1,), (0,)))
        squares += product(one, arrived[n], ((1,), (1,)))
    for f in range(far):
        for q in range(width // LANES):
            pieces[f, q * own : (q + 1) * own] = partial[
                f * own : (f + 1) * own, q * LANES : (q + 1) * LANES
            ].astype(jnp.bfloat16)
        last = squares[:, f * own : (f + 1) * own]
        last = jnp.concatenate([last, jnp.zeros((8, LANES - own), jnp.float32)], axis=1)
        pieces[f, width // LANES * own :] = last.astype(jnp.bfloat16)


def per_device(
    tokens,
    seq_lengths,
    state_re,
    state_im,
    gain_in,
    w_in,
    decay_rate,
    frequency,
    log_step,
    in_re,
    in_im,
    readout_real,
    readout_imaginary,
    skip_scale,
    gain_out,
    w_out,
):
    near, far, dp = (lax.axis_size(a) for a in ("near", "far", "dp"))
    here, place_far = lax.axis_index("near"), lax.axis_index("far")
    seq_local, steps, width = tokens.shape
    seqs_state = state_re.shape[1]
    channels = skip_scale.shape[1]
    spare = LANES - channels
    own = seq_local * steps
    kept = far * LIVE_PER_SEQ * seq_local
    live_own = LIVE_PER_SEQ * seq_local
    states = (state_re, state_im)
    tall = channels + 8

    lengths = lax.dynamic_slice_in_dim(
        seq_lengths, lax.axis_index("dp") * seqs_state, seqs_state, 0
    )
    step = jnp.arange(steps, dtype=jnp.int32)
    live = (step[:, None, None] < lengths[None, :, None]).astype(jnp.float32)
    live = jnp.broadcast_to(live, (steps, seqs_state, LANES)).reshape(-1, LANES)
    in_all_lanes = [(0, 0), (0, spare)]
    weights = recurrence_weights(
        decay_rate, frequency, log_step, in_re, in_im, readout_real, readout_imaginary
    ) + (jnp.pad(skip_scale, in_all_lanes), jnp.pad(gain_out, in_all_lanes))

    starts = jnp.cumsum(seq_lengths) - seq_lengths
    place = jnp.where(step < seq_lengths[:, None], starts[:, None] + step, -1)
    place = place.reshape(dp, -1)
    place_home = place.reshape(far, near, own)
    slot = jnp.arange(LANES, dtype=jnp.int32)
    token_of = (slot // live_own * near + jnp.arange(near)[:, None]) * live_own
    token_of = jnp.where(slot < kept, token_of + slot % live_own, -2)

    def in_lanes_of(slots):
        slots = slots.reshape(-1).astype(jnp.int32)
        return jnp.broadcast_to(slots[:, None], (slots.size, LANES))

    start = tokens.reshape(own, width)
    near_in = permuted_from_near(w_in[0].T)
    gathered = from_everyone(start, "far")
    values = gathered.astype(jnp.float32)
    squares = jnp.sum(values * values, axis=-1)
    scaled = (values * gain_in[0]).astype(jnp.bfloat16).reshape(far * own, width)
    projected = product(scaled, near_in.reshape(near * channels, width), ((1,), (1,)))
    projected = projected.reshape(far, own, near * channels)
    pieces = jnp.stack(
        [in_lanes(projected[..., n * channels : (n + 1) * channels], squares) for n in range(near)]
    )
    arrived = exchanged(pieces.reshape(near * dp, own, LANES), ("near", "dp"))
    sent, *done = recur(
        0, channels, (tall, LANES), arrived.reshape(near, dp, own, LANES), live, states, weights, ()
    )
    wanted = (place_far * near + jnp.arange(near)[:, None]) * live_own
    wanted = jnp.where(slot[:16] < live_own, wanted + slot[:16], -2).reshape(-1)
    held = lax.dynamic_slice_in_dim(place_home, here, 1, 1).reshape(-1)
    pick_held = (wanted[:, None] == held[None, :]).astype(jnp.bfloat16)
    handed = jnp.dot(
        pick_held, gathered.reshape(far * own, width), preferred_element_type=jnp.float32
    )
    handed = handed.astype(jnp.bfloat16).reshape(near, 16, width)
    arrived = from_everyone(sent, "dp")
    pieces = call(
        functools.partial(live_out_kernel, channels),
        jax.ShapeDtypeStruct((near, kept + 8 + 16, width), jnp.bfloat16),
        "live_out",
        [pltpu.VMEM((near * LANES, dp * LANES), jnp.bfloat16)],
    )(arrived, in_lanes_of(token_of), place, jnp.pad(w_out[0], [(0, 8), (0, 0)]), handed)
    part = jnp.sum(exchanged(pieces, "near").astype(jnp.float32), axis=0)
    before = part[kept + 8 : kept + 8 + live_own]
    last = part[kept, :kept].reshape(far, 1, live_own)
    last = jnp.pad(last, [(0, 0), (0, 0), (0, width - live_own)])
    pieces = jnp.concatenate([part[:kept].reshape(far, live_own, width), last], axis=1)
    total = jnp.sum(exchanged(pieces.astype(jnp.bfloat16), "far").astype(jnp.float32), axis=0)
    inv_out = lax.rsqrt(total[live_own, :live_own] / CHANNELS + EPSILON)
    current = (before + total[:live_own] * inv_out[:, None]).astype(jnp.bfloat16)

    to_near, current = lax.optimization_barrier((w_out[1], current))
    everyone = from_everyone(current, "far")
    near_out, everyone = lax.optimization_barrier((permuted_from_near(to_near), everyone))
    everyone = from_everyone(everyone.reshape(kept, width), "near").reshape(near * kept, width)
    compact = token_of[:, :kept].reshape(-1)
    pieces = call(
        live_in_kernel,
        jax.ShapeDtypeStruct((dp, tall, LANES), jnp.bfloat16),
        "live_in",
        [pltpu.VMEM((near * kept, dp * LANES), jnp.bfloat16)],
    )(everyone, in_lanes_of(compact), place, gain_in[1:2], w_in[1].T)
    arrived = exchanged(pieces, "dp")
    sent, *done = recur(
        1, channels, (near, own, LANES), arrived, live, states, weights, done
    )
    pieces = jnp.broadcast_to(sent[:, None], (near, dp, own, LANES))
    arrived = exchanged(pieces.reshape(near * dp, own, LANES), ("near", "dp"))
    deep = jnp.pad(near_out, [(0, 0), (0, spare), (0, 0)])
    rows_out = width // LANES * own
    pieces = call(
        functools.partial(out_kernel, channels),
        jax.ShapeDtypeStruct((far, rows_out + 8, LANES), jnp.bfloat16),
        "out",
    )(arrived.reshape(near, dp * own, LANES), deep)
    total = jnp.sum(exchanged(pieces, "far").astype(jnp.float32), axis=0)
    mixed = jnp.concatenate(
        [total[i * own : (i + 1) * own] for i in range(width // LANES)], axis=-1
    )
    inv_out = lax.rsqrt(total[rows_out, :own] / CHANNELS + EPSILON)
    place_own = lax.dynamic_slice_in_dim(held.reshape(far, own), place_far, 1, 0).reshape(own)
    pick_own = (place_own[:, None] == compact[None, :]).astype(jnp.bfloat16)
    after = jnp.dot(pick_own, everyone, preferred_element_type=jnp.float32)
    before = jnp.where((place_own >= 0)[:, None], after, start.astype(jnp.float32))
    result = (before + mixed * inv_out[:, None]).astype(jnp.bfloat16)
    return (result.reshape(tokens.shape), *done)


def solution(mesh):
    grp, tp, dp = (mesh.shape[a] for a in ("grp", "tp", "dp"))
    split = Mesh(
        mesh.devices.reshape(grp, tp // NEAR, NEAR, dp), ("grp", "far", "near", "dp")
    )
    tp = ("far", "near")
    in_specs = (
        P(("grp", "far", "near"), None, "dp"),
        P("grp"),
        P(None, ("grp", "dp"), tp),
        P(None, ("grp", "dp"), tp),
        P(None, "dp"),
        P(None, "dp", tp),
        P(None, tp),
        P(None, tp),
        P(None, tp),
        P(None, tp, None, None),
        P(None, tp, None, None),
        P(None, tp, None, None),
        P(None, tp, None, None),
        P(None, tp),
        P(None, tp),
        P(None, tp, "dp"),
    )
    out_specs = (
        P(("grp", "far", "near"), None, "dp"),
        P(None, ("grp", "dp"), tp),
        P(None, ("grp", "dp"), tp),
    )
    return jax.shard_map(
        per_device, mesh=split, in_specs=in_specs, out_specs=out_specs, check_vma=False
    )
```

time: 331 us -> 323 us (0.976)
  blocking collectives: 111 us -> 64.5 us
  waiting for transfers between devices: 75.4 us -> 107 us
  Pallas kernels: 5.15 us -> 13 us
  starting transfers between devices: 111 us -> 105 us
  local copies, waits for them, and re-layouts: 20.2 us -> 24.8 us
    all_to_all x1 -> x0, blocking collectives: 43.1 us -> none  [from_everyone(): lax.all_to_all(jnp.broadcast_to(shard[None], (peers, *shard.shape)), axis...]
    all_to_all x1 -> x4, waiting for transfers between devices: 3.52 us -> 45.9 us  [from_everyone(): lax.all_to_all(jnp.broadcast_to(shard[None], (peers, *shard.shape)), axis...]
    all_to_all x1 -> x4, starting transfers between devices: 42.4 us -> 57 us  [from_everyone(): lax.all_to_all(jnp.broadcast_to(shard[None], (peers, *shard.shape)), axis...]
    all_to_all x4 -> x3, starting transfers between devices: 40.4 us -> 26.9 us  [exchanged(): return lax.all_to_all(pieces, axis, 0, 0, tiled=True)]
    ppermute x9 -> x6, waiting for transfers between devices: 19.2 us -> 9.19 us  [permuted_from_near(): lax.ppermute(shard, 'near', [(p, p ^ d) for p in range(peers)])]
    pallas_call x2 -> x5, Pallas kernels: 5.15 us -> 13 us  [the longest x2 5.09 us: recur(): call(functools.partial(recur_kernel, depth, channels, rows // seqs), (jax...]
    ppermute x9 -> x6, starting transfers between devices: 28.5 us -> 21.2 us  [permuted_from_near(): lax.ppermute(shard, 'near', [(p, p ^ d) for p in range(peers)])]
    all_to_all x2 -> x3, blocking collectives: 67.8 us -> 64.5 us  [exchanged(): return lax.all_to_all(pieces, axis, 0, 0, tiled=True)]
  transfers between devices with their start and end apart: 14 -> 13, of which waited for: 10 -> 9; matrix products, arithmetic and copies ran while one was open for 2% -> 4% of each run, Pallas kernels for 0% -> 0%
where the time goes in v4:
time: 323 us; the launch traced here: 321 us
  waiting for transfers between devices  107 us (33%)
  starting transfers between devices  105 us (33%)
  blocking collectives  64.5 us (20%)
  local copies, waits for them, and re-layouts  24.8 us (8%)
  Pallas kernels  13 us (4%)
  other arithmetic  3.32 us (1%)
    all_to_all x3, blocking collectives, exchanged(): return lax.all_to_all(pieces, axis, 0, 0, tiled=True)  64.5 us
    all_to_all x4, starting transfers between devices, from_everyone(): lax.all_to_all(jnp.broadcast_to(shard[None], (peers, *shard.shape)), axis...  57 us
    all_to_all x3, waiting for transfers between devices, exchanged(): return lax.all_to_all(pieces, axis, 0, 0, tiled=True)  52.3 us
    all_to_all x4, waiting for transfers between devices, from_everyone(): lax.all_to_all(jnp.broadcast_to(shard[None], (peers, *shard.shape)), axis...  45.9 us
    all_to_all x3, starting transfers between devices, exchanged(): return lax.all_to_all(pieces, axis, 0, 0, tiled=True)  26.9 us
    ppermute x6, starting transfers between devices, permuted_from_near(): lax.ppermute(shard, 'near', [(p, p ^ d) for p in range(peers)])  21.2 us
    ppermute x6, waiting for transfers between devices, permuted_from_near(): lax.ppermute(shard, 'near', [(p, p ^ d) for p in range(peers)])  9.19 us
    unnamed x38, local copies, waits for them, and re-layouts  6.51 us
  transfers between devices with their start and end apart: 13, of which 9 were waited for; matrix products, arithmetic and copies ran while one was open for 4% of the time, Pallas kernels for 0%

profile of v4, /device:TPU:97, one launch (start us, length us, event | category | flops | bytes accessed | tf_op | source)
XLA Modules:
  0.0 321.4 jit_solution(8410775521785108850)
XLA Ops:
  0.6 1.5 slice_bitcast_fusion
  2.2 4.4 %collective-permute-start = (bf16[64,512]{1,0:T(8,128)(2,1)S(1)}, bf16[64,512]{1,0:T(8,128)(2,1)S(1)}, u32[]{:S(2)}, u32[]{:S(2)}) collective-permute-start(bf16[64,512]{1,0:T(8,128)(2,1)S(1)} %get-tuple-element.36), channel_id=1, source_target_pairs={{0,24},{8,16},{16,8},{24,0},{1,25},{9,17},{17,9},{25,1},{2,26},{10... | collective-permute-start | bytes 196616 | tf_op jit(solution)/shard_map/ppermute | solution.py:31
  6.6 4.2 %collective-permute-start.1 = (bf16[64,512]{1,0:T(8,128)(2,1)S(1)}, bf16[64,512]{1,0:T(8,128)(2,1)S(1)}, u32[]{:S(2)}, u32[]{:S(2)}) collective-permute-start(bf16[64,512]{1,0:T(8,128)(2,1)S(1)} %get-tuple-element.36), channel_id=1, source_target_pairs={{0,16},{8,24},{16,0},{24,8},{1,17},{9,25},{17,1},{25,9},{2,18},{10... | collective-permute-start | bytes 196616 | tf_op jit(solution)/shard_map/ppermute | solution.py:31
  10.8 3.1 collective-permute-start.2
  14.6 40.5 %all-to-all-start = ((bf16[8,32,512]{2,1,0:T(8,128)(2,1)}), bf16[8,32,512]{2,1,0:T(8,128)(2,1)S(1)}, u32[]{:S(2)}, u32[]{:S(2)}) async-start(bf16[8,32,512]{2,1,0:T(8,128)(2,1)} %broadcast_in_dim.56), calls=%async_computation | async-start | bytes 524288 | tf_op jit(solution)/shard_map/all_to_all | solution.py:22
  63.1 28.5 %all-to-all-done = bf16[8,32,512]{2,1,0:T(8,128)(2,1)S(1)} async-done(((bf16[8,32,512]{2,1,0:T(8,128)(2,1)}), bf16[8,32,512]{2,1,0:T(8,128)(2,1)S(1)}, u32[]{:S(2)}, u32[]{:S(2)}) %all-to-all-start) | async-done | bytes 262176 | tf_op jit(solution)/shard_map/all_to_all | solution.py:22
  93.2 10.5 %all-to-all-start.1 = ((bf16[32,32,128]{2,1,0:T(8,128)(2,1)}), bf16[32,32,128]{2,1,0:T(8,128)(2,1)S(1)}, u32[]{:S(2)}, u32[]{:S(2)}) async-start(bf16[32,32,128]{2,1,0:T(8,128)(2,1)} %bitcast.19), calls=%async_computation.1 | async-start | bytes 524288 | tf_op jit(solution)/shard_map/all_to_all | solution.py:42
  111.8 1.9 all-to-all-done.1
  114.4 2.6 recur.2
  117.0 1.4 broadcast_in_dim.58
  118.4 3.6 %all-to-all-start.2 = ((bf16[8,72,128]{2,1,0:T(8,128)(2,1)}), bf16[8,72,128]{2,1,0:T(8,128)(2,1)S(1)}, u32[]{:S(2)}, u32[]{:S(2)}) async-start(bf16[8,72,128]{2,1,0:T(8,128)(2,1)} %broadcast_in_dim.58), calls=%async_computation.2 | async-start | bytes 294912 | tf_op jit(solution)/shard_map/all_to_all | solution.py:22
  122.8 4.6 %all-to-all-done.2.arrived = bf16[8,72,128]{2,1,0:T(8,128)(2,1)S(1)} async-done(((bf16[8,72,128]{2,1,0:T(8,128)(2,1)}), bf16[8,72,128]{2,1,0:T(8,128)(2,1)S(1)}, u32[]{:S(2)}, u32[]{:S(2)}) %all-to-all-start.2) | async-done | bytes 147488 | tf_op jit(solution)/shard_map/all_to_all | solution.py:22
  128.3 3.2 %live_out.1 = bf16[4,120,512]{2,1,0:T(8,128)(2,1)} custom-call(bf16[8,72,128]{2,1,0:T(8,128)(2,1)} %copy-done.4, s32[512,128]{1,0:T(8,128)} %broadcast_in_dim.59.token_of, s32[8,128]{1,0:T(8,128)} %add_select_fusion.1.place, bf16[72,512]{1,0:T(8,128)(2,1)} %pad.51.w_out, bf16[4,16,512]{2,1,0:T(8,128)(2,1)} %bitcast.102), custom_call_target="tpu_custom_call" | custom-call | flops 200000000 | bytes 1048576 | tf_op jit(solution)/shard_map/live_out/pallas_call | solution.py:308
  131.5 15.6 %all_to_all.50 = bf16[4,120,512]{2,1,0:T(8,128)(2,1)S(1)} all-to-all(bf16[4,120,512]{2,1,0:T(8,128)(2,1)} %live_out.1), channel_id=1, replica_groups=mesh['grp'=2,'far'=8,'near'=4,'dp'=8] {'near'}, dimensions={0} | all-to-all | bytes 983040 | tf_op jit(solution)/shard_map/all_to_all | solution.py:42
  147.4 32.6 %all_to_all.51 = bf16[8,13,512]{2,1,0:T(8,128)(2,1)S(1)} all-to-all(bf16[8,13,512]{2,1,0:T(8,128)(2,1)S(1)} %fusion.8), channel_id=1, replica_groups=mesh['grp'=2,'far'=8,'near'=4,'dp'=8] {'far'}, dimensions={0} | all-to-all | bytes 212992 | tf_op jit(solution)/shard_map/all_to_all | solution.py:42
  180.8 6.5 %all-to-all-start.5 = ((bf16[8,12,512]{2,1,0:T(8,128)(2,1)}), bf16[8,12,512]{2,1,0:T(8,128)(2,1)S(1)}, u32[]{:S(2)}, u32[]{:S(2)}) async-start(bf16[8,12,512]{2,1,0:T(8,128)(2,1)} %broadcast_in_dim.116), calls=%async_computation.5 | async-start | bytes 262144 | tf_op jit(solution)/shard_map/all_to_all | solution.py:22
  187.3 3.6 %collective-permute-start.3 = (bf16[64,512]{1,0:T(8,128)(2,1)S(1)}, bf16[64,512]{1,0:T(8,128)(2,1)S(1)}, u32[]{:S(2)}, u32[]{:S(2)}) collective-permute-start(bf16[64,512]{1,0:T(8,128)(2,1)S(1)} %get-tuple-element.14), channel_id=1, source_target_pairs={{0,24},{8,16},{16,8},{24,0},{1,25},{9,17},{17,9},{25,1},{2,26},{10... | collective-permute-start | bytes 196616 | tf_op jit(solution)/shard_map/ppermute | solution.py:31
  190.9 4.0 %collective-permute-start.4 = (bf16[64,512]{1,0:T(8,128)(2,1)S(1)}, bf16[64,512]{1,0:T(8,128)(2,1)S(1)}, u32[]{:S(2)}, u32[]{:S(2)}) collective-permute-start(bf16[64,512]{1,0:T(8,128)(2,1)S(1)} %get-tuple-element.14), channel_id=1, source_target_pairs={{0,16},{8,24},{16,0},{24,8},{1,17},{9,25},{17,1},{25,9},{2,18},{10... | collective-permute-start | bytes 196616 | tf_op jit(solution)/shard_map/ppermute | solution.py:31
  194.9 2.0 collective-permute-start.5
  196.8 8.0 %collective-permute-done.4 = bf16[64,512]{1,0:T(8,128)(2,1)S(1)} collective-permute-done((bf16[64,512]{1,0:T(8,128)(2,1)S(1)}, bf16[64,512]{1,0:T(8,128)(2,1)S(1)}, u32[]{:S(2)}, u32[]{:S(2)}) %collective-permute-start.4) | collective-permute-done | bytes 65568 | tf_op jit(solution)/shard_map/ppermute | solution.py:31
  206.1 6.3 %all-to-all-done.5 = bf16[8,12,512]{2,1,0:T(8,128)(2,1)S(1)} async-done(((bf16[8,12,512]{2,1,0:T(8,128)(2,1)}), bf16[8,12,512]{2,1,0:T(8,128)(2,1)S(1)}, u32[]{:S(2)}, u32[]{:S(2)}) %all-to-all-start.5) | async-done | bytes 98336 | tf_op jit(solution)/shard_map/all_to_all | solution.py:22
  213.2 6.5 %all-to-all-start.6 = ((bf16[4,96,512]{2,1,0:T(8,128)(2,1)}), bf16[4,96,512]{2,1,0:T(8,128)(2,1)S(1)}, u32[]{:S(2)}, u32[]{:S(2)}) async-start(bf16[4,96,512]{2,1,0:T(8,128)(2,1)} %broadcast_in_dim.118), calls=%async_computation.6 | async-start | bytes 786432 | tf_op jit(solution)/shard_map/all_to_all | solution.py:22
  219.8 6.5 %all-to-all-done.6 = bf16[4,96,512]{2,1,0:T(8,128)(2,1)S(1)} async-done(((bf16[4,96,512]{2,1,0:T(8,128)(2,1)}), bf16[4,96,512]{2,1,0:T(8,128)(2,1)S(1)}, u32[]{:S(2)}, u32[]{:S(2)}) %all-to-all-start.6) | async-done | bytes 393248 | tf_op jit(solution)/shard_map/all_to_all | solution.py:22
  227.1 2.3 live_in.1
  229.5 16.3 %all_to_all.52.arrived = bf16[8,72,128]{2,1,0:T(8,128)(2,1)} all-to-all(bf16[8,72,128]{2,1,0:T(8,128)(2,1)} %live_in.1), channel_id=1, replica_groups=mesh['grp'=2,'far'=8,'near'=4,'dp'=8] {'dp'}, dimensions={0} | all-to-all | bytes 294912 | tf_op jit(solution)/shard_map/all_to_all | solution.py:42
  245.7 2.5 recur.3
  248.2 1.5 broadcast_in_dim.120
  249.7 5.9 %all-to-all-start.8 = ((bf16[32,32,128]{2,1,0:T(8,128)(2,1)}), bf16[32,32,128]{2,1,0:T(8,128)(2,1)S(1)}, u32[]{:S(2)}, u32[]{:S(2)}) async-start(bf16[32,32,128]{2,1,0:T(8,128)(2,1)} %bitcast.40), calls=%async_computation.8 | async-start | bytes 524288 | tf_op jit(solution)/shard_map/all_to_all | solution.py:42
  256.5 9.3 %all-to-all-done.8 = bf16[32,32,128]{2,1,0:T(8,128)(2,1)S(1)} async-done(((bf16[32,32,128]{2,1,0:T(8,128)(2,1)}), bf16[32,32,128]{2,1,0:T(8,128)(2,1)S(1)}, u32[]{:S(2)}, u32[]{:S(2)}) %all-to-all-start.8) | async-done | bytes 262176 | tf_op jit(solution)/shard_map/all_to_all | solution.py:42
  266.5 2.3 out.1
  268.8 10.6 %all-to-all-start.9 = ((bf16[8,136,128]{2,1,0:T(8,128)(2,1)}), bf16[8,136,128]{2,1,0:T(8,128)(2,1)S(1)}, u32[]{:S(2)}, u32[]{:S(2)}) async-start(bf16[8,136,128]{2,1,0:T(8,128)(2,1)} %out.1), calls=%async_computation.9 | async-start | bytes 557056 | tf_op jit(solution)/shard_map/all_to_all | solution.py:42
  279.5 41.0 %all-to-all-done.9 = bf16[8,136,128]{2,1,0:T(8,128)(2,1)S(1)} async-done(((bf16[8,136,128]{2,1,0:T(8,128)(2,1)}), bf16[8,136,128]{2,1,0:T(8,128)(2,1)S(1)}, u32[]{:S(2)}, u32[]{:S(2)}) %all-to-all-start.9) | async-done | bytes 278560 | tf_op jit(solution)/shard_map/all_to_all | solution.py:42
  (156 shorter events, 26.9 us)
Async XLA Ops:
  0.6 13.3 %copy-start.6 = (bf16[4,8,512]{2,1,0:T(8,128)(2,1)S(1)}, bf16[4,8,512]{2,1,0:T(8,128)(2,1)}, u32[]{:S(2)}) copy-start(bf16[4,8,512]{2,1,0:T(8,128)(2,1)} %param.16) | copy-start | bytes 98308
  2.2 60.1 %collective-permute-start = (bf16[64,512]{1,0:T(8,128)(2,1)S(1)}, bf16[64,512]{1,0:T(8,128)(2,1)S(1)}, u32[]{:S(2)}, u32[]{:S(2)}) collective-permute-start(bf16[64,512]{1,0:T(8,128)(2,1)S(1)} %get-tuple-element.36), channel_id=1, source_target_pairs={{0,24},{8,16},{16,8},{24,0},{1,25},{9,17},{17,9},{25,1},{2,26},{10... | collective-permute-start | bytes 196616 | tf_op jit(solution)/shard_map/ppermute | solution.py:31
  6.6 55.7 %collective-permute-start.1 = (bf16[64,512]{1,0:T(8,128)(2,1)S(1)}, bf16[64,512]{1,0:T(8,128)(2,1)S(1)}, u32[]{:S(2)}, u32[]{:S(2)}) collective-permute-start(bf16[64,512]{1,0:T(8,128)(2,1)S(1)} %get-tuple-element.36), channel_id=1, source_target_pairs={{0,16},{8,24},{16,0},{24,8},{1,17},{9,25},{17,1},{25,9},{2,18},{10... | collective-permute-start | bytes 196616 | tf_op jit(solution)/shard_map/ppermute | solution.py:31
  10.8 51.6 %collective-permute-start.2 = (bf16[64,512]{1,0:T(8,128)(2,1)S(1)}, bf16[64,512]{1,0:T(8,128)(2,1)S(1)}, u32[]{:S(2)}, u32[]{:S(2)}) collective-permute-start(bf16[64,512]{1,0:T(8,128)(2,1)S(1)} %get-tuple-element.36), channel_id=1, source_target_pairs={{0,8},{8,0},{16,24},{24,16},{1,9},{9,1},{17,25},{25,17},{2,10},{10... | collective-permute-start | bytes 196616 | tf_op jit(solution)/shard_map/ppermute | solution.py:31
  14.6 77.0 %all-to-all-start = ((bf16[8,32,512]{2,1,0:T(8,128)(2,1)}), bf16[8,32,512]{2,1,0:T(8,128)(2,1)S(1)}, u32[]{:S(2)}, u32[]{:S(2)}) async-start(bf16[8,32,512]{2,1,0:T(8,128)(2,1)} %broadcast_in_dim.56), calls=%async_computation | async-start | bytes 524288 | tf_op jit(solution)/shard_map/all_to_all | solution.py:22
  55.1 0.7 copy-start.16
  55.8 0.7 copy-start.12
  56.5 0.7 copy-start.15
  57.8 0.8 copy-start.8
  58.6 0.8 copy-start.9
  60.0 0.7 copy-start.14
  60.0 1.4 copy-start.10
  60.0 1.4 copy-start.11
  62.1 0.9 copy-start.5
  93.2 20.5 %all-to-all-start.1 = ((bf16[32,32,128]{2,1,0:T(8,128)(2,1)}), bf16[32,32,128]{2,1,0:T(8,128)(2,1)S(1)}, u32[]{:S(2)}, u32[]{:S(2)}) async-start(bf16[32,32,128]{2,1,0:T(8,128)(2,1)} %bitcast.19), calls=%async_computation.1 | async-start | bytes 524288 | tf_op jit(solution)/shard_map/all_to_all | solution.py:42
  103.7 0.7 copy-start.13
  106.2 0.8 copy-start.17
  107.0 0.7 copy-start.18
  109.0 0.9 copy-start.7
  113.7 0.7 copy-start.2
  118.4 9.0 %all-to-all-start.2 = ((bf16[8,72,128]{2,1,0:T(8,128)(2,1)}), bf16[8,72,128]{2,1,0:T(8,128)(2,1)S(1)}, u32[]{:S(2)}, u32[]{:S(2)}) async-start(bf16[8,72,128]{2,1,0:T(8,128)(2,1)} %broadcast_in_dim.58), calls=%async_computation.2 | async-start | bytes 294912 | tf_op jit(solution)/shard_map/all_to_all | solution.py:22
  127.5 0.8 copy-start.4
  180.8 31.6 %all-to-all-start.5 = ((bf16[8,12,512]{2,1,0:T(8,128)(2,1)}), bf16[8,12,512]{2,1,0:T(8,128)(2,1)S(1)}, u32[]{:S(2)}, u32[]{:S(2)}) async-start(bf16[8,12,512]{2,1,0:T(8,128)(2,1)} %broadcast_in_dim.116), calls=%async_computation.5 | async-start | bytes 262144 | tf_op jit(solution)/shard_map/all_to_all | solution.py:22
  187.3 9.5 %collective-permute-start.3 = (bf16[64,512]{1,0:T(8,128)(2,1)S(1)}, bf16[64,512]{1,0:T(8,128)(2,1)S(1)}, u32[]{:S(2)}, u32[]{:S(2)}) collective-permute-start(bf16[64,512]{1,0:T(8,128)(2,1)S(1)} %get-tuple-element.14), channel_id=1, source_target_pairs={{0,24},{8,16},{16,8},{24,0},{1,25},{9,17},{17,9},{25,1},{2,26},{10... | collective-permute-start | bytes 196616 | tf_op jit(solution)/shard_map/ppermute | solution.py:31
  190.9 14.0 %collective-permute-start.4 = (bf16[64,512]{1,0:T(8,128)(2,1)S(1)}, bf16[64,512]{1,0:T(8,128)(2,1)S(1)}, u32[]{:S(2)}, u32[]{:S(2)}) collective-permute-start(bf16[64,512]{1,0:T(8,128)(2,1)S(1)} %get-tuple-element.14), channel_id=1, source_target_pairs={{0,16},{8,24},{16,0},{24,8},{1,17},{9,25},{17,1},{25,9},{2,18},{10... | collective-permute-start | bytes 196616 | tf_op jit(solution)/shard_map/ppermute | solution.py:31
  194.9 11.2 %collective-permute-start.5 = (bf16[64,512]{1,0:T(8,128)(2,1)S(1)}, bf16[64,512]{1,0:T(8,128)(2,1)S(1)}, u32[]{:S(2)}, u32[]{:S(2)}) collective-permute-start(bf16[64,512]{1,0:T(8,128)(2,1)S(1)} %get-tuple-element.14), channel_id=1, source_target_pairs={{0,8},{8,0},{16,24},{24,16},{1,9},{9,1},{17,25},{25,17},{2,10},{10... | collective-permute-start | bytes 196616 | tf_op jit(solution)/shard_map/ppermute | solution.py:31
  213.2 13.1 %all-to-all-start.6 = ((bf16[4,96,512]{2,1,0:T(8,128)(2,1)}), bf16[4,96,512]{2,1,0:T(8,128)(2,1)S(1)}, u32[]{:S(2)}, u32[]{:S(2)}) async-start(bf16[4,96,512]{2,1,0:T(8,128)(2,1)} %broadcast_in_dim.118), calls=%async_computation.6 | async-start | bytes 786432 | tf_op jit(solution)/shard_map/all_to_all | solution.py:22
  226.3 0.8 copy-start
  249.7 16.1 %all-to-all-start.8 = ((bf16[32,32,128]{2,1,0:T(8,128)(2,1)}), bf16[32,32,128]{2,1,0:T(8,128)(2,1)S(1)}, u32[]{:S(2)}, u32[]{:S(2)}) async-start(bf16[32,32,128]{2,1,0:T(8,128)(2,1)} %bitcast.40), calls=%async_computation.8 | async-start | bytes 524288 | tf_op jit(solution)/shard_map/all_to_all | solution.py:42
  265.8 0.7 copy-start.3
  268.8 51.7 %copy-start.1 = (bf16[4,96,512]{2,1,0:T(8,128)(2,1)S(1)}, bf16[4,96,512]{2,1,0:T(8,128)(2,1)}, u32[]{:S(2)}) copy-start(bf16[4,96,512]{2,1,0:T(8,128)(2,1)} %copy-done) | copy-start | bytes 1179652
  268.8 51.6 %all-to-all-start.9 = ((bf16[8,136,128]{2,1,0:T(8,128)(2,1)}), bf16[8,136,128]{2,1,0:T(8,128)(2,1)S(1)}, u32[]{:S(2)}, u32[]{:S(2)}) async-start(bf16[8,136,128]{2,1,0:T(8,128)(2,1)} %out.1), calls=%async_computation.9 | async-start | bytes 557056 | tf_op jit(solution)/shard_map/all_to_all | solution.py:42

commit v5 on v3

v5 whole, which is shorter than its diff:
```python
import functools

import jax
import jax.numpy as jnp
from jax import lax
from jax.experimental import pallas as pl
from jax.experimental.pallas import tpu as pltpu
from jax.sharding import Mesh, PartitionSpec as P

D = 4096
CHANNELS = 2048


EPSILON = 1e-06
LIVE_PER_SEQ = 3
NEAR = 4
LANES = 128


def from_everyone(shard, axis):
    peers = lax.axis_size(axis)
    return lax.all_to_all(
        jnp.broadcast_to(shard[None], (peers, *shard.shape)), axis, 0, 0, tiled=True
    )


def traded(parts):
    peers = lax.axis_size("near")
    return [parts[0]] + [
        lax.ppermute(parts[d], "near", [(p, p ^ d) for p in range(peers)])
        for d in range(1, peers)
    ]


def permuted_from_near(shard):
    peers = lax.axis_size("near")
    mine = lax.axis_index("near")
    came = traded([shard] * peers)
    bit = 1
    while bit < peers:
        odd = (mine & bit) != 0
        came = [jnp.where(odd, came[p ^ bit], came[p]) for p in range(peers)]
        bit *= 2
    return jnp.stack(came)


def exchanged(pieces, axis):
    return lax.all_to_all(pieces, axis, 0, 0, tiled=True)


def recurrence_weights(
    decay_rate, frequency, log_step, in_re, in_im, readout_real, readout_imaginary
):
    layers, groups, states, channels = in_re.shape
    step_dt = jnp.exp(log_step)[..., None]
    real_part = -decay_rate.reshape(layers, groups, states)
    imag_part = frequency.reshape(layers, groups, states)
    magnitude = jnp.exp(real_part * step_dt)
    carry_re = magnitude * jnp.cos(imag_part * step_dt)
    carry_im = magnitude * jnp.sin(imag_part * step_dt)
    denominator = real_part * real_part + imag_part * imag_part
    factor_re = (((carry_re - 1.0) * real_part + carry_im * imag_part) / denominator)[..., None]
    factor_im = ((carry_im * real_part - (carry_re - 1.0) * imag_part) / denominator)[..., None]
    carry = jnp.stack([carry_re, carry_im], axis=1).reshape(layers, 2, groups * states)
    same = jnp.eye(groups, dtype=jnp.float32)
    drive = jnp.stack(
        [factor_re * in_re - factor_im * in_im, factor_re * in_im + factor_im * in_re], axis=1
    )
    drive = drive.transpose(0, 2, 4, 1, 3)[:, :, :, :, None] * same[:, None, None, :, None]
    drive = drive.reshape(layers, groups * channels, -1)
    read = jnp.stack([readout_real, -readout_imaginary], axis=1)
    read = read.transpose(0, 1, 2, 4, 3)[:, :, :, :, None] * same[:, None, :, None]
    read = read.reshape(layers, -1, groups * channels)
    spare = LANES - groups * channels
    drive = jnp.pad(drive, [(0, 0), (0, spare), (0, 0)]).astype(jnp.bfloat16)
    read = jnp.pad(read, [(0, 0), (0, 0), (0, spare)]).astype(jnp.bfloat16)
    return carry, drive, read


def product(left, right, dims):
    return lax.dot_general(left, right, (dims, ((), ())), preferred_element_type=jnp.float32)


def recur_kernel(
    depth, channels, steps, arrived, slot_of, re, im, carry, drive, read, skip, gain, *rest
):
    first = depth == 0
    if first:
        sent, final_re, final_im, hidden = rest
    else:
        done_re, done_im, sent, final_re, final_im, hidden = rest
        final_re[:depth] = done_re[...]
        final_im[:depth] = done_im[...]
    seqs, states = re.shape[1:]
    rows = seqs * steps
    at = lax.broadcasted_iota(jnp.int32, (rows, rows), 0)
    to = lax.broadcasted_iota(jnp.int32, (rows, rows), 1)
    by_step = ((at % seqs) * steps + at // seqs == to).astype(jnp.float32)
    by_step = by_step.astype(jnp.bfloat16)
    by_live = (slot_of[...] == to).astype(jnp.float32).astype(jnp.bfloat16)
    total = arrived[:, 0].astype(jnp.float32)
    for j in range(1, arrived.shape[1]):
        total += arrived[:, j].astype(jnp.float32)
    total = total.reshape(rows, LANES)
    inv_rms = lax.rsqrt(total[:, channels : channels + 1] / D + EPSILON)
    driven = (total * inv_rms).astype(jnp.bfloat16)
    driven = product(by_step if first else by_live, driven, ((1,), (0,)))
    matrix = drive[depth]
    pushed = product(driven.astype(jnp.bfloat16), matrix, ((1,), (0,)))
    carry_re, carry_im = carry[depth, 0:1], carry[depth, 1:2]
    real, imag = re[depth], im[depth]
    for t in range(steps):
        now = slice(t * seqs, (t + 1) * seqs)
        active = jnp.concatenate([slot_of[now]] * (states // LANES), axis=1) >= 0
        next_re = carry_re * real - carry_im * imag + pushed[now, :states]
        next_im = carry_re * imag + carry_im * real + pushed[now, states:]
        real = jnp.where(active, next_re, real)
        imag = jnp.where(active, next_im, imag)
        hidden[now, :states] = real.astype(jnp.bfloat16)
        hidden[now, states:] = imag.astype(jnp.bfloat16)
    final_re[depth] = real
    final_im[depth] = imag
    value = product(hidden[...], read[depth], ((1,), (0,)))
    value = value + skip[depth : depth + 1] * driven
    bent = 0.7978845608028654 * (value + 0.044715 * value * value * value)
    value = jnp.where(slot_of[...] >= 0, 0.5 * value * (1.0 + jnp.tanh(bent)), 0.0)
    squares = jnp.sum(value * value, axis=1, keepdims=True)
    lane = lax.broadcasted_iota(jnp.int32, (rows, LANES), 1)
    out = jnp.where(lane == channels, squares, value * gain[depth : depth + 1])
    out = product(by_live if first else by_step, out.astype(jnp.bfloat16), ((0,), (0,)))
    out = out.reshape(sent.shape[0], *sent.shape[2:]).astype(jnp.bfloat16)
    for j in range(sent.shape[1]):
        sent[:, j] = out


def call(kernel, out_shape, name, scratch_shapes=()):
    return pl.pallas_call(
        kernel,
        out_shape=out_shape,
        scratch_shapes=scratch_shapes,
        cost_estimate=pl.CostEstimate(
            flops=200_000_000, bytes_accessed=1 << 20, transcendentals=1 << 14
        ),
        name=name,
    )


def recur(depth, channels, arrived, slot_of, states, weights, done):
    _, seqs, width = states[0].shape
    rows = slot_of.shape[0]
    final = jax.ShapeDtypeStruct((depth + 1, seqs, width), jnp.float32)
    return call(
        functools.partial(recur_kernel, depth, channels, rows // seqs),
        (jax.ShapeDtypeStruct(arrived.shape, jnp.bfloat16), final, final),
        "recur",
        [pltpu.VMEM((rows, 2 * width), jnp.bfloat16)],
    )(arrived, slot_of, *states, *weights, *done)


def with_zeros(block):
    channels, width = block.shape
    return jnp.concatenate([block, jnp.zeros((LANES - channels, width), block.dtype)], axis=0)


def in_kernel(gathered, near_in, gain_row, *rest):
    *row_of, pieces = rest
    near, dp, own, _ = pieces.shape
    channels = near_in.shape[1]
    values = gathered[...].astype(jnp.float32)
    rows = values.shape[0]
    squares = jnp.sum(values * values, axis=1, keepdims=True)
    scaled = (values * gain_row[...]).astype(jnp.bfloat16)
    lane = lax.broadcasted_iota(jnp.int32, (rows, LANES), 1)
    if row_of:
        spread = lax.broadcasted_iota(jnp.int32, (rows, dp * own), 0) == row_of[0][...]
        spread = spread.astype(jnp.float32).astype(jnp.bfloat16)
    for n in range(near):
        out = product(scaled, with_zeros(near_in[n]), ((1,), (1,)))
        out = jnp.where(lane == channels, squares, out).astype(jnp.bfloat16)
        if row_of:
            out = product(spread, out, ((0,), (0,))).astype(jnp.bfloat16)
        pieces[n] = out.reshape(dp, own, LANES)


def live_out_kernel(live_own, arrived, w_out, row_of, pieces):
    near, slots, _ = arrived.shape
    far, rows, width = pieces.shape
    channels = w_out.shape[1]
    pick = lax.broadcasted_iota(jnp.int32, (far * rows, slots), 0) == row_of[...]
    pick = pick.astype(jnp.float32).astype(jnp.bfloat16)
    lane = lax.broadcasted_iota(jnp.int32, (8, LANES), 1)
    one = (lane == channels).astype(jnp.float32).astype(jnp.bfloat16)
    partial, squares = 0.0, 0.0
    for n in range(near):
        live = product(pick, arrived[n], ((1,), (0,))).astype(jnp.bfloat16)
        partial += product(live, with_zeros(w_out[n]), ((1,), (0,)))
        squares += product(one, live, ((1,), (1,)))
    squares = jnp.concatenate(
        [squares[:1], jnp.zeros((1, width - far * rows), jnp.float32)], axis=1
    )
    at = lax.broadcasted_iota(jnp.int32, (far * rows, width), 0) % rows
    partial = jnp.where(at == live_own, squares, partial)
    pieces[...] = partial.astype(jnp.bfloat16).reshape(pieces.shape)


def out_kernel(arrived, w_out, pieces):
    near, rows, _ = arrived.shape
    far, _, _ = pieces.shape
    channels, width = w_out.shape[1:]
    own = rows // far
    lane = lax.broadcasted_iota(jnp.int32, (8, LANES), 1)
    one = (lane == channels).astype(jnp.float32).astype(jnp.bfloat16)
    partial, squares = 0.0, 0.0
    for n in range(near):
        partial += product(arrived[n], with_zeros(w_out[n]), ((1,), (0,)))
        squares += product(one, arrived[n], ((1,), (1,)))
    for f in range(far):
        for q in range(width // LANES):
            pieces[f, q * own : (q + 1) * own] = partial[
                f * own : (f + 1) * own, q * LANES : (q + 1) * LANES
            ].astype(jnp.bfloat16)
        last = squares[:, f * own : (f + 1) * own]
        last = jnp.concatenate([last, jnp.zeros((8, LANES - own), jnp.float32)], axis=1)
        pieces[f, width // LANES * own :] = last.astype(jnp.bfloat16)


def per_device(
    tokens,
    seq_lengths,
    state_re,
    state_im,
    gain_in,
    w_in,
    decay_rate,
    frequency,
    log_step,
    in_re,
    in_im,
    readout_real,
    readout_imaginary,
    skip_scale,
    gain_out,
    w_out,
):
    near, far, dp = (lax.axis_size(a) for a in ("near", "far", "dp"))
    here, far_here = lax.axis_index("near"), lax.axis_index("far")
    dp_here = lax.axis_index("dp")
    seq_local, steps, width = tokens.shape
    seqs_state = state_re.shape[1]
    channels = skip_scale.shape[1]
    own = seq_local * steps
    live_own = LIVE_PER_SEQ * seq_local
    block = -(-(live_own + 1) // 16) * 16
    few = -(-own // near)
    states = (state_re, state_im)
    start = tokens.reshape(own, width)
    joint = ("near", "dp")

    def int_range(size):
        return jnp.arange(size, dtype=jnp.int32)

    ends = jnp.cumsum(seq_lengths)
    starts = ends - seq_lengths
    step = int_range(steps)
    place = jnp.where(step < seq_lengths[:, None], starts[:, None] + step, -1)
    dp_starts, dp_ends = starts[::seqs_state], ends[seqs_state - 1 :: seqs_state]

    def first_of(begin, column):
        return (begin - column + near - 1) // near

    def row_of_number(h):
        return h // live_own * block + h % live_own

    def same(left, right):
        return (left[:, None] == right[None, :]).astype(jnp.bfloat16)

    def exact(pick, rows):
        return jnp.dot(pick, rows, preferred_element_type=jnp.float32).astype(jnp.bfloat16)

    mine = lax.dynamic_slice_in_dim(place, dp_here * seqs_state, seqs_state, 0).T.reshape(-1)
    begin = lax.dynamic_slice_in_dim(dp_starts, dp_here, 1)
    slot_of = mine % near * own + mine // near - first_of(begin, mine % near)
    slot_of = jnp.where(mine >= 0, slot_of, -1)
    slot_of = jnp.broadcast_to(slot_of[:, None], (slot_of.size, LANES))
    number = first_of(dp_starts, here)[:, None] + int_range(own)
    row_of = jnp.where(number * near + here < dp_ends[:, None], row_of_number(number), -1)
    row_of = row_of.reshape(1, -1)
    peer = here ^ int_range(near)
    kept = (far_here * live_own + int_range(block)) * near + peer[:, None]
    kept = jnp.where(int_range(block) < live_own, kept, -2).reshape(-1)
    place_home = place.reshape(far, near, own)
    held = lax.dynamic_slice_in_dim(place_home, here, 1, 1).reshape(-1)
    pick_kept = same(kept, held)
    home_starts = lax.dynamic_slice_in_dim(
        starts[::seq_local].reshape(far, near), far_here, 1, 0
    ).reshape(-1)
    home_ends = lax.dynamic_slice_in_dim(
        ends[seq_local - 1 :: seq_local].reshape(far, near), far_here, 1, 0
    ).reshape(-1)
    number = first_of(home_starts[peer], here)[:, None] + int_range(few)
    back = jnp.where(
        number * near + here < home_ends[peer][:, None], row_of_number(number), -1
    ).reshape(-1)
    pick_back = same(back, int_range(far * block))
    place_own = lax.dynamic_slice_in_dim(held.reshape(far, own), far_here, 1, 0).reshape(-1)
    column = place_own % near
    source = (column ^ here) * few + place_own // near
    source = source - first_of(lax.dynamic_slice_in_dim(home_starts, here, 1), column)
    pick_own = same(jnp.where(place_own >= 0, source, -1), int_range(near * few))
    in_all_lanes = [(0, 0), (0, LANES - channels)]
    weights = recurrence_weights(
        decay_rate, frequency, log_step, in_re, in_im, readout_real, readout_imaginary
    ) + (jnp.pad(skip_scale, in_all_lanes), jnp.pad(gain_out, in_all_lanes))
    pieces_of = jax.ShapeDtypeStruct((near, dp, own, LANES), jnp.bfloat16)

    def joined(pieces):
        return exchanged(pieces.reshape(near * dp, own, LANES), joint).reshape(pieces.shape)

    def summed(pieces):
        return jnp.sum(exchanged(pieces, "far").astype(jnp.float32), axis=0)

    weights_0 = permuted_from_near(jnp.stack([w_in[0].T, w_out[0]]))
    gathered = from_everyone(start, "far")
    gathered, weights_0, weights, slot_of, row_of, pick_kept, pick_back, pick_own = (
        lax.optimization_barrier(
            (gathered, weights_0, weights, slot_of, row_of, pick_kept, pick_back, pick_own)
        )
    )
    gathered = gathered.reshape(far * own, width)
    pieces = call(in_kernel, pieces_of, "project")(gathered, weights_0[:, 0], gain_in[0:1])
    sent, *done = recur(0, channels, joined(pieces), slot_of, states, weights, ())
    pieces = call(
        functools.partial(live_out_kernel, live_own),
        jax.ShapeDtypeStruct((far, block, width), jnp.bfloat16),
        "live_out",
    )(joined(sent).reshape(near, dp * own, LANES), weights_0[:, 1], row_of)
    handed = exact(pick_kept, gathered).reshape(near, block, width)
    to_near = w_in[1].T
    pieces, handed, to_near = lax.optimization_barrier((pieces, handed, to_near))
    total = summed(pieces)
    near_in = permuted_from_near(to_near)
    handed = traded([handed[d] for d in range(near)])
    total, near_in, handed = lax.optimization_barrier((total, near_in, handed))
    before = sum(h.astype(jnp.float32) for h in handed)
    squares = lax.dynamic_slice_in_dim(total[live_own, : far * block], far_here * block, block)
    inv_out = lax.rsqrt(squares / CHANNELS + EPSILON)
    current = (before + total * inv_out[:, None]).astype(jnp.bfloat16)
    current = jnp.where((int_range(block) < live_own)[:, None], current, 0)

    to_near, current = lax.optimization_barrier((w_out[1], current))
    gathered = from_everyone(current, "far")
    near_out, gathered = lax.optimization_barrier((permuted_from_near(to_near), gathered))
    gathered = gathered.reshape(far * block, width)
    pieces = call(in_kernel, pieces_of, "project")(gathered, near_in, gain_in[1:2], row_of)
    sent, *done = recur(1, channels, joined(pieces), slot_of, states, weights, done)
    rows_out = width // LANES * own
    pieces = call(
        out_kernel, jax.ShapeDtypeStruct((far, rows_out + 8, LANES), jnp.bfloat16), "out"
    )(joined(sent).reshape(near, dp * own, LANES), near_out)
    back = exact(pick_back, gathered).reshape(near, few, width)
    pieces, back = lax.optimization_barrier((pieces, back))
    total = summed(pieces)
    back = jnp.stack(traded([back[d] for d in range(near)])).reshape(near * few, width)
    after = jnp.dot(pick_own, back, preferred_element_type=jnp.float32)
    total, after = lax.optimization_barrier((total, after))
    mixed = jnp.concatenate(
        [total[i * own : (i + 1) * own] for i in range(width // LANES)], axis=-1
    )
    inv_out = lax.rsqrt(total[rows_out, :own] / CHANNELS + EPSILON)
    before = jnp.where((place_own >= 0)[:, None], after, start.astype(jnp.float32))
    result = (before + mixed * inv_out[:, None]).astype(jnp.bfloat16)
    return (result.reshape(tokens.shape), *done)


def solution(mesh):
    grp, tp, dp = (mesh.shape[a] for a in ("grp", "tp", "dp"))
    split = Mesh(
        mesh.devices.reshape(grp, tp // NEAR, NEAR, dp), ("grp", "far", "near", "dp")
    )
    tp = ("far", "near")
    in_specs = (
        P(("grp", "far", "near"), None, "dp"),
        P("grp"),
        P(None, ("grp", "dp"), tp),
        P(None, ("grp", "dp"), tp),
        P(None, "dp"),
        P(None, "dp", tp),
        P(None, tp),
        P(None, tp),
        P(None, tp),
        P(None, tp, None, None),
        P(None, tp, None, None),
        P(None, tp, None, None),
        P(None, tp, None, None),
        P(None, tp),
        P(None, tp),
        P(None, tp, "dp"),
    )
    out_specs = (
        P(("grp", "far", "near"), None, "dp"),
        P(None, ("grp", "dp"), tp),
        P(None, ("grp", "dp"), tp),
    )
    return jax.shard_map(
        per_device, mesh=split, in_specs=in_specs, out_specs=out_specs, check_vma=False
    )
```

time: 331 us -> 312 us (0.943)
  the two profiles are of different devices: /device:TPU:97 before, /device:TPU:40 now
where the time goes in v5:
time: 312 us; the launch traced here: 311 us
  starting transfers between devices  136 us (44%)
  waiting for transfers between devices  92.4 us (30%)
  blocking collectives  39.9 us (13%)
  local copies, waits for them, and re-layouts  19.3 us (6%)
  Pallas kernels  14.8 us (5%)
  other arithmetic  6.22 us (2%)
    all_to_all x2, starting transfers between devices, from_everyone(): lax.all_to_all(jnp.broadcast_to(shard[None], (peers, *shard.shape)), axis...  56.5 us
    ppermute x15, starting transfers between devices, traded(): lax.ppermute(parts[d], 'near', [(p, p ^ d) for p in range(peers)])  54.4 us
    all_to_all x4, waiting for transfers between devices, exchanged(): return lax.all_to_all(pieces, axis, 0, 0, tiled=True)  53.6 us
    all_to_all x2, blocking collectives, exchanged(): return lax.all_to_all(pieces, axis, 0, 0, tiled=True)  39.9 us
    all_to_all x2, waiting for transfers between devices, from_everyone(): lax.all_to_all(jnp.broadcast_to(shard[None], (peers, *shard.shape)), axis...  26.1 us
    all_to_all x4, starting transfers between devices, exchanged(): return lax.all_to_all(pieces, axis, 0, 0, tiled=True)  25.4 us
    ppermute x15, waiting for transfers between devices, traded(): lax.ppermute(parts[d], 'near', [(p, p ^ d) for p in range(peers)])  12.7 us
  transfers between devices with their start and end apart: 21, of which 9 were waited for; matrix products, arithmetic and copies ran while one was open for 5% of the time, Pallas kernels for 0%

profile of v5, /device:TPU:40, one launch (start us, length us, event | category | flops | bytes accessed | tf_op | source)
XLA Modules:
  0.0 310.7 jit_solution(15264939526613462844)
XLA Ops:
  1.6 9.1 %collective-permute-start = (bf16[2,64,512]{2,1,0:T(8,128)(2,1)S(1)}, bf16[2,64,512]{2,1,0:T(8,128)(2,1)S(1)}, u32[]{:S(2)}, u32[]{:S(2)}) collective-permute-start(bf16[2,64,512]{2,1,0:T(8,128)(2,1)S(1)} %pad_maximum_fusion.3), channel_id=1, source_target_pairs={{0,24},{8,16},{16,8},{24,0},{1,25},{9,17},{17,9},{25,1},{2,26},{10... | collective-permute-start | bytes 393224 | tf_op jit(solution)/shard_map/ppermute | solution.py:30
  12.8 2.5 collective-permute-start.2
  16.0 40.7 %all-to-all-start = ((bf16[8,32,512]{2,1,0:T(8,128)(2,1)}), bf16[8,32,512]{2,1,0:T(8,128)(2,1)S(1)}, u32[]{:S(2)}, u32[]{:S(2)}) async-start(bf16[8,32,512]{2,1,0:T(8,128)(2,1)} %broadcast_in_dim.47), calls=%async_computation | async-start | bytes 524288 | tf_op jit(solution)/shard_map/all_to_all | solution.py:22
  74.1 14.7 %all-to-all-done = bf16[8,32,512]{2,1,0:T(8,128)(2,1)S(1)} async-done(((bf16[8,32,512]{2,1,0:T(8,128)(2,1)}), bf16[8,32,512]{2,1,0:T(8,128)(2,1)S(1)}, u32[]{:S(2)}, u32[]{:S(2)}) %all-to-all-start) | async-done | bytes 262176 | tf_op jit(solution)/shard_map/all_to_all | solution.py:22
  92.6 24.3 %all_to_all.40 = bf16[32,32,128]{2,1,0:T(8,128)(2,1)} all-to-all(bf16[32,32,128]{2,1,0:T(8,128)(2,1)} %bitcast.130), channel_id=1, replica_groups=mesh['grp'=2,'far'=8,'near'=4,'dp'=8] {'near','dp'}, dimensions={0} | all-to-all | bytes 524288 | tf_op jit(solution)/shard_map/all_to_all | solution.py:48
  116.8 2.7 recur.2
  119.5 4.9 %all-to-all-start.2 = ((bf16[32,32,128]{2,1,0:T(8,128)(2,1)}), bf16[32,32,128]{2,1,0:T(8,128)(2,1)S(1)}, u32[]{:S(2)}, u32[]{:S(2)}) async-start(bf16[32,32,128]{2,1,0:T(8,128)(2,1)} %bitcast.136), calls=%async_computation.2 | async-start | bytes 524288 | tf_op jit(solution)/shard_map/all_to_all | solution.py:48
  124.7 9.9 %all-to-all-done.2 = bf16[32,32,128]{2,1,0:T(8,128)(2,1)S(1)} async-done(((bf16[32,32,128]{2,1,0:T(8,128)(2,1)}), bf16[32,32,128]{2,1,0:T(8,128)(2,1)S(1)}, u32[]{:S(2)}, u32[]{:S(2)}) %all-to-all-start.2) | async-done | bytes 262176 | tf_op jit(solution)/shard_map/all_to_all | solution.py:48
  137.7 6.8 %all-to-all-start.3 = ((bf16[8,16,512]{2,1,0:T(8,128)(2,1)}), bf16[8,16,512]{2,1,0:T(8,128)(2,1)S(1)}, u32[]{:S(2)}, u32[]{:S(2)}) async-start(bf16[8,16,512]{2,1,0:T(8,128)(2,1)} %live_out.1), calls=%async_computation.3 | async-start | bytes 262144 | tf_op jit(solution)/shard_map/all_to_all | solution.py:48
  144.5 3.3 %collective-permute-start.3 = (bf16[64,512]{1,0:T(8,128)(2,1)S(1)}, bf16[64,512]{1,0:T(8,128)(2,1)S(1)}, u32[]{:S(2)}, u32[]{:S(2)}) collective-permute-start(bf16[64,512]{1,0:T(8,128)(2,1)S(1)} %get-tuple-element.50), channel_id=1, source_target_pairs={{0,24},{8,16},{16,8},{24,0},{1,25},{9,17},{17,9},{25,1},{2,26},{10... | collective-permute-start | bytes 196616 | tf_op jit(solution)/shard_map/ppermute | solution.py:30
  147.8 3.1 collective-permute-start.4
  150.9 3.8 %collective-permute-start.5 = (bf16[64,512]{1,0:T(8,128)(2,1)S(1)}, bf16[64,512]{1,0:T(8,128)(2,1)S(1)}, u32[]{:S(2)}, u32[]{:S(2)}) collective-permute-start(bf16[64,512]{1,0:T(8,128)(2,1)S(1)} %get-tuple-element.50), channel_id=1, source_target_pairs={{0,8},{8,0},{16,24},{24,16},{1,9},{9,1},{17,25},{25,17},{2,10},{10... | collective-permute-start | bytes 196616 | tf_op jit(solution)/shard_map/ppermute | solution.py:30
  156.8 3.7 %collective-permute-start.7 = (bf16[16,512]{1,0:T(8,128)(2,1)S(1)}, bf16[16,512]{1,0:T(8,128)(2,1)S(1)}, u32[]{:S(2)}, u32[]{:S(2)}) collective-permute-start(bf16[16,512]{1,0:T(8,128)(2,1)S(1)} %get-tuple-element.98), channel_id=1, source_target_pairs={{0,16},{8,24},{16,0},{24,8},{1,17},{9,25},{17,1},{25,9},{2,18},{10... | collective-permute-start | bytes 49160 | tf_op jit(solution)/shard_map/ppermute | solution.py:30
  160.6 4.4 %collective-permute-start.8 = (bf16[16,512]{1,0:T(8,128)(2,1)S(1)}, bf16[16,512]{1,0:T(8,128)(2,1)S(1)}, u32[]{:S(2)}, u32[]{:S(2)}) collective-permute-start(bf16[16,512]{1,0:T(8,128)(2,1)S(1)} %get-tuple-element.97), channel_id=1, source_target_pairs={{0,24},{8,16},{16,8},{24,0},{1,25},{9,17},{17,9},{25,1},{2,26},{10... | collective-permute-start | bytes 49160 | tf_op jit(solution)/shard_map/ppermute | solution.py:30
  165.7 8.1 %all-to-all-done.3 = bf16[8,16,512]{2,1,0:T(8,128)(2,1)S(1)} async-done(((bf16[8,16,512]{2,1,0:T(8,128)(2,1)}), bf16[8,16,512]{2,1,0:T(8,128)(2,1)S(1)}, u32[]{:S(2)}, u32[]{:S(2)}) %all-to-all-start.3) | async-done | bytes 131104 | tf_op jit(solution)/shard_map/all_to_all | solution.py:48
  174.7 15.7 %all-to-all-start.4 = ((bf16[8,16,512]{2,1,0:T(8,128)(2,1)}), bf16[8,16,512]{2,1,0:T(8,128)(2,1)S(1)}, u32[]{:S(2)}, u32[]{:S(2)}) async-start(bf16[8,16,512]{2,1,0:T(8,128)(2,1)} %broadcast_in_dim.57), calls=%async_computation.4 | async-start | bytes 262144 | tf_op jit(solution)/shard_map/all_to_all | solution.py:22
  192.4 4.9 %collective-permute-start.11 = (bf16[64,512]{1,0:T(8,128)(2,1)S(1)}, bf16[64,512]{1,0:T(8,128)(2,1)S(1)}, u32[]{:S(2)}, u32[]{:S(2)}) collective-permute-start(bf16[64,512]{1,0:T(8,128)(2,1)S(1)} %get-tuple-element.57), channel_id=1, source_target_pairs={{0,8},{8,0},{16,24},{24,16},{1,9},{9,1},{17,25},{25,17},{2,10},{10... | collective-permute-start | bytes 196616 | tf_op jit(solution)/shard_map/ppermute | solution.py:30
  197.4 3.3 %collective-permute-start.9 = (bf16[64,512]{1,0:T(8,128)(2,1)S(1)}, bf16[64,512]{1,0:T(8,128)(2,1)S(1)}, u32[]{:S(2)}, u32[]{:S(2)}) collective-permute-start(bf16[64,512]{1,0:T(8,128)(2,1)S(1)} %get-tuple-element.57), channel_id=1, source_target_pairs={{0,24},{8,16},{16,8},{24,0},{1,25},{9,17},{17,9},{25,1},{2,26},{10... | collective-permute-start | bytes 196616 | tf_op jit(solution)/shard_map/ppermute | solution.py:30
  200.7 2.7 collective-permute-done.11
  203.4 3.5 %collective-permute-done.9 = bf16[64,512]{1,0:T(8,128)(2,1)S(1)} collective-permute-done((bf16[64,512]{1,0:T(8,128)(2,1)S(1)}, bf16[64,512]{1,0:T(8,128)(2,1)S(1)}, u32[]{:S(2)}, u32[]{:S(2)}) %collective-permute-start.9) | collective-permute-done | bytes 65568 | tf_op jit(solution)/shard_map/ppermute | solution.py:30
  207.7 11.4 %all-to-all-done.4 = bf16[8,16,512]{2,1,0:T(8,128)(2,1)S(1)} async-done(((bf16[8,16,512]{2,1,0:T(8,128)(2,1)}), bf16[8,16,512]{2,1,0:T(8,128)(2,1)S(1)}, u32[]{:S(2)}, u32[]{:S(2)}) %all-to-all-start.4) | async-done | bytes 131104 | tf_op jit(solution)/shard_map/all_to_all | solution.py:22
  219.7 2.7 project.3
  222.4 15.6 %all_to_all.41 = bf16[32,32,128]{2,1,0:T(8,128)(2,1)} all-to-all(bf16[32,32,128]{2,1,0:T(8,128)(2,1)} %bitcast.137), channel_id=1, replica_groups=mesh['grp'=2,'far'=8,'near'=4,'dp'=8] {'near','dp'}, dimensions={0} | all-to-all | bytes 524288 | tf_op jit(solution)/shard_map/all_to_all | solution.py:48
  238.0 2.7 recur.3
  240.7 4.9 %all-to-all-start.6 = ((bf16[32,32,128]{2,1,0:T(8,128)(2,1)}), bf16[32,32,128]{2,1,0:T(8,128)(2,1)S(1)}, u32[]{:S(2)}, u32[]{:S(2)}) async-start(bf16[32,32,128]{2,1,0:T(8,128)(2,1)} %bitcast.134), calls=%async_computation.6 | async-start | bytes 524288 | tf_op jit(solution)/shard_map/all_to_all | solution.py:48
  245.8 10.0 %all-to-all-done.6 = bf16[32,32,128]{2,1,0:T(8,128)(2,1)S(1)} async-done(((bf16[32,32,128]{2,1,0:T(8,128)(2,1)}), bf16[32,32,128]{2,1,0:T(8,128)(2,1)S(1)}, u32[]{:S(2)}, u32[]{:S(2)}) %all-to-all-start.6) | async-done | bytes 262176 | tf_op jit(solution)/shard_map/all_to_all | solution.py:48
  258.7 8.8 %all-to-all-start.7 = ((bf16[8,136,128]{2,1,0:T(8,128)(2,1)}), bf16[8,136,128]{2,1,0:T(8,128)(2,1)S(1)}, u32[]{:S(2)}, u32[]{:S(2)}) async-start(bf16[8,136,128]{2,1,0:T(8,128)(2,1)} %out.1), calls=%async_computation.7 | async-start | bytes 557056 | tf_op jit(solution)/shard_map/all_to_all | solution.py:48
  267.5 3.0 collective-permute-start.12
  270.5 2.6 collective-permute-start.13
  273.1 4.6 %collective-permute-start.14 = (bf16[8,512]{1,0:T(8,128)(2,1)S(1)}, bf16[8,512]{1,0:T(8,128)(2,1)S(1)}, u32[]{:S(2)}, u32[]{:S(2)}) collective-permute-start(bf16[8,512]{1,0:T(8,128)(2,1)S(1)} %get-tuple-element.102), channel_id=1, source_target_pairs={{0,24},{8,16},{16,8},{24,0},{1,25},{9,17},{17,9},{25,1},{2,26},{10... | collective-permute-start | bytes 24584 | tf_op jit(solution)/shard_map/ppermute | solution.py:30
  277.7 6.5 %collective-permute-done.12 = bf16[8,512]{1,0:T(8,128)(2,1)S(1)} collective-permute-done((bf16[8,512]{1,0:T(8,128)(2,1)S(1)}, bf16[8,512]{1,0:T(8,128)(2,1)S(1)}, u32[]{:S(2)}, u32[]{:S(2)}) %collective-permute-start.12) | collective-permute-done | bytes 8224 | tf_op jit(solution)/shard_map/ppermute | solution.py:30
  284.3 25.6 %all-to-all-done.7 = bf16[8,136,128]{2,1,0:T(8,128)(2,1)S(1)} async-done(((bf16[8,136,128]{2,1,0:T(8,128)(2,1)}), bf16[8,136,128]{2,1,0:T(8,128)(2,1)S(1)}, u32[]{:S(2)}, u32[]{:S(2)}) %all-to-all-start.7) | async-done | bytes 278560 | tf_op jit(solution)/shard_map/all_to_all | solution.py:48
  (174 shorter events, 38.7 us)
Async XLA Ops:
  0.6 1.0 copy-start.6
  1.6 13.7 %copy-start.7 = (bf16[4,8,512]{2,1,0:T(8,128)(2,1)S(1)}, bf16[4,8,512]{2,1,0:T(8,128)(2,1)}, u32[]{:S(2)}) copy-start(bf16[4,8,512]{2,1,0:T(8,128)(2,1)} %param.16) | copy-start | bytes 98308
  1.6 72.3 %collective-permute-start = (bf16[2,64,512]{2,1,0:T(8,128)(2,1)S(1)}, bf16[2,64,512]{2,1,0:T(8,128)(2,1)S(1)}, u32[]{:S(2)}, u32[]{:S(2)}) collective-permute-start(bf16[2,64,512]{2,1,0:T(8,128)(2,1)S(1)} %pad_maximum_fusion.3), channel_id=1, source_target_pairs={{0,24},{8,16},{16,8},{24,0},{1,25},{9,17},{17,9},{25,1},{2,26},{10... | collective-permute-start | bytes 393224 | tf_op jit(solution)/shard_map/ppermute | solution.py:30
  10.8 63.2 %collective-permute-start.1 = (bf16[2,64,512]{2,1,0:T(8,128)(2,1)S(1)}, bf16[2,64,512]{2,1,0:T(8,128)(2,1)S(1)}, u32[]{:S(2)}, u32[]{:S(2)}) collective-permute-start(bf16[2,64,512]{2,1,0:T(8,128)(2,1)S(1)} %pad_maximum_fusion.3), channel_id=1, source_target_pairs={{0,16},{8,24},{16,0},{24,8},{1,17},{9,25},{17,1},{25,9},{2,18},{10... | collective-permute-start | bytes 393224 | tf_op jit(solution)/shard_map/ppermute | solution.py:30
  12.8 61.2 %collective-permute-start.2 = (bf16[2,64,512]{2,1,0:T(8,128)(2,1)S(1)}, bf16[2,64,512]{2,1,0:T(8,128)(2,1)S(1)}, u32[]{:S(2)}, u32[]{:S(2)}) collective-permute-start(bf16[2,64,512]{2,1,0:T(8,128)(2,1)S(1)} %pad_maximum_fusion.3), channel_id=1, source_target_pairs={{0,8},{8,0},{16,24},{24,16},{1,9},{9,1},{17,25},{25,17},{2,10},{10... | collective-permute-start | bytes 393224 | tf_op jit(solution)/shard_map/ppermute | solution.py:30
  16.0 72.8 %all-to-all-start = ((bf16[8,32,512]{2,1,0:T(8,128)(2,1)}), bf16[8,32,512]{2,1,0:T(8,128)(2,1)S(1)}, u32[]{:S(2)}, u32[]{:S(2)}) async-start(bf16[8,32,512]{2,1,0:T(8,128)(2,1)} %broadcast_in_dim.47), calls=%async_computation | async-start | bytes 524288 | tf_op jit(solution)/shard_map/all_to_all | solution.py:22
  62.3 1.5 copy-start.16
  62.3 1.7 copy-start.12
  62.4 1.6 copy-start.15
  62.5 1.9 copy-start.9
  62.5 1.9 copy-start.10
  65.6 0.8 copy-start.8
  88.8 1.6 copy-start
  119.5 4.9 %copy-start.1 = (bf16[8,32,512]{2,1,0:T(8,128)(2,1)S(1)}, bf16[8,32,512]{2,1,0:T(8,128)(2,1)}, u32[]{:S(2)}) copy-start(bf16[8,32,512]{2,1,0:T(8,128)(2,1)} %copy-done) | copy-start | bytes 786436
  119.5 15.1 %all-to-all-start.2 = ((bf16[32,32,128]{2,1,0:T(8,128)(2,1)}), bf16[32,32,128]{2,1,0:T(8,128)(2,1)S(1)}, u32[]{:S(2)}, u32[]{:S(2)}) async-start(bf16[32,32,128]{2,1,0:T(8,128)(2,1)} %bitcast.136), calls=%async_computation.2 | async-start | bytes 524288 | tf_op jit(solution)/shard_map/all_to_all | solution.py:48
  137.7 36.2 %all-to-all-start.3 = ((bf16[8,16,512]{2,1,0:T(8,128)(2,1)}), bf16[8,16,512]{2,1,0:T(8,128)(2,1)S(1)}, u32[]{:S(2)}, u32[]{:S(2)}) async-start(bf16[8,16,512]{2,1,0:T(8,128)(2,1)} %live_out.1), calls=%async_computation.3 | async-start | bytes 262144 | tf_op jit(solution)/shard_map/all_to_all | solution.py:48
  144.5 16.1 %collective-permute-start.3 = (bf16[64,512]{1,0:T(8,128)(2,1)S(1)}, bf16[64,512]{1,0:T(8,128)(2,1)S(1)}, u32[]{:S(2)}, u32[]{:S(2)}) collective-permute-start(bf16[64,512]{1,0:T(8,128)(2,1)S(1)} %get-tuple-element.50), channel_id=1, source_target_pairs={{0,24},{8,16},{16,8},{24,0},{1,25},{9,17},{17,9},{25,1},{2,26},{10... | collective-permute-start | bytes 196616 | tf_op jit(solution)/shard_map/ppermute | solution.py:30
  147.8 17.1 %collective-permute-start.4 = (bf16[64,512]{1,0:T(8,128)(2,1)S(1)}, bf16[64,512]{1,0:T(8,128)(2,1)S(1)}, u32[]{:S(2)}, u32[]{:S(2)}) collective-permute-start(bf16[64,512]{1,0:T(8,128)(2,1)S(1)} %get-tuple-element.50), channel_id=1, source_target_pairs={{0,16},{8,24},{16,0},{24,8},{1,17},{9,25},{17,1},{25,9},{2,18},{10... | collective-permute-start | bytes 196616 | tf_op jit(solution)/shard_map/ppermute | solution.py:30
  150.9 14.1 %collective-permute-start.5 = (bf16[64,512]{1,0:T(8,128)(2,1)S(1)}, bf16[64,512]{1,0:T(8,128)(2,1)S(1)}, u32[]{:S(2)}, u32[]{:S(2)}) collective-permute-start(bf16[64,512]{1,0:T(8,128)(2,1)S(1)} %get-tuple-element.50), channel_id=1, source_target_pairs={{0,8},{8,0},{16,24},{24,16},{1,9},{9,1},{17,25},{25,17},{2,10},{10... | collective-permute-start | bytes 196616 | tf_op jit(solution)/shard_map/ppermute | solution.py:30
  154.7 19.2 %collective-permute-start.6 = (bf16[16,512]{1,0:T(8,128)(2,1)S(1)}, bf16[16,512]{1,0:T(8,128)(2,1)S(1)}, u32[]{:S(2)}, u32[]{:S(2)}) collective-permute-start(bf16[16,512]{1,0:T(8,128)(2,1)S(1)} %get-tuple-element.99), channel_id=1, source_target_pairs={{0,8},{8,0},{16,24},{24,16},{1,9},{9,1},{17,25},{25,17},{2,10},{10... | collective-permute-start | bytes 49160 | tf_op jit(solution)/shard_map/ppermute | solution.py:30
  156.8 17.1 %collective-permute-start.7 = (bf16[16,512]{1,0:T(8,128)(2,1)S(1)}, bf16[16,512]{1,0:T(8,128)(2,1)S(1)}, u32[]{:S(2)}, u32[]{:S(2)}) collective-permute-start(bf16[16,512]{1,0:T(8,128)(2,1)S(1)} %get-tuple-element.98), channel_id=1, source_target_pairs={{0,16},{8,24},{16,0},{24,8},{1,17},{9,25},{17,1},{25,9},{2,18},{10... | collective-permute-start | bytes 49160 | tf_op jit(solution)/shard_map/ppermute | solution.py:30
  160.6 13.3 %collective-permute-start.8 = (bf16[16,512]{1,0:T(8,128)(2,1)S(1)}, bf16[16,512]{1,0:T(8,128)(2,1)S(1)}, u32[]{:S(2)}, u32[]{:S(2)}) collective-permute-start(bf16[16,512]{1,0:T(8,128)(2,1)S(1)} %get-tuple-element.97), channel_id=1, source_target_pairs={{0,24},{8,16},{16,8},{24,0},{1,25},{9,17},{17,9},{25,1},{2,26},{10... | collective-permute-start | bytes 49160 | tf_op jit(solution)/shard_map/ppermute | solution.py:30
  174.7 44.3 %all-to-all-start.4 = ((bf16[8,16,512]{2,1,0:T(8,128)(2,1)}), bf16[8,16,512]{2,1,0:T(8,128)(2,1)S(1)}, u32[]{:S(2)}, u32[]{:S(2)}) async-start(bf16[8,16,512]{2,1,0:T(8,128)(2,1)} %broadcast_in_dim.57), calls=%async_computation.4 | async-start | bytes 262144 | tf_op jit(solution)/shard_map/all_to_all | solution.py:22
  190.5 10.2 %collective-permute-start.10 = (bf16[64,512]{1,0:T(8,128)(2,1)S(1)}, bf16[64,512]{1,0:T(8,128)(2,1)S(1)}, u32[]{:S(2)}, u32[]{:S(2)}) collective-permute-start(bf16[64,512]{1,0:T(8,128)(2,1)S(1)} %get-tuple-element.57), channel_id=1, source_target_pairs={{0,16},{8,24},{16,0},{24,8},{1,17},{9,25},{17,1},{25,9},{2,18},{10... | collective-permute-start | bytes 196616 | tf_op jit(solution)/shard_map/ppermute | solution.py:30
  192.4 11.0 %collective-permute-start.11 = (bf16[64,512]{1,0:T(8,128)(2,1)S(1)}, bf16[64,512]{1,0:T(8,128)(2,1)S(1)}, u32[]{:S(2)}, u32[]{:S(2)}) collective-permute-start(bf16[64,512]{1,0:T(8,128)(2,1)S(1)} %get-tuple-element.57), channel_id=1, source_target_pairs={{0,8},{8,0},{16,24},{24,16},{1,9},{9,1},{17,25},{25,17},{2,10},{10... | collective-permute-start | bytes 196616 | tf_op jit(solution)/shard_map/ppermute | solution.py:30
  197.4 9.6 %collective-permute-start.9 = (bf16[64,512]{1,0:T(8,128)(2,1)S(1)}, bf16[64,512]{1,0:T(8,128)(2,1)S(1)}, u32[]{:S(2)}, u32[]{:S(2)}) collective-permute-start(bf16[64,512]{1,0:T(8,128)(2,1)S(1)} %get-tuple-element.57), channel_id=1, source_target_pairs={{0,24},{8,16},{16,8},{24,0},{1,25},{9,17},{17,9},{25,1},{2,26},{10... | collective-permute-start | bytes 196616 | tf_op jit(solution)/shard_map/ppermute | solution.py:30
  240.7 4.9 %copy-start.4 = (bf16[8,16,512]{2,1,0:T(8,128)(2,1)S(1)}, bf16[8,16,512]{2,1,0:T(8,128)(2,1)}, u32[]{:S(2)}) copy-start(bf16[8,16,512]{2,1,0:T(8,128)(2,1)} %copy-done.3) | copy-start | bytes 393220
  240.7 15.0 %all-to-all-start.6 = ((bf16[32,32,128]{2,1,0:T(8,128)(2,1)}), bf16[32,32,128]{2,1,0:T(8,128)(2,1)S(1)}, u32[]{:S(2)}, u32[]{:S(2)}) async-start(bf16[32,32,128]{2,1,0:T(8,128)(2,1)} %bitcast.134), calls=%async_computation.6 | async-start | bytes 524288 | tf_op jit(solution)/shard_map/all_to_all | solution.py:48
  258.7 51.2 %all-to-all-start.7 = ((bf16[8,136,128]{2,1,0:T(8,128)(2,1)}), bf16[8,136,128]{2,1,0:T(8,128)(2,1)S(1)}, u32[]{:S(2)}, u32[]{:S(2)}) async-start(bf16[8,136,128]{2,1,0:T(8,128)(2,1)} %out.1), calls=%async_computation.7 | async-start | bytes 557056 | tf_op jit(solution)/shard_map/all_to_all | solution.py:48
  267.5 16.7 %collective-permute-start.12 = (bf16[8,512]{1,0:T(8,128)(2,1)S(1)}, bf16[8,512]{1,0:T(8,128)(2,1)S(1)}, u32[]{:S(2)}, u32[]{:S(2)}) collective-permute-start(bf16[8,512]{1,0:T(8,128)(2,1)S(1)} %get-tuple-element.104), channel_id=1, source_target_pairs={{0,8},{8,0},{16,24},{24,16},{1,9},{9,1},{17,25},{25,17},{2,10},{10... | collective-permute-start | bytes 24584 | tf_op jit(solution)/shard_map/ppermute | solution.py:30
  270.5 13.7 %collective-permute-start.13 = (bf16[8,512]{1,0:T(8,128)(2,1)S(1)}, bf16[8,512]{1,0:T(8,128)(2,1)S(1)}, u32[]{:S(2)}, u32[]{:S(2)}) collective-permute-start(bf16[8,512]{1,0:T(8,128)(2,1)S(1)} %get-tuple-element.103), channel_id=1, source_target_pairs={{0,16},{8,24},{16,0},{24,8},{1,17},{9,25},{17,1},{25,9},{2,18},{10... | collective-permute-start | bytes 24584 | tf_op jit(solution)/shard_map/ppermute | solution.py:30
  273.1 11.1 %collective-permute-start.14 = (bf16[8,512]{1,0:T(8,128)(2,1)S(1)}, bf16[8,512]{1,0:T(8,128)(2,1)S(1)}, u32[]{:S(2)}, u32[]{:S(2)}) collective-permute-start(bf16[8,512]{1,0:T(8,128)(2,1)S(1)} %get-tuple-element.102), channel_id=1, source_target_pairs={{0,24},{8,16},{16,8},{24,0},{1,25},{9,17},{17,9},{25,1},{2,26},{10... | collective-permute-start | bytes 24584 | tf_op jit(solution)/shard_map/ppermute | solution.py:30
  (8 other events, 5.7 us)

commit v6 on v5

--- a/solution.py
+++ b/solution.py
@@ -32,10 +32,9 @@
     ]
 
 
-def permuted_from_near(shard):
+def by_place(came):
     peers = lax.axis_size("near")
     mine = lax.axis_index("near")
-    came = traded([shard] * peers)
     bit = 1
     while bit < peers:
         odd = (mine & bit) != 0
@@ -82,7 +81,7 @@
 
 
 def recur_kernel(
-    depth, channels, steps, arrived, slot_of, re, im, carry, drive, read, skip, gain, *rest
+    depth, channels, steps, arrived, slot_of, re, im, carry, drive, read, skip, *rest
 ):
     first = depth == 0
     if first:
@@ -124,12 +123,14 @@
     value = value + skip[depth : depth + 1] * driven
     bent = 0.7978845608028654 * (value + 0.044715 * value * value * value)
     value = jnp.where(slot_of[...] >= 0, 0.5 * value * (1.0 + jnp.tanh(bent)), 0.0)
-    squares = jnp.sum(value * value, axis=1, keepdims=True)
-    lane = lax.broadcasted_iota(jnp.int32, (rows, LANES), 1)
-    out = jnp.where(lane == channels, squares, value * gain[depth : depth + 1])
-    out = product(by_live if first else by_step, out.astype(jnp.bfloat16), ((0,), (0,)))
-    out = out.reshape(sent.shape[0], *sent.shape[2:]).astype(jnp.bfloat16)
-    for j in range(sent.shape[1]):
+    out = value.astype(jnp.bfloat16)
+    out = product(by_live if first else by_step, out, ((0,), (0,)))
+    near, dp, half, _ = sent.shape
+    out = out.reshape(near, 2, half, LANES)
+    low, high = out[:, 0].reshape(-1, LANES), out[:, 1].reshape(-1, LANES)
+    out = low + pltpu.roll(high, LANES // 2, 1)
+    out = out.reshape(near, half, LANES).astype(jnp.bfloat16)
+    for j in range(dp):
         sent[:, j] = out
 
 
@@ -148,18 +149,27 @@
 def recur(depth, channels, arrived, slot_of, states, weights, done):
     _, seqs, width = states[0].shape
     rows = slot_of.shape[0]
+    near, dp, own, _ = arrived.shape
     final = jax.ShapeDtypeStruct((depth + 1, seqs, width), jnp.float32)
     return call(
         functools.partial(recur_kernel, depth, channels, rows // seqs),
-        (jax.ShapeDtypeStruct(arrived.shape, jnp.bfloat16), final, final),
+        (jax.ShapeDtypeStruct((near, dp, own // 2, LANES), jnp.bfloat16), final, final),
         "recur",
         [pltpu.VMEM((rows, 2 * width), jnp.bfloat16)],
     )(arrived, slot_of, *states, *weights, *done)
 
 
-def with_zeros(block):
+def with_zeros(block, ahead=False):
     channels, width = block.shape
-    return jnp.concatenate([block, jnp.zeros((LANES - channels, width), block.dtype)], axis=0)
+    zeros = jnp.zeros((LANES - channels, width), block.dtype)
+    return jnp.concatenate([zeros, block] if ahead else [block, zeros], axis=0)
+
+
+def squared(rows, half):
+    lane = lax.broadcasted_iota(jnp.int32, (8, LANES), 1)
+    one = (lane // (LANES // 2) == half).astype(jnp.float32).astype(jnp.bfloat16)
+    rows = rows.astype(jnp.float32)
+    return product(one, (rows * rows).astype(jnp.bfloat16), ((1,), (1,)))
 
 
 def in_kernel(gathered, near_in, gain_row, *rest):
@@ -185,16 +195,14 @@
 def live_out_kernel(live_own, arrived, w_out, row_of, pieces):
     near, slots, _ = arrived.shape
     far, rows, width = pieces.shape
-    channels = w_out.shape[1]
-    pick = lax.broadcasted_iota(jnp.int32, (far * rows, slots), 0) == row_of[...]
-    pick = pick.astype(jnp.float32).astype(jnp.bfloat16)
-    lane = lax.broadcasted_iota(jnp.int32, (8, LANES), 1)
-    one = (lane == channels).astype(jnp.float32).astype(jnp.bfloat16)
+    at = lax.broadcasted_iota(jnp.int32, (far * rows, slots), 0)
     partial, squares = 0.0, 0.0
-    for n in range(near):
-        live = product(pick, arrived[n], ((1,), (0,))).astype(jnp.bfloat16)
-        partial += product(live, with_zeros(w_out[n]), ((1,), (0,)))
-        squares += product(one, live, ((1,), (1,)))
+    for half in range(2):
+        pick = (at == row_of[half : half + 1]).astype(jnp.float32).astype(jnp.bfloat16)
+        for n in range(near):
+            live = product(pick, arrived[n], ((1,), (0,))).astype(jnp.bfloat16)
+            partial += product(live, with_zeros(w_out[n], half == 1), ((1,), (0,)))
+            squares += squared(live, half)
     squares = jnp.concatenate(
         [squares[:1], jnp.zeros((1, width - far * rows), jnp.float32)], axis=1
     )
@@ -206,21 +214,25 @@
 def out_kernel(arrived, w_out, pieces):
     near, rows, _ = arrived.shape
     far, _, _ = pieces.shape
-    channels, width = w_out.shape[1:]
-    own = rows // far
-    lane = lax.broadcasted_iota(jnp.int32, (8, LANES), 1)
-    one = (lane == channels).astype(jnp.float32).astype(jnp.bfloat16)
-    partial, squares = 0.0, 0.0
-    for n in range(near):
-        partial += product(arrived[n], with_zeros(w_out[n]), ((1,), (0,)))
-        squares += product(one, arrived[n], ((1,), (1,)))
+    width = w_out.shape[2]
+    few = rows // far
+    own = 2 * few
+    lasts = []
+    for half in range(2):
+        partial, squares = 0.0, 0.0
+        for n in range(near):
+            partial += product(arrived[n], with_zeros(w_out[n], half == 1), ((1,), (0,)))
+            squares += squared(arrived[n], half)
+        lasts.append(squares)
+        for f in range(far):
+            for q in range(width // LANES):
+                at = q * own + half * few
+                pieces[f, at : at + few] = partial[
+                    f * few : (f + 1) * few, q * LANES : (q + 1) * LANES
+                ].astype(jnp.bfloat16)
     for f in range(far):
-        for q in range(width // LANES):
-            pieces[f, q * own : (q + 1) * own] = partial[
-                f * own : (f + 1) * own, q * LANES : (q + 1) * LANES
-            ].astype(jnp.bfloat16)
-        last = squares[:, f * own : (f + 1) * own]
-        last = jnp.concatenate([last, jnp.zeros((8, LANES - own), jnp.float32)], axis=1)
+        last = [squares[:, f * few : (f + 1) * few] for squares in lasts]
+        last = jnp.concatenate(last + [jnp.zeros((8, LANES - own), jnp.float32)], axis=1)
         pieces[f, width // LANES * own :] = last.astype(jnp.bfloat16)
 
 
@@ -284,6 +296,7 @@
     slot_of = jnp.broadcast_to(slot_of[:, None], (slot_of.size, LANES))
     number = first_of(dp_starts, here)[:, None] + int_range(own)
     row_of = jnp.where(number * near + here < dp_ends[:, None], row_of_number(number), -1)
+    row_of_half = row_of.reshape(dp, 2, own // 2).swapaxes(0, 1).reshape(2, -1)
     row_of = row_of.reshape(1, -1)
     peer = here ^ int_range(near)
     kept = (far_here * live_own + int_range(block)) * near + peer[:, None]
@@ -310,53 +323,57 @@
     in_all_lanes = [(0, 0), (0, LANES - channels)]
     weights = recurrence_weights(
         decay_rate, frequency, log_step, in_re, in_im, readout_real, readout_imaginary
-    ) + (jnp.pad(skip_scale, in_all_lanes), jnp.pad(gain_out, in_all_lanes))
+    ) + (jnp.pad(skip_scale, in_all_lanes),)
     pieces_of = jax.ShapeDtypeStruct((near, dp, own, LANES), jnp.bfloat16)
 
     def joined(pieces):
-        return exchanged(pieces.reshape(near * dp, own, LANES), joint).reshape(pieces.shape)
+        flat = pieces.reshape(near * dp, -1, LANES)
+        return exchanged(flat, joint).reshape(pieces.shape)
 
     def summed(pieces):
         return jnp.sum(exchanged(pieces, "far").astype(jnp.float32), axis=0)
 
-    weights_0 = permuted_from_near(jnp.stack([w_in[0].T, w_out[0]]))
+    def weights_of(d):
+        scaled = w_out[d].astype(jnp.float32) * gain_out[d][:, None]
+        return jnp.concatenate([w_in[d].T, scaled.astype(jnp.bfloat16)], axis=0)
+
+    weights_0 = by_place(traded([weights_of(0)] * near))
     gathered = from_everyone(start, "far")
-    gathered, weights_0, weights, slot_of, row_of, pick_kept, pick_back, pick_own = (
-        lax.optimization_barrier(
-            (gathered, weights_0, weights, slot_of, row_of, pick_kept, pick_back, pick_own)
-        )
-    )
+    picks = (pick_kept, pick_back, pick_own)
+    tables = (slot_of, row_of, row_of_half, picks, weights, weights_of(1))
+    gathered, weights_0, tables = lax.optimization_barrier((gathered, weights_0, tables))
+    slot_of, row_of, row_of_half, picks, weights, weights_1 = tables
+    pick_kept, pick_back, pick_own = picks
     gathered = gathered.reshape(far * own, width)
-    pieces = call(in_kernel, pieces_of, "project")(gathered, weights_0[:, 0], gain_in[0:1])
+    pieces = call(in_kernel, pieces_of, "project")(gathered, weights_0[:, :channels], gain_in[0:1])
     sent, *done = recur(0, channels, joined(pieces), slot_of, states, weights, ())
     pieces = call(
         functools.partial(live_out_kernel, live_own),
         jax.ShapeDtypeStruct((far, block, width), jnp.bfloat16),
         "live_out",
-    )(joined(sent).reshape(near, dp * own, LANES), weights_0[:, 1], row_of)
+    )(joined(sent).reshape(near, -1, LANES), weights_0[:, channels:], row_of_half)
     handed = exact(pick_kept, gathered).reshape(near, block, width)
-    to_near = w_in[1].T
-    pieces, handed, to_near = lax.optimization_barrier((pieces, handed, to_near))
+    parts = [jnp.concatenate([weights_1, handed[d]], axis=0) for d in range(near)]
+    pieces, parts = lax.optimization_barrier((pieces, parts))
     total = summed(pieces)
-    near_in = permuted_from_near(to_near)
-    handed = traded([handed[d] for d in range(near)])
-    total, near_in, handed = lax.optimization_barrier((total, near_in, handed))
-    before = sum(h.astype(jnp.float32) for h in handed)
+    total, came = lax.optimization_barrier((total, traded(parts)))
+    before = sum(c[2 * channels :].astype(jnp.float32) for c in came)
+    weights_1 = by_place([c[: 2 * channels] for c in came])
     squares = lax.dynamic_slice_in_dim(total[live_own, : far * block], far_here * block, block)
     inv_out = lax.rsqrt(squares / CHANNELS + EPSILON)
     current = (before + total * inv_out[:, None]).astype(jnp.bfloat16)
     current = jnp.where((int_range(block) < live_own)[:, None], current, 0)
 
-    to_near, current = lax.optimization_barrier((w_out[1], current))
     gathered = from_everyone(current, "far")
-    near_out, gathered = lax.optimization_barrier((permuted_from_near(to_near), gathered))
     gathered = gathered.reshape(far * block, width)
-    pieces = call(in_kernel, pieces_of, "project")(gathered, near_in, gain_in[1:2], row_of)
+    pieces = call(in_kernel, pieces_of, "project")(
+        gathered, weights_1[:, :channels], gain_in[1:2], row_of
+    )
     sent, *done = recur(1, channels, joined(pieces), slot_of, states, weights, done)
     rows_out = width // LANES * own
     pieces = call(
         out_kernel, jax.ShapeDtypeStruct((far, rows_out + 8, LANES), jnp.bfloat16), "out"
-    )(joined(sent).reshape(near, dp * own, LANES), near_out)
+    )(joined(sent).reshape(near, -1, LANES), weights_1[:, channels:])
     back = exact(pick_back, gathered).reshape(near, few, width)
     pieces, back = lax.optimization_barrier((pieces, back))
     total = summed(pieces)

time: 312 us -> 304 us (0.974)
  starting transfers between devices: 136 us -> 109 us
  waiting for transfers between devices: 92.4 us -> 109 us
    ppermute x15 -> x9, starting transfers between devices: 54.4 us -> 34 us  [traded(): lax.ppermute(parts[d], 'near', [(p, p ^ d) for p in range(peers)])]
    all_to_all x2, waiting for transfers between devices: 26.1 us -> 41.6 us  [from_everyone(): lax.all_to_all(jnp.broadcast_to(shard[None], (peers, *shard.shape)), axis...]
    all_to_all x4, waiting for transfers between devices: 53.6 us -> 59.3 us  [exchanged(): return lax.all_to_all(pieces, axis, 0, 0, tiled=True)]
    ppermute x15 -> x9, waiting for transfers between devices: 12.7 us -> 7.71 us  [traded(): lax.ppermute(parts[d], 'near', [(p, p ^ d) for p in range(peers)])]
    all_to_all x4, starting transfers between devices: 25.4 us -> 20.6 us  [exchanged(): return lax.all_to_all(pieces, axis, 0, 0, tiled=True)]
  transfers between devices with their start and end apart: 21 -> 15, of which waited for: 9 -> 8; matrix products, arithmetic and copies ran while one was open for 5% -> 6% of each run, Pallas kernels for 0% -> 0%
where the time goes in v6:
time: 304 us; the launch traced here: 302 us
  starting transfers between devices  109 us (36%)
  waiting for transfers between devices  109 us (36%)
  blocking collectives  41.7 us (14%)
  local copies, waits for them, and re-layouts  19.9 us (7%)
  Pallas kernels  15.4 us (5%)
  other arithmetic  5.57 us (2%)
    all_to_all x4, waiting for transfers between devices, exchanged(): return lax.all_to_all(pieces, axis, 0, 0, tiled=True)  59.3 us
    all_to_all x2, starting transfers between devices, from_everyone(): lax.all_to_all(jnp.broadcast_to(shard[None], (peers, *shard.shape)), axis...  54.7 us
    all_to_all x2, blocking collectives, exchanged(): return lax.all_to_all(pieces, axis, 0, 0, tiled=True)  41.7 us
    all_to_all x2, waiting for transfers between devices, from_everyone(): lax.all_to_all(jnp.broadcast_to(shard[None], (peers, *shard.shape)), axis...  41.6 us
    ppermute x9, starting transfers between devices, traded(): lax.ppermute(parts[d], 'near', [(p, p ^ d) for p in range(peers)])  34 us
    all_to_all x4, starting transfers between devices, exchanged(): return lax.all_to_all(pieces, axis, 0, 0, tiled=True)  20.6 us
    ppermute x9, waiting for transfers between devices, traded(): lax.ppermute(parts[d], 'near', [(p, p ^ d) for p in range(peers)])  7.71 us
  transfers between devices with their start and end apart: 15, of which 8 were waited for; matrix products, arithmetic and copies ran while one was open for 6% of the time, Pallas kernels for 0%

profile of v6, /device:TPU:40, one launch (start us, length us, event | category | flops | bytes accessed | tf_op | source)
XLA Modules:
  0.0 302.2 jit_solution(17281448065185371593)
XLA Ops:
  1.4 0.9 slice_bitcast_fusion
  2.5 9.1 %collective-permute-start = (bf16[128,512]{1,0:T(8,128)(2,1)S(1)}, bf16[128,512]{1,0:T(8,128)(2,1)S(1)}, u32[]{:S(2)}, u32[]{:S(2)}) collective-permute-start(bf16[128,512]{1,0:T(8,128)(2,1)S(1)} %pad_maximum_fusion.6), channel_id=1, source_target_pairs={{0,24},{8,16},{16,8},{24,0},{1,25},{9,17},{17,9},{25,1},{2,26},{10... | collective-permute-start | bytes 393224 | tf_op jit(solution)/shard_map/ppermute | solution.py:30
  11.6 2.0 collective-permute-start.1
  13.6 2.5 collective-permute-start.2
  16.8 40.7 %all-to-all-start = ((bf16[8,32,512]{2,1,0:T(8,128)(2,1)}), bf16[8,32,512]{2,1,0:T(8,128)(2,1)S(1)}, u32[]{:S(2)}, u32[]{:S(2)}) async-start(bf16[8,32,512]{2,1,0:T(8,128)(2,1)} %broadcast_in_dim.47), calls=%async_computation | async-start | bytes 524288 | tf_op jit(solution)/shard_map/all_to_all | solution.py:22
  74.7 15.0 %all-to-all-done = bf16[8,32,512]{2,1,0:T(8,128)(2,1)S(1)} async-done(((bf16[8,32,512]{2,1,0:T(8,128)(2,1)}), bf16[8,32,512]{2,1,0:T(8,128)(2,1)S(1)}, u32[]{:S(2)}, u32[]{:S(2)}) %all-to-all-start) | async-done | bytes 262176 | tf_op jit(solution)/shard_map/all_to_all | solution.py:22
  90.4 0.9 fusion.31
  91.2 2.2 project.2
  93.4 24.3 %all_to_all.40 = bf16[32,32,128]{2,1,0:T(8,128)(2,1)} all-to-all(bf16[32,32,128]{2,1,0:T(8,128)(2,1)} %bitcast.108), channel_id=1, replica_groups=mesh['grp'=2,'far'=8,'near'=4,'dp'=8] {'near','dp'}, dimensions={0} | all-to-all | bytes 524288 | tf_op jit(solution)/shard_map/all_to_all | solution.py:47
  117.7 2.6 recur.2
  120.3 4.9 %all-to-all-start.2 = ((bf16[32,16,128]{2,1,0:T(8,128)(2,1)}), bf16[32,16,128]{2,1,0:T(8,128)(2,1)S(1)}, u32[]{:S(2)}, u32[]{:S(2)}) async-start(bf16[32,16,128]{2,1,0:T(8,128)(2,1)} %bitcast.114), calls=%async_computation.2 | async-start | bytes 262144 | tf_op jit(solution)/shard_map/all_to_all | solution.py:47
  125.5 7.8 %all-to-all-done.2 = bf16[32,16,128]{2,1,0:T(8,128)(2,1)S(1)} async-done(((bf16[32,16,128]{2,1,0:T(8,128)(2,1)}), bf16[32,16,128]{2,1,0:T(8,128)(2,1)S(1)}, u32[]{:S(2)}, u32[]{:S(2)}) %all-to-all-start.2) | async-done | bytes 131104 | tf_op jit(solution)/shard_map/all_to_all | solution.py:47
  133.9 3.0 live_out.1
  136.9 6.8 %all-to-all-start.3 = ((bf16[8,16,512]{2,1,0:T(8,128)(2,1)}), bf16[8,16,512]{2,1,0:T(8,128)(2,1)S(1)}, u32[]{:S(2)}, u32[]{:S(2)}) async-start(bf16[8,16,512]{2,1,0:T(8,128)(2,1)} %live_out.1), calls=%async_computation.3 | async-start | bytes 262144 | tf_op jit(solution)/shard_map/all_to_all | solution.py:47
  143.7 2.6 collective-permute-start.3
  146.3 3.0 collective-permute-start.4
  149.3 4.6 %collective-permute-start.5 = (bf16[144,512]{1,0:T(8,128)(2,1)S(1)}, bf16[144,512]{1,0:T(8,128)(2,1)S(1)}, u32[]{:S(2)}, u32[]{:S(2)}) collective-permute-start(bf16[144,512]{1,0:T(8,128)(2,1)S(1)} %get-tuple-element.51), channel_id=1, source_target_pairs={{0,24},{8,16},{16,8},{24,0},{1,25},{9,17},{17,9},{25,1},{2,26},{10... | collective-permute-start | bytes 442376 | tf_op jit(solution)/shard_map/ppermute | solution.py:30
  154.0 19.6 %all-to-all-done.3 = bf16[8,16,512]{2,1,0:T(8,128)(2,1)S(1)} async-done(((bf16[8,16,512]{2,1,0:T(8,128)(2,1)}), bf16[8,16,512]{2,1,0:T(8,128)(2,1)S(1)}, u32[]{:S(2)}, u32[]{:S(2)}) %all-to-all-start.3) | async-done | bytes 131104 | tf_op jit(solution)/shard_map/all_to_all | solution.py:47
  174.4 14.0 %all-to-all-start.4 = ((bf16[8,16,512]{2,1,0:T(8,128)(2,1)}), bf16[8,16,512]{2,1,0:T(8,128)(2,1)S(1)}, u32[]{:S(2)}, u32[]{:S(2)}) async-start(bf16[8,16,512]{2,1,0:T(8,128)(2,1)} %broadcast_in_dim.57), calls=%async_computation.4 | async-start | bytes 262144 | tf_op jit(solution)/shard_map/all_to_all | solution.py:22
  189.4 26.7 %all-to-all-done.4 = bf16[8,16,512]{2,1,0:T(8,128)(2,1)S(1)} async-done(((bf16[8,16,512]{2,1,0:T(8,128)(2,1)}), bf16[8,16,512]{2,1,0:T(8,128)(2,1)S(1)}, u32[]{:S(2)}, u32[]{:S(2)}) %all-to-all-start.4) | async-done | bytes 131104 | tf_op jit(solution)/shard_map/all_to_all | solution.py:22
  216.7 2.7 project.3
  219.4 17.4 %all_to_all.41 = bf16[32,32,128]{2,1,0:T(8,128)(2,1)} all-to-all(bf16[32,32,128]{2,1,0:T(8,128)(2,1)} %bitcast.112), channel_id=1, replica_groups=mesh['grp'=2,'far'=8,'near'=4,'dp'=8] {'near','dp'}, dimensions={0} | all-to-all | bytes 524288 | tf_op jit(solution)/shard_map/all_to_all | solution.py:47
  236.9 2.6 recur.3
  239.5 4.9 %all-to-all-start.6 = ((bf16[32,16,128]{2,1,0:T(8,128)(2,1)}), bf16[32,16,128]{2,1,0:T(8,128)(2,1)S(1)}, u32[]{:S(2)}, u32[]{:S(2)}) async-start(bf16[32,16,128]{2,1,0:T(8,128)(2,1)} %bitcast.115), calls=%async_computation.6 | async-start | bytes 262144 | tf_op jit(solution)/shard_map/all_to_all | solution.py:47
  244.5 7.9 %all-to-all-done.6 = bf16[32,16,128]{2,1,0:T(8,128)(2,1)S(1)} async-done(((bf16[32,16,128]{2,1,0:T(8,128)(2,1)}), bf16[32,16,128]{2,1,0:T(8,128)(2,1)S(1)}, u32[]{:S(2)}, u32[]{:S(2)}) %all-to-all-start.6) | async-done | bytes 131104 | tf_op jit(solution)/shard_map/all_to_all | solution.py:47
  253.1 2.3 out.1
  255.4 3.9 %all-to-all-start.7 = ((bf16[8,136,128]{2,1,0:T(8,128)(2,1)}), bf16[8,136,128]{2,1,0:T(8,128)(2,1)S(1)}, u32[]{:S(2)}, u32[]{:S(2)}) async-start(bf16[8,136,128]{2,1,0:T(8,128)(2,1)} %out.1), calls=%async_computation.7 | async-start | bytes 557056 | tf_op jit(solution)/shard_map/all_to_all | solution.py:47
  259.4 2.9 collective-permute-start.8
  262.3 3.0 %collective-permute-start.7 = (bf16[8,512]{1,0:T(8,128)(2,1)S(1)}, bf16[8,512]{1,0:T(8,128)(2,1)S(1)}, u32[]{:S(2)}, u32[]{:S(2)}) collective-permute-start(bf16[8,512]{1,0:T(8,128)(2,1)S(1)} %get-tuple-element.101), channel_id=1, source_target_pairs={{0,16},{8,24},{16,0},{24,8},{1,17},{9,25},{17,1},{25,9},{2,18},{10... | collective-permute-start | bytes 24584 | tf_op jit(solution)/shard_map/ppermute | solution.py:30
  265.3 4.2 %collective-permute-start.6 = (bf16[8,512]{1,0:T(8,128)(2,1)S(1)}, bf16[8,512]{1,0:T(8,128)(2,1)S(1)}, u32[]{:S(2)}, u32[]{:S(2)}) collective-permute-start(bf16[8,512]{1,0:T(8,128)(2,1)S(1)} %get-tuple-element.102), channel_id=1, source_target_pairs={{0,8},{8,0},{16,24},{24,16},{1,9},{9,1},{17,25},{25,17},{2,10},{10... | collective-permute-start | bytes 24584 | tf_op jit(solution)/shard_map/ppermute | solution.py:30
  269.9 7.4 %collective-permute-done.6 = bf16[8,512]{1,0:T(8,128)(2,1)S(1)} collective-permute-done((bf16[8,512]{1,0:T(8,128)(2,1)S(1)}, bf16[8,512]{1,0:T(8,128)(2,1)S(1)}, u32[]{:S(2)}, u32[]{:S(2)}) %collective-permute-start.6) | collective-permute-done | bytes 8224 | tf_op jit(solution)/shard_map/ppermute | solution.py:30
  277.4 24.0 %all-to-all-done.7 = bf16[8,136,128]{2,1,0:T(8,128)(2,1)S(1)} async-done(((bf16[8,136,128]{2,1,0:T(8,128)(2,1)}), bf16[8,136,128]{2,1,0:T(8,128)(2,1)S(1)}, u32[]{:S(2)}, u32[]{:S(2)}) %all-to-all-start.7) | async-done | bytes 278560 | tf_op jit(solution)/shard_map/all_to_all | solution.py:47
  (169 shorter events, 24.3 us)
Async XLA Ops:
  1.4 1.0 copy-start.4
  2.4 13.7 %copy-start.7 = (bf16[4,8,512]{2,1,0:T(8,128)(2,1)S(1)}, bf16[4,8,512]{2,1,0:T(8,128)(2,1)}, u32[]{:S(2)}) copy-start(bf16[4,8,512]{2,1,0:T(8,128)(2,1)} %param.16) | copy-start | bytes 98308
  2.5 71.9 %collective-permute-start = (bf16[128,512]{1,0:T(8,128)(2,1)S(1)}, bf16[128,512]{1,0:T(8,128)(2,1)S(1)}, u32[]{:S(2)}, u32[]{:S(2)}) collective-permute-start(bf16[128,512]{1,0:T(8,128)(2,1)S(1)} %pad_maximum_fusion.6), channel_id=1, source_target_pairs={{0,24},{8,16},{16,8},{24,0},{1,25},{9,17},{17,9},{25,1},{2,26},{10... | collective-permute-start | bytes 393224 | tf_op jit(solution)/shard_map/ppermute | solution.py:30
  11.6 62.8 %collective-permute-start.1 = (bf16[128,512]{1,0:T(8,128)(2,1)S(1)}, bf16[128,512]{1,0:T(8,128)(2,1)S(1)}, u32[]{:S(2)}, u32[]{:S(2)}) collective-permute-start(bf16[128,512]{1,0:T(8,128)(2,1)S(1)} %pad_maximum_fusion.6), channel_id=1, source_target_pairs={{0,16},{8,24},{16,0},{24,8},{1,17},{9,25},{17,1},{25,9},{2,18},{10... | collective-permute-start | bytes 393224 | tf_op jit(solution)/shard_map/ppermute | solution.py:30
  13.6 60.9 %collective-permute-start.2 = (bf16[128,512]{1,0:T(8,128)(2,1)S(1)}, bf16[128,512]{1,0:T(8,128)(2,1)S(1)}, u32[]{:S(2)}, u32[]{:S(2)}) collective-permute-start(bf16[128,512]{1,0:T(8,128)(2,1)S(1)} %pad_maximum_fusion.6), channel_id=1, source_target_pairs={{0,8},{8,0},{16,24},{24,16},{1,9},{9,1},{17,25},{25,17},{2,10},{10... | collective-permute-start | bytes 393224 | tf_op jit(solution)/shard_map/ppermute | solution.py:30
  16.8 72.8 %all-to-all-start = ((bf16[8,32,512]{2,1,0:T(8,128)(2,1)}), bf16[8,32,512]{2,1,0:T(8,128)(2,1)S(1)}, u32[]{:S(2)}, u32[]{:S(2)}) async-start(bf16[8,32,512]{2,1,0:T(8,128)(2,1)} %broadcast_in_dim.47), calls=%async_computation | async-start | bytes 524288 | tf_op jit(solution)/shard_map/all_to_all | solution.py:22
  57.6 0.7 copy-start.13
  62.8 0.9 copy-start.16
  62.8 1.0 copy-start.12
  62.8 1.1 copy-start.15
  62.9 1.5 copy-start.10
  63.5 0.8 copy-start.9
  65.1 0.8 copy-start.8
  66.0 0.7 copy-start.14
  66.0 4.3 %copy-start.11 = (f32[2,4,16,64]{3,2,1,0:T(8,128)S(1)}, f32[2,4,16,64]{3,2,1,0:T(8,128)}, u32[]{:S(2)}) copy-start(f32[2,4,16,64]{3,2,1,0:T(8,128)} %param.27) | copy-start | bytes 98308
  73.0 0.8 copy-start.17
  89.6 1.6 copy-start
  120.3 4.9 %copy-start.1 = (bf16[8,32,512]{2,1,0:T(8,128)(2,1)S(1)}, bf16[8,32,512]{2,1,0:T(8,128)(2,1)}, u32[]{:S(2)}) copy-start(bf16[8,32,512]{2,1,0:T(8,128)(2,1)} %copy-done) | copy-start | bytes 786436
  120.3 13.0 %all-to-all-start.2 = ((bf16[32,16,128]{2,1,0:T(8,128)(2,1)}), bf16[32,16,128]{2,1,0:T(8,128)(2,1)S(1)}, u32[]{:S(2)}, u32[]{:S(2)}) async-start(bf16[32,16,128]{2,1,0:T(8,128)(2,1)} %bitcast.114), calls=%async_computation.2 | async-start | bytes 262144 | tf_op jit(solution)/shard_map/all_to_all | solution.py:47
  136.9 36.6 %all-to-all-start.3 = ((bf16[8,16,512]{2,1,0:T(8,128)(2,1)}), bf16[8,16,512]{2,1,0:T(8,128)(2,1)S(1)}, u32[]{:S(2)}, u32[]{:S(2)}) async-start(bf16[8,16,512]{2,1,0:T(8,128)(2,1)} %live_out.1), calls=%async_computation.3 | async-start | bytes 262144 | tf_op jit(solution)/shard_map/all_to_all | solution.py:47
  143.7 29.8 %collective-permute-start.3 = (bf16[144,512]{1,0:T(8,128)(2,1)S(1)}, bf16[144,512]{1,0:T(8,128)(2,1)S(1)}, u32[]{:S(2)}, u32[]{:S(2)}) collective-permute-start(bf16[144,512]{1,0:T(8,128)(2,1)S(1)} %get-tuple-element.49), channel_id=1, source_target_pairs={{0,8},{8,0},{16,24},{24,16},{1,9},{9,1},{17,25},{25,17},{2,10},{10... | collective-permute-start | bytes 442376 | tf_op jit(solution)/shard_map/ppermute | solution.py:30
  146.3 27.3 %collective-permute-start.4 = (bf16[144,512]{1,0:T(8,128)(2,1)S(1)}, bf16[144,512]{1,0:T(8,128)(2,1)S(1)}, u32[]{:S(2)}, u32[]{:S(2)}) collective-permute-start(bf16[144,512]{1,0:T(8,128)(2,1)S(1)} %get-tuple-element.50), channel_id=1, source_target_pairs={{0,16},{8,24},{16,0},{24,8},{1,17},{9,25},{17,1},{25,9},{2,18},{10... | collective-permute-start | bytes 442376 | tf_op jit(solution)/shard_map/ppermute | solution.py:30
  149.3 24.2 %collective-permute-start.5 = (bf16[144,512]{1,0:T(8,128)(2,1)S(1)}, bf16[144,512]{1,0:T(8,128)(2,1)S(1)}, u32[]{:S(2)}, u32[]{:S(2)}) collective-permute-start(bf16[144,512]{1,0:T(8,128)(2,1)S(1)} %get-tuple-element.51), channel_id=1, source_target_pairs={{0,24},{8,16},{16,8},{24,0},{1,25},{9,17},{17,9},{25,1},{2,26},{10... | collective-permute-start | bytes 442376 | tf_op jit(solution)/shard_map/ppermute | solution.py:30
  174.4 41.7 %all-to-all-start.4 = ((bf16[8,16,512]{2,1,0:T(8,128)(2,1)}), bf16[8,16,512]{2,1,0:T(8,128)(2,1)S(1)}, u32[]{:S(2)}, u32[]{:S(2)}) async-start(bf16[8,16,512]{2,1,0:T(8,128)(2,1)} %broadcast_in_dim.57), calls=%async_computation.4 | async-start | bytes 262144 | tf_op jit(solution)/shard_map/all_to_all | solution.py:22
  216.1 0.7 copy-start.2
  239.5 4.9 %copy-start.3 = (bf16[8,16,512]{2,1,0:T(8,128)(2,1)S(1)}, bf16[8,16,512]{2,1,0:T(8,128)(2,1)}, u32[]{:S(2)}) copy-start(bf16[8,16,512]{2,1,0:T(8,128)(2,1)} %copy-done.2) | copy-start | bytes 393220
  239.5 13.0 %all-to-all-start.6 = ((bf16[32,16,128]{2,1,0:T(8,128)(2,1)}), bf16[32,16,128]{2,1,0:T(8,128)(2,1)S(1)}, u32[]{:S(2)}, u32[]{:S(2)}) async-start(bf16[32,16,128]{2,1,0:T(8,128)(2,1)} %bitcast.115), calls=%async_computation.6 | async-start | bytes 262144 | tf_op jit(solution)/shard_map/all_to_all | solution.py:47
  252.4 0.7 copy-start.6
  255.4 46.0 %all-to-all-start.7 = ((bf16[8,136,128]{2,1,0:T(8,128)(2,1)}), bf16[8,136,128]{2,1,0:T(8,128)(2,1)S(1)}, u32[]{:S(2)}, u32[]{:S(2)}) async-start(bf16[8,136,128]{2,1,0:T(8,128)(2,1)} %out.1), calls=%async_computation.7 | async-start | bytes 557056 | tf_op jit(solution)/shard_map/all_to_all | solution.py:47
  259.4 10.3 %collective-permute-start.8 = (bf16[8,512]{1,0:T(8,128)(2,1)S(1)}, bf16[8,512]{1,0:T(8,128)(2,1)S(1)}, u32[]{:S(2)}, u32[]{:S(2)}) collective-permute-start(bf16[8,512]{1,0:T(8,128)(2,1)S(1)} %get-tuple-element.100), channel_id=1, source_target_pairs={{0,24},{8,16},{16,8},{24,0},{1,25},{9,17},{17,9},{25,1},{2,26},{10... | collective-permute-start | bytes 24584 | tf_op jit(solution)/shard_map/ppermute | solution.py:30
  262.3 7.6 %collective-permute-start.7 = (bf16[8,512]{1,0:T(8,128)(2,1)S(1)}, bf16[8,512]{1,0:T(8,128)(2,1)S(1)}, u32[]{:S(2)}, u32[]{:S(2)}) collective-permute-start(bf16[8,512]{1,0:T(8,128)(2,1)S(1)} %get-tuple-element.101), channel_id=1, source_target_pairs={{0,16},{8,24},{16,0},{24,8},{1,17},{9,25},{17,1},{25,9},{2,18},{10... | collective-permute-start | bytes 24584 | tf_op jit(solution)/shard_map/ppermute | solution.py:30
  265.3 12.0 %collective-permute-start.6 = (bf16[8,512]{1,0:T(8,128)(2,1)S(1)}, bf16[8,512]{1,0:T(8,128)(2,1)S(1)}, u32[]{:S(2)}, u32[]{:S(2)}) collective-permute-start(bf16[8,512]{1,0:T(8,128)(2,1)S(1)} %get-tuple-element.102), channel_id=1, source_target_pairs={{0,8},{8,0},{16,24},{24,16},{1,9},{9,1},{17,25},{25,17},{2,10},{10... | collective-permute-start | bytes 24584 | tf_op jit(solution)/shard_map/ppermute | solution.py:30
  (1 other events, 0.6 us)

commit v7 on v6

--- a/solution.py
+++ b/solution.py
@@ -24,12 +24,9 @@
     )
 
 
-def traded(parts):
+def swapped(block, d):
     peers = lax.axis_size("near")
-    return [parts[0]] + [
-        lax.ppermute(parts[d], "near", [(p, p ^ d) for p in range(peers)])
-        for d in range(1, peers)
-    ]
+    return lax.ppermute(block, "near", [(p, p ^ d) for p in range(peers)])
 
 
 def by_place(came):
@@ -337,12 +334,15 @@
         scaled = w_out[d].astype(jnp.float32) * gain_out[d][:, None]
         return jnp.concatenate([w_in[d].T, scaled.astype(jnp.bfloat16)], axis=0)
 
-    weights_0 = by_place(traded([weights_of(0)] * near))
+    own_0, own_1 = weights_of(0), weights_of(1)
+    from_next = swapped(jnp.concatenate([own_0, own_1], axis=0), 1)
+    next_0, next_1 = from_next[: 2 * channels], from_next[2 * channels :]
+    weights_0 = by_place([own_0, next_0, swapped(own_0, 2), swapped(own_0, 3)])
     gathered = from_everyone(start, "far")
     picks = (pick_kept, pick_back, pick_own)
-    tables = (slot_of, row_of, row_of_half, picks, weights, weights_of(1))
+    tables = (slot_of, row_of, row_of_half, picks, weights, own_1, next_1)
     gathered, weights_0, tables = lax.optimization_barrier((gathered, weights_0, tables))
-    slot_of, row_of, row_of_half, picks, weights, weights_1 = tables
+    slot_of, row_of, row_of_half, picks, weights, own_1, next_1 = tables
     pick_kept, pick_back, pick_own = picks
     gathered = gathered.reshape(far * own, width)
     pieces = call(in_kernel, pieces_of, "project")(gathered, weights_0[:, :channels], gain_in[0:1])
@@ -353,31 +353,48 @@
         "live_out",
     )(joined(sent).reshape(near, -1, LANES), weights_0[:, channels:], row_of_half)
     handed = exact(pick_kept, gathered).reshape(near, block, width)
-    parts = [jnp.concatenate([weights_1, handed[d]], axis=0) for d in range(near)]
-    pieces, parts = lax.optimization_barrier((pieces, parts))
+    part = jnp.concatenate(
+        [own_1[:channels], next_1[:channels], handed[2], handed[3]], axis=0
+    )
+    pieces, part = lax.optimization_barrier((pieces, part))
     total = summed(pieces)
-    total, came = lax.optimization_barrier((total, traded(parts)))
-    before = sum(c[2 * channels :].astype(jnp.float32) for c in came)
-    weights_1 = by_place([c[: 2 * channels] for c in came])
+    came = swapped(part, 2)
+    cut = [channels, 2 * channels, 2 * channels + block]
+    far_in, far_next_in, for_me, for_next = jnp.split(came, cut)
+    from_next = swapped(handed[1] + for_next, 1)
+    total, for_me, from_next, far_in, far_next_in = lax.optimization_barrier(
+        (total, for_me, from_next, far_in, far_next_in)
+    )
+    before = (handed[0] + for_me + from_next).astype(jnp.float32)
+    near_in = by_place([own_1[:channels], next_1[:channels], far_in, far_next_in])
     squares = lax.dynamic_slice_in_dim(total[live_own, : far * block], far_here * block, block)
     inv_out = lax.rsqrt(squares / CHANNELS + EPSILON)
     current = (before + total * inv_out[:, None]).astype(jnp.bfloat16)
     current = jnp.where((int_range(block) < live_own)[:, None], current, 0)
 
-    gathered = from_everyone(current, "far")
+    part = jnp.concatenate([own_1[channels:], next_1[channels:]], axis=0)
+    part, current = lax.optimization_barrier((part, current))
+    came, gathered = lax.optimization_barrier(
+        (swapped(part, 2), from_everyone(current, "far"))
+    )
+    near_out = by_place(
+        [own_1[channels:], next_1[channels:], came[:channels], came[channels:]]
+    )
     gathered = gathered.reshape(far * block, width)
     pieces = call(in_kernel, pieces_of, "project")(
-        gathered, weights_1[:, :channels], gain_in[1:2], row_of
+        gathered, near_in, gain_in[1:2], row_of
     )
     sent, *done = recur(1, channels, joined(pieces), slot_of, states, weights, done)
     rows_out = width // LANES * own
     pieces = call(
         out_kernel, jax.ShapeDtypeStruct((far, rows_out + 8, LANES), jnp.bfloat16), "out"
-    )(joined(sent).reshape(near, -1, LANES), weights_1[:, channels:])
+    )(joined(sent).reshape(near, -1, LANES), near_out)
     back = exact(pick_back, gathered).reshape(near, few, width)
     pieces, back = lax.optimization_barrier((pieces, back))
     total = summed(pieces)
-    back = jnp.stack(traded([back[d] for d in range(near)])).reshape(near * few, width)
+    came = swapped(back[2:], 2)
+    from_next = swapped(jnp.stack([back[1], came[1]]), 1)
+    back = jnp.stack([back[0], from_next[0], came[0], from_next[1]]).reshape(near * few, width)
     after = jnp.dot(pick_own, back, preferred_element_type=jnp.float32)
     total, after = lax.optimization_barrier((total, after))
     mixed = jnp.concatenate(

time: 304 us -> 312 us (1.026)
    ppermute x9 -> x8, waiting for transfers between devices: 7.71 us -> 42 us  [swapped(): return lax.ppermute(block, 'near', [(p, p ^ d) for p in range(peers)])]
    all_to_all x4, waiting for transfers between devices: 59.3 us -> 42.9 us  [exchanged(): return lax.all_to_all(pieces, axis, 0, 0, tiled=True)]
    all_to_all x2, waiting for transfers between devices: 41.6 us -> 26.7 us  [from_everyone(): lax.all_to_all(jnp.broadcast_to(shard[None], (peers, *shard.shape)), axis...]
    all_to_all x4, starting transfers between devices: 20.6 us -> 23.9 us  [exchanged(): return lax.all_to_all(pieces, axis, 0, 0, tiled=True)]
    ppermute x9 -> x8, starting transfers between devices: 34 us -> 31 us  [swapped(): return lax.ppermute(block, 'near', [(p, p ^ d) for p in range(peers)])]
  transfers between devices with their start and end apart: 15 -> 14, of which waited for: 8 -> 10; matrix products, arithmetic and copies ran while one was open for 6% -> 6% of each run, Pallas kernels for 0% -> 0%
where the time goes in v7:
time: 312 us; the launch traced here: 310 us
  starting transfers between devices  112 us (36%)
  waiting for transfers between devices  112 us (36%)
  blocking collectives  41.8 us (13%)
  local copies, waits for them, and re-layouts  20.6 us (7%)
  Pallas kernels  15.4 us (5%)
  other arithmetic  6.99 us (2%)
    all_to_all x2, starting transfers between devices, from_everyone(): lax.all_to_all(jnp.broadcast_to(shard[None], (peers, *shard.shape)), axis...  57.1 us
    all_to_all x4, waiting for transfers between devices, exchanged(): return lax.all_to_all(pieces, axis, 0, 0, tiled=True)  42.9 us
    ppermute x8, waiting for transfers between devices, swapped(): return lax.ppermute(block, 'near', [(p, p ^ d) for p in range(peers)])  42 us
    all_to_all x2, blocking collectives, exchanged(): return lax.all_to_all(pieces, axis, 0, 0, tiled=True)  41.8 us
    ppermute x8, starting transfers between devices, swapped(): return lax.ppermute(block, 'near', [(p, p ^ d) for p in range(peers)])  31 us
    all_to_all x2, waiting for transfers between devices, from_everyone(): lax.all_to_all(jnp.broadcast_to(shard[None], (peers, *shard.shape)), axis...  26.7 us
    all_to_all x4, starting transfers between devices, exchanged(): return lax.all_to_all(pieces, axis, 0, 0, tiled=True)  23.9 us
  transfers between devices with their start and end apart: 14, of which 10 were waited for; matrix products, arithmetic and copies ran while one was open for 6% of the time, Pallas kernels for 0%

profile of v7, /device:TPU:40, one launch (start us, length us, event | category | flops | bytes accessed | tf_op | source)
XLA Modules:
  0.0 310.1 jit_solution(12350398361665970080)
XLA Ops:
  2.5 9.1 %collective-permute-start = (bf16[128,512]{1,0:T(8,128)(2,1)S(1)}, bf16[128,512]{1,0:T(8,128)(2,1)S(1)}, u32[]{:S(2)}, u32[]{:S(2)}) collective-permute-start(bf16[128,512]{1,0:T(8,128)(2,1)S(1)} %pad_maximum_fusion.5), channel_id=1, source_target_pairs={{0,24},{8,16},{16,8},{24,0},{1,25},{9,17},{17,9},{25,1},{2,26},{10... | collective-permute-start | bytes 393224 | tf_op jit(solution)/shard_map/ppermute | solution.py:29
  11.6 2.0 collective-permute-start.1
  13.6 2.5 collective-permute-start.2
  16.9 40.7 %all-to-all-start = ((bf16[8,32,512]{2,1,0:T(8,128)(2,1)}), bf16[8,32,512]{2,1,0:T(8,128)(2,1)S(1)}, u32[]{:S(2)}, u32[]{:S(2)}) async-start(bf16[8,32,512]{2,1,0:T(8,128)(2,1)} %broadcast_in_dim.46), calls=%async_computation | async-start | bytes 524288 | tf_op jit(solution)/shard_map/all_to_all | solution.py:22
  74.7 14.9 %all-to-all-done = bf16[8,32,512]{2,1,0:T(8,128)(2,1)S(1)} async-done(((bf16[8,32,512]{2,1,0:T(8,128)(2,1)}), bf16[8,32,512]{2,1,0:T(8,128)(2,1)S(1)}, u32[]{:S(2)}, u32[]{:S(2)}) %all-to-all-start) | async-done | bytes 262176 | tf_op jit(solution)/shard_map/all_to_all | solution.py:22
  91.1 2.2 project.2
  93.3 26.2 %all_to_all.40 = bf16[32,32,128]{2,1,0:T(8,128)(2,1)} all-to-all(bf16[32,32,128]{2,1,0:T(8,128)(2,1)} %bitcast.107), channel_id=1, replica_groups=mesh['grp'=2,'far'=8,'near'=4,'dp'=8] {'near','dp'}, dimensions={0} | all-to-all | bytes 524288 | tf_op jit(solution)/shard_map/all_to_all | solution.py:44
  119.5 2.6 recur.2
  122.1 4.9 %all-to-all-start.2 = ((bf16[32,16,128]{2,1,0:T(8,128)(2,1)}), bf16[32,16,128]{2,1,0:T(8,128)(2,1)S(1)}, u32[]{:S(2)}, u32[]{:S(2)}) async-start(bf16[32,16,128]{2,1,0:T(8,128)(2,1)} %bitcast.115), calls=%async_computation.2 | async-start | bytes 262144 | tf_op jit(solution)/shard_map/all_to_all | solution.py:44
  128.7 6.4 %all-to-all-done.2 = bf16[32,16,128]{2,1,0:T(8,128)(2,1)S(1)} async-done(((bf16[32,16,128]{2,1,0:T(8,128)(2,1)}), bf16[32,16,128]{2,1,0:T(8,128)(2,1)S(1)}, u32[]{:S(2)}, u32[]{:S(2)}) %all-to-all-start.2) | async-done | bytes 131104 | tf_op jit(solution)/shard_map/all_to_all | solution.py:44
  135.7 3.0 live_out.1
  138.7 5.1 %all-to-all-start.3 = ((bf16[8,16,512]{2,1,0:T(8,128)(2,1)}), bf16[8,16,512]{2,1,0:T(8,128)(2,1)S(1)}, u32[]{:S(2)}, u32[]{:S(2)}) async-start(bf16[8,16,512]{2,1,0:T(8,128)(2,1)} %live_out.1), calls=%async_computation.3 | async-start | bytes 262144 | tf_op jit(solution)/shard_map/all_to_all | solution.py:44
  143.8 2.7 collective-permute-start.3
  146.5 17.7 %collective-permute-done.3 = bf16[160,512]{1,0:T(8,128)(2,1)S(1)} collective-permute-done((bf16[160,512]{1,0:T(8,128)(2,1)S(1)}, bf16[160,512]{1,0:T(8,128)(2,1)S(1)}, u32[]{:S(2)}, u32[]{:S(2)}) %collective-permute-start.3) | collective-permute-done | bytes 163872 | tf_op jit(solution)/shard_map/ppermute | solution.py:29
  164.2 2.0 collective-permute-start.4
  166.2 8.0 %all-to-all-done.3 = bf16[8,16,512]{2,1,0:T(8,128)(2,1)S(1)} async-done(((bf16[8,16,512]{2,1,0:T(8,128)(2,1)}), bf16[8,16,512]{2,1,0:T(8,128)(2,1)S(1)}, u32[]{:S(2)}, u32[]{:S(2)}) %all-to-all-start.3) | async-done | bytes 131104 | tf_op jit(solution)/shard_map/all_to_all | solution.py:44
  175.2 16.3 %all-to-all-start.4 = ((bf16[8,16,512]{2,1,0:T(8,128)(2,1)}), bf16[8,16,512]{2,1,0:T(8,128)(2,1)S(1)}, u32[]{:S(2)}, u32[]{:S(2)}) async-start(bf16[8,16,512]{2,1,0:T(8,128)(2,1)} %broadcast_in_dim.57), calls=%async_computation.4 | async-start | bytes 262144 | tf_op jit(solution)/shard_map/all_to_all | solution.py:22
  191.5 1.9 collective-permute-start.5
  194.2 14.1 %collective-permute-done.5 = bf16[128,512]{1,0:T(8,128)(2,1)S(1)} collective-permute-done((bf16[128,512]{1,0:T(8,128)(2,1)S(1)}, bf16[128,512]{1,0:T(8,128)(2,1)S(1)}, u32[]{:S(2)}, u32[]{:S(2)}) %collective-permute-start.5) | collective-permute-done | bytes 131104 | tf_op jit(solution)/shard_map/ppermute | solution.py:29
  208.3 11.8 %all-to-all-done.4 = bf16[8,16,512]{2,1,0:T(8,128)(2,1)S(1)} async-done(((bf16[8,16,512]{2,1,0:T(8,128)(2,1)}), bf16[8,16,512]{2,1,0:T(8,128)(2,1)S(1)}, u32[]{:S(2)}, u32[]{:S(2)}) %all-to-all-start.4) | async-done | bytes 131104 | tf_op jit(solution)/shard_map/all_to_all | solution.py:22
  220.8 2.7 project.3
  223.5 15.6 %all_to_all.41 = bf16[32,32,128]{2,1,0:T(8,128)(2,1)} all-to-all(bf16[32,32,128]{2,1,0:T(8,128)(2,1)} %bitcast.111), channel_id=1, replica_groups=mesh['grp'=2,'far'=8,'near'=4,'dp'=8] {'near','dp'}, dimensions={0} | all-to-all | bytes 524288 | tf_op jit(solution)/shard_map/all_to_all | solution.py:44
  239.1 2.6 recur.3
  241.7 4.8 %all-to-all-start.6 = ((bf16[32,16,128]{2,1,0:T(8,128)(2,1)}), bf16[32,16,128]{2,1,0:T(8,128)(2,1)S(1)}, u32[]{:S(2)}, u32[]{:S(2)}) async-start(bf16[32,16,128]{2,1,0:T(8,128)(2,1)} %bitcast.112), calls=%async_computation.6 | async-start | bytes 262144 | tf_op jit(solution)/shard_map/all_to_all | solution.py:44
  247.5 7.0 %all-to-all-done.6 = bf16[32,16,128]{2,1,0:T(8,128)(2,1)S(1)} async-done(((bf16[32,16,128]{2,1,0:T(8,128)(2,1)}), bf16[32,16,128]{2,1,0:T(8,128)(2,1)S(1)}, u32[]{:S(2)}, u32[]{:S(2)}) %all-to-all-start.6) | async-done | bytes 131104 | tf_op jit(solution)/shard_map/all_to_all | solution.py:44
  255.2 2.3 out.1
  257.5 9.2 %all-to-all-start.7 = ((bf16[8,136,128]{2,1,0:T(8,128)(2,1)}), bf16[8,136,128]{2,1,0:T(8,128)(2,1)S(1)}, u32[]{:S(2)}, u32[]{:S(2)}) async-start(bf16[8,136,128]{2,1,0:T(8,128)(2,1)} %out.1), calls=%async_computation.7 | async-start | bytes 557056 | tf_op jit(solution)/shard_map/all_to_all | solution.py:44
  266.7 2.7 collective-permute-start.6
  269.4 7.7 %collective-permute-done.6 = bf16[2,8,512]{2,1,0:T(8,128)(2,1)S(1)} collective-permute-done((bf16[2,8,512]{2,1,0:T(8,128)(2,1)S(1)}, bf16[2,8,512]{2,1,0:T(8,128)(2,1)S(1)}, u32[]{:S(2)}, u32[]{:S(2)}) %collective-permute-start.6) | collective-permute-done | bytes 16416 | tf_op jit(solution)/shard_map/ppermute | solution.py:29
  277.1 8.1 %collective-permute-start.7 = (bf16[2,8,512]{2,1,0:T(8,128)(2,1)S(1)}, bf16[2,8,512]{2,1,0:T(8,128)(2,1)S(1)}, u32[]{:S(2)}, u32[]{:S(2)}) collective-permute-start(bf16[2,8,512]{2,1,0:T(8,128)(2,1)S(1)} %pad_maximum_fusion.8), channel_id=1, source_target_pairs={{0,8},{8,0},{16,24},{24,16},{1,9},{9,1},{17,25},{25,17},{2,10},{10... | collective-permute-start | bytes 49160 | tf_op jit(solution)/shard_map/ppermute | solution.py:29
  285.2 2.5 collective-permute-done.7
  287.9 21.5 %all-to-all-done.7 = bf16[8,136,128]{2,1,0:T(8,128)(2,1)S(1)} async-done(((bf16[8,136,128]{2,1,0:T(8,128)(2,1)}), bf16[8,136,128]{2,1,0:T(8,128)(2,1)S(1)}, u32[]{:S(2)}, u32[]{:S(2)}) %all-to-all-start.7) | async-done | bytes 278560 | tf_op jit(solution)/shard_map/all_to_all | solution.py:44
  (188 shorter events, 28.0 us)
Async XLA Ops:
  1.4 1.0 copy-start.8
  2.5 71.9 %collective-permute-start = (bf16[128,512]{1,0:T(8,128)(2,1)S(1)}, bf16[128,512]{1,0:T(8,128)(2,1)S(1)}, u32[]{:S(2)}, u32[]{:S(2)}) collective-permute-start(bf16[128,512]{1,0:T(8,128)(2,1)S(1)} %pad_maximum_fusion.5), channel_id=1, source_target_pairs={{0,24},{8,16},{16,8},{24,0},{1,25},{9,17},{17,9},{25,1},{2,26},{10... | collective-permute-start | bytes 393224 | tf_op jit(solution)/shard_map/ppermute | solution.py:29
  11.6 62.8 %collective-permute-start.1 = (bf16[128,512]{1,0:T(8,128)(2,1)S(1)}, bf16[128,512]{1,0:T(8,128)(2,1)S(1)}, u32[]{:S(2)}, u32[]{:S(2)}) collective-permute-start(bf16[128,512]{1,0:T(8,128)(2,1)S(1)} %pad_maximum_fusion.5), channel_id=1, source_target_pairs={{0,16},{8,24},{16,0},{24,8},{1,17},{9,25},{17,1},{25,9},{2,18},{10... | collective-permute-start | bytes 393224 | tf_op jit(solution)/shard_map/ppermute | solution.py:29
  13.6 2.6 copy-start.11
  13.6 60.8 %collective-permute-start.2 = (bf16[256,512]{1,0:T(8,128)(2,1)S(1)}, bf16[256,512]{1,0:T(8,128)(2,1)S(1)}, u32[]{:S(2)}, u32[]{:S(2)}) collective-permute-start(bf16[256,512]{1,0:T(8,128)(2,1)S(1)} %pad_maximum_fusion.1), channel_id=1, source_target_pairs={{0,8},{8,0},{16,24},{24,16},{1,9},{9,1},{17,25},{25,17},{2,10},{10... | collective-permute-start | bytes 786440 | tf_op jit(solution)/shard_map/ppermute | solution.py:29
  16.9 72.7 %all-to-all-start = ((bf16[8,32,512]{2,1,0:T(8,128)(2,1)}), bf16[8,32,512]{2,1,0:T(8,128)(2,1)S(1)}, u32[]{:S(2)}, u32[]{:S(2)}) async-start(bf16[8,32,512]{2,1,0:T(8,128)(2,1)} %broadcast_in_dim.46), calls=%async_computation | async-start | bytes 524288 | tf_op jit(solution)/shard_map/all_to_all | solution.py:22
  63.0 1.6 copy-start.20
  63.1 1.7 copy-start.16
  63.1 1.7 copy-start.19
  63.4 1.8 copy-start.13
  63.4 1.8 copy-start.14
  66.9 0.8 copy-start.12
  67.7 2.5 copy-start.15
  73.1 0.8 copy-start.21
  74.4 52.8 %copy-start.2 = (bf16[128,512]{1,0:T(8,128)(2,1)}, bf16[128,512]{1,0:T(8,128)(2,1)S(1)}, u32[]{:S(2)}) copy-start(bf16[128,512]{1,0:T(8,128)(2,1)S(1)} %pad_maximum_fusion.6) | copy-start | bytes 393220
  89.6 1.6 copy-start
  122.1 4.9 %copy-start.1 = (bf16[8,32,512]{2,1,0:T(8,128)(2,1)S(1)}, bf16[8,32,512]{2,1,0:T(8,128)(2,1)}, u32[]{:S(2)}) copy-start(bf16[8,32,512]{2,1,0:T(8,128)(2,1)} %copy-done) | copy-start | bytes 786436
  122.1 13.0 %all-to-all-start.2 = ((bf16[32,16,128]{2,1,0:T(8,128)(2,1)}), bf16[32,16,128]{2,1,0:T(8,128)(2,1)S(1)}, u32[]{:S(2)}, u32[]{:S(2)}) async-start(bf16[32,16,128]{2,1,0:T(8,128)(2,1)} %bitcast.115), calls=%async_computation.2 | async-start | bytes 262144 | tf_op jit(solution)/shard_map/all_to_all | solution.py:44
  127.8 0.8 slice-start
  127.8 0.8 slice-start.1
  138.7 25.5 %copy-start.7 = (bf16[64,512]{1,0:T(8,128)(2,1)S(1)}, bf16[64,512]{1,0:T(8,128)(2,1)}, u32[]{:S(2)}) copy-start(bf16[64,512]{1,0:T(8,128)(2,1)} %copy-done.6) | copy-start | bytes 196612
  138.7 35.5 %all-to-all-start.3 = ((bf16[8,16,512]{2,1,0:T(8,128)(2,1)}), bf16[8,16,512]{2,1,0:T(8,128)(2,1)S(1)}, u32[]{:S(2)}, u32[]{:S(2)}) async-start(bf16[8,16,512]{2,1,0:T(8,128)(2,1)} %live_out.1), calls=%async_computation.3 | async-start | bytes 262144 | tf_op jit(solution)/shard_map/all_to_all | solution.py:44
  143.8 20.4 %collective-permute-start.3 = (bf16[160,512]{1,0:T(8,128)(2,1)S(1)}, bf16[160,512]{1,0:T(8,128)(2,1)S(1)}, u32[]{:S(2)}, u32[]{:S(2)}) collective-permute-start(bf16[160,512]{1,0:T(8,128)(2,1)S(1)} %pad_maximum_fusion.4), channel_id=1, source_target_pairs={{0,16},{8,24},{16,0},{24,8},{1,17},{9,25},{17,1},{25,9},{2,18},{10... | collective-permute-start | bytes 491528 | tf_op jit(solution)/shard_map/ppermute | solution.py:29
  164.2 10.1 %collective-permute-start.4 = (bf16[16,512]{1,0:T(8,128)(2,1)S(1)}, bf16[16,512]{1,0:T(8,128)(2,1)S(1)}, u32[]{:S(2)}, u32[]{:S(2)}) collective-permute-start(bf16[16,512]{1,0:T(8,128)(2,1)S(1)} %get-tuple-element.90), channel_id=1, source_target_pairs={{0,8},{8,0},{16,24},{24,16},{1,9},{9,1},{17,25},{25,17},{2,10},{10... | collective-permute-start | bytes 49160 | tf_op jit(solution)/shard_map/ppermute | solution.py:29
  166.2 8.2 %copy-start.3 = (bf16[128,512]{1,0:T(8,128)(2,1)S(1)}, bf16[128,512]{1,0:T(8,128)(2,1)}, u32[]{:S(2)}) copy-start(bf16[128,512]{1,0:T(8,128)(2,1)} %copy-done.2) | copy-start | bytes 393220
  175.2 45.0 %all-to-all-start.4 = ((bf16[8,16,512]{2,1,0:T(8,128)(2,1)}), bf16[8,16,512]{2,1,0:T(8,128)(2,1)S(1)}, u32[]{:S(2)}, u32[]{:S(2)}) async-start(bf16[8,16,512]{2,1,0:T(8,128)(2,1)} %broadcast_in_dim.57), calls=%async_computation.4 | async-start | bytes 262144 | tf_op jit(solution)/shard_map/all_to_all | solution.py:22
  191.5 16.8 %collective-permute-start.5 = (bf16[128,512]{1,0:T(8,128)(2,1)S(1)}, bf16[128,512]{1,0:T(8,128)(2,1)S(1)}, u32[]{:S(2)}, u32[]{:S(2)}) collective-permute-start(bf16[128,512]{1,0:T(8,128)(2,1)S(1)} %pad_maximum_fusion.7), channel_id=1, source_target_pairs={{0,16},{8,24},{16,0},{24,8},{1,17},{9,25},{17,1},{25,9},{2,18},{10... | collective-permute-start | bytes 393224 | tf_op jit(solution)/shard_map/ppermute | solution.py:29
  241.7 12.8 %all-to-all-start.6 = ((bf16[32,16,128]{2,1,0:T(8,128)(2,1)}), bf16[32,16,128]{2,1,0:T(8,128)(2,1)S(1)}, u32[]{:S(2)}, u32[]{:S(2)}) async-start(bf16[32,16,128]{2,1,0:T(8,128)(2,1)} %bitcast.112), calls=%async_computation.6 | async-start | bytes 262144 | tf_op jit(solution)/shard_map/all_to_all | solution.py:44
  246.5 0.9 copy-start.5
  257.5 51.8 %all-to-all-start.7 = ((bf16[8,136,128]{2,1,0:T(8,128)(2,1)}), bf16[8,136,128]{2,1,0:T(8,128)(2,1)S(1)}, u32[]{:S(2)}, u32[]{:S(2)}) async-start(bf16[8,136,128]{2,1,0:T(8,128)(2,1)} %out.1), calls=%async_computation.7 | async-start | bytes 557056 | tf_op jit(solution)/shard_map/all_to_all | solution.py:44
  266.7 10.4 %collective-permute-start.6 = (bf16[2,8,512]{2,1,0:T(8,128)(2,1)S(1)}, bf16[2,8,512]{2,1,0:T(8,128)(2,1)S(1)}, u32[]{:S(2)}, u32[]{:S(2)}) collective-permute-start(bf16[2,8,512]{2,1,0:T(8,128)(2,1)S(1)} %slice.152), channel_id=1, source_target_pairs={{0,16},{8,24},{16,0},{24,8},{1,17},{9,25},{17,1},{25,9},{2,18},{10... | collective-permute-start | bytes 49160 | tf_op jit(solution)/shard_map/ppermute | solution.py:29
  277.1 10.6 %collective-permute-start.7 = (bf16[2,8,512]{2,1,0:T(8,128)(2,1)S(1)}, bf16[2,8,512]{2,1,0:T(8,128)(2,1)S(1)}, u32[]{:S(2)}, u32[]{:S(2)}) collective-permute-start(bf16[2,8,512]{2,1,0:T(8,128)(2,1)S(1)} %pad_maximum_fusion.8), channel_id=1, source_target_pairs={{0,8},{8,0},{16,24},{24,16},{1,9},{9,1},{17,25},{25,17},{2,10},{10... | collective-permute-start | bytes 49160 | tf_op jit(solution)/shard_map/ppermute | solution.py:29
  (6 other events, 3.9 us)

commit v8 on v6

--- a/solution.py
+++ b/solution.py
@@ -142,6 +142,7 @@
         cost_estimate=pl.CostEstimate(
             flops=200_000_000, bytes_accessed=1 << 20, transcendentals=1 << 14
         ),
+        compiler_params=pltpu.CompilerParams(vmem_limit_bytes=16 << 20),
         name=name,
     )
 
@@ -172,10 +173,9 @@
     return product(one, (rows * rows).astype(jnp.bfloat16), ((1,), (1,)))
 
 
-def in_kernel(gathered, near_in, gain_row, *rest):
+def in_kernel(channels, gathered, both, gain_row, *rest):
     *row_of, pieces = rest
     near, dp, own, _ = pieces.shape
-    channels = near_in.shape[1]
     values = gathered[...].astype(jnp.float32)
     rows = values.shape[0]
     squares = jnp.sum(values * values, axis=1, keepdims=True)
@@ -185,14 +185,14 @@
         spread = lax.broadcasted_iota(jnp.int32, (rows, dp * own), 0) == row_of[0][...]
         spread = spread.astype(jnp.float32).astype(jnp.bfloat16)
     for n in range(near):
-        out = product(scaled, with_zeros(near_in[n]), ((1,), (1,)))
+        out = product(scaled, with_zeros(both[n, :channels]), ((1,), (1,)))
         out = jnp.where(lane == channels, squares, out).astype(jnp.bfloat16)
         if row_of:
             out = product(spread, out, ((0,), (0,))).astype(jnp.bfloat16)
         pieces[n] = out.reshape(dp, own, LANES)
 
 
-def live_out_kernel(live_own, arrived, w_out, row_of, pieces):
+def live_out_kernel(channels, live_own, arrived, both, row_of, pieces):
     near, slots, _ = arrived.shape
     far, rows, width = pieces.shape
     at = lax.broadcasted_iota(jnp.int32, (far * rows, slots), 0)
@@ -201,7 +201,7 @@
         pick = (at == row_of[half : half + 1]).astype(jnp.float32).astype(jnp.bfloat16)
         for n in range(near):
             live = product(pick, arrived[n], ((1,), (0,))).astype(jnp.bfloat16)
-            partial += product(live, with_zeros(w_out[n], half == 1), ((1,), (0,)))
+            partial += product(live, with_zeros(both[n, channels:], half == 1), ((1,), (0,)))
             squares += squared(live, half)
     squares = jnp.concatenate(
         [squares[:1], jnp.zeros((1, width - far * rows), jnp.float32)], axis=1
@@ -211,17 +211,17 @@
     pieces[...] = partial.astype(jnp.bfloat16).reshape(pieces.shape)
 
 
-def out_kernel(arrived, w_out, pieces):
+def out_kernel(channels, arrived, both, pieces):
     near, rows, _ = arrived.shape
     far, _, _ = pieces.shape
-    width = w_out.shape[2]
+    width = both.shape[2]
     few = rows // far
     own = 2 * few
     lasts = []
     for half in range(2):
         partial, squares = 0.0, 0.0
         for n in range(near):
-            partial += product(arrived[n], with_zeros(w_out[n], half == 1), ((1,), (0,)))
+            partial += product(arrived[n], with_zeros(both[n, channels:], half == 1), ((1,), (0,)))
             squares += squared(arrived[n], half)
         lasts.append(squares)
         for f in range(far):
@@ -342,23 +342,24 @@
     picks = (pick_kept, pick_back, pick_own)
     tables = (slot_of, row_of, row_of_half, picks, weights, weights_of(1))
     gathered, weights_0, tables = lax.optimization_barrier((gathered, weights_0, tables))
-    slot_of, row_of, row_of_half, picks, weights, weights_1 = tables
+    slot_of, row_of, row_of_half, picks, weights, own_1 = tables
     pick_kept, pick_back, pick_own = picks
     gathered = gathered.reshape(far * own, width)
-    pieces = call(in_kernel, pieces_of, "project")(gathered, weights_0[:, :channels], gain_in[0:1])
-    sent, *done = recur(0, channels, joined(pieces), slot_of, states, weights, ())
+    project = call(functools.partial(in_kernel, channels), pieces_of, "project")
+    pieces = project(gathered, weights_0, gain_in[0:1])
+    handed = exact(pick_kept, gathered).reshape(near, block, width)
+    parts = [jnp.concatenate([own_1, handed[d]], axis=0) for d in range(near)]
+    pieces, parts = lax.optimization_barrier((pieces, parts))
+    arrived, came = lax.optimization_barrier((joined(pieces), traded(parts)))
+    before = sum(c[2 * channels :].astype(jnp.float32) for c in came)
+    weights_1 = by_place([c[: 2 * channels] for c in came])
+    sent, *done = recur(0, channels, arrived, slot_of, states, weights, ())
     pieces = call(
-        functools.partial(live_out_kernel, live_own),
+        functools.partial(live_out_kernel, channels, live_own),
         jax.ShapeDtypeStruct((far, block, width), jnp.bfloat16),
         "live_out",
-    )(joined(sent).reshape(near, -1, LANES), weights_0[:, channels:], row_of_half)
-    handed = exact(pick_kept, gathered).reshape(near, block, width)
-    parts = [jnp.concatenate([weights_1, handed[d]], axis=0) for d in range(near)]
-    pieces, parts = lax.optimization_barrier((pieces, parts))
+    )(joined(sent).reshape(near, -1, LANES), weights_0, row_of_half)
     total = summed(pieces)
-    total, came = lax.optimization_barrier((total, traded(parts)))
-    before = sum(c[2 * channels :].astype(jnp.float32) for c in came)
-    weights_1 = by_place([c[: 2 * channels] for c in came])
     squares = lax.dynamic_slice_in_dim(total[live_own, : far * block], far_here * block, block)
     inv_out = lax.rsqrt(squares / CHANNELS + EPSILON)
     current = (before + total * inv_out[:, None]).astype(jnp.bfloat16)
@@ -366,14 +367,14 @@
 
     gathered = from_everyone(current, "far")
     gathered = gathered.reshape(far * block, width)
-    pieces = call(in_kernel, pieces_of, "project")(
-        gathered, weights_1[:, :channels], gain_in[1:2], row_of
-    )
+    pieces = project(gathered, weights_1, gain_in[1:2], row_of)
     sent, *done = recur(1, channels, joined(pieces), slot_of, states, weights, done)
     rows_out = width // LANES * own
     pieces = call(
-        out_kernel, jax.ShapeDtypeStruct((far, rows_out + 8, LANES), jnp.bfloat16), "out"
-    )(joined(sent).reshape(near, -1, LANES), weights_1[:, channels:])
+        functools.partial(out_kernel, channels),
+        jax.ShapeDtypeStruct((far, rows_out + 8, LANES), jnp.bfloat16),
+        "out",
+    )(joined(sent).reshape(near, -1, LANES), weights_1)
     back = exact(pick_back, gathered).reshape(near, few, width)
     pieces, back = lax.optimization_barrier((pieces, back))
     total = summed(pieces)

time: 304 us -> 293 us (0.964)
  waiting for transfers between devices: 109 us -> 125 us
  blocking collectives: 41.7 us -> 32 us
  Pallas kernels: 15.4 us -> 7.58 us
  local copies, waits for them, and re-layouts: 19.9 us -> 13.5 us
    all_to_all x2, starting transfers between devices: 54.7 us -> 44.9 us  [from_everyone(): lax.all_to_all(jnp.broadcast_to(shard[None], (peers, *shard.shape)), axis...]
    all_to_all x2, blocking collectives: 41.7 us -> 32 us  [exchanged(): return lax.all_to_all(pieces, axis, 0, 0, tiled=True)]
    ppermute x9, waiting for transfers between devices: 7.71 us -> 16.4 us  [traded(): lax.ppermute(parts[d], 'near', [(p, p ^ d) for p in range(peers)])]
    all_to_all x4, starting transfers between devices: 20.6 us -> 29.3 us  [exchanged(): return lax.all_to_all(pieces, axis, 0, 0, tiled=True)]
    all_to_all x2, waiting for transfers between devices: 41.6 us -> 47.3 us  [from_everyone(): lax.all_to_all(jnp.broadcast_to(shard[None], (peers, *shard.shape)), axis...]
    pallas_call x4, Pallas kernels: 10.2 us -> 5.43 us  [the longest x1 2.02 us: per_device(): call(functools.partial(live_out_kernel, channels, live_own), jax.ShapeDty...]
    pallas_call x2, Pallas kernels: 5.2 us -> 2.15 us  [recur(): call(functools.partial(recur_kernel, depth, channels, rows // seqs), (jax...]
  transfers between devices with their start and end apart: 15 -> 15, of which waited for: 8 -> 8; matrix products, arithmetic and copies ran while one was open for 6% -> 4% of each run, Pallas kernels for 0% -> 0%
where the time goes in v8:
time: 293 us; the launch traced here: 292 us
  waiting for transfers between devices  125 us (43%)
  starting transfers between devices  108 us (37%)
  blocking collectives  32 us (11%)
  local copies, waits for them, and re-layouts  13.5 us (5%)
  Pallas kernels  7.58 us (3%)
  other arithmetic  3.9 us (1%)
    all_to_all x4, waiting for transfers between devices, exchanged(): return lax.all_to_all(pieces, axis, 0, 0, tiled=True)  61.1 us
    all_to_all x2, waiting for transfers between devices, from_everyone(): lax.all_to_all(jnp.broadcast_to(shard[None], (peers, *shard.shape)), axis...  47.3 us
    all_to_all x2, starting transfers between devices, from_everyone(): lax.all_to_all(jnp.broadcast_to(shard[None], (peers, *shard.shape)), axis...  44.9 us
    ppermute x9, starting transfers between devices, traded(): lax.ppermute(parts[d], 'near', [(p, p ^ d) for p in range(peers)])  34 us
    all_to_all x2, blocking collectives, exchanged(): return lax.all_to_all(pieces, axis, 0, 0, tiled=True)  32 us
    all_to_all x4, starting transfers between devices, exchanged(): return lax.all_to_all(pieces, axis, 0, 0, tiled=True)  29.3 us
    ppermute x9, waiting for transfers between devices, traded(): lax.ppermute(parts[d], 'near', [(p, p ^ d) for p in range(peers)])  16.4 us
  transfers between devices with their start and end apart: 15, of which 8 were waited for; matrix products, arithmetic and copies ran while one was open for 4% of the time, Pallas kernels for 0%

profile of v8, /device:TPU:40, one launch (start us, length us, event | category | flops | bytes accessed | tf_op | source)
XLA Modules:
  0.0 291.8 jit_solution(1805986408470062475)
XLA Ops:
  0.6 0.8 slice_bitcast_fusion.5
  1.4 0.9 slice_bitcast_fusion
  2.5 9.1 %collective-permute-start = (bf16[128,512]{1,0:T(8,128)(2,1)S(1)}, bf16[128,512]{1,0:T(8,128)(2,1)S(1)}, u32[]{:S(2)}, u32[]{:S(2)}) collective-permute-start(bf16[128,512]{1,0:T(8,128)(2,1)S(1)} %pad_maximum_fusion.6), channel_id=1, source_target_pairs={{0,24},{8,16},{16,8},{24,0},{1,25},{9,17},{17,9},{25,1},{2,26},{10... | collective-permute-start | bytes 393224 | tf_op jit(solution)/shard_map/ppermute | solution.py:30
  11.6 2.0 collective-permute-start.1
  13.6 2.5 collective-permute-start.2
  16.8 40.7 %all-to-all-start = ((bf16[8,32,512]{2,1,0:T(8,128)(2,1)}), bf16[8,32,512]{2,1,0:T(8,128)(2,1)S(1)}, u32[]{:S(2)}, u32[]{:S(2)}) async-start(bf16[8,32,512]{2,1,0:T(8,128)(2,1)} %broadcast_in_dim.47), calls=%async_computation | async-start | bytes 524288 | tf_op jit(solution)/shard_map/all_to_all | solution.py:22
  71.1 18.6 %all-to-all-done = bf16[8,32,512]{2,1,0:T(8,128)(2,1)S(1)} async-done(((bf16[8,32,512]{2,1,0:T(8,128)(2,1)}), bf16[8,32,512]{2,1,0:T(8,128)(2,1)S(1)}, u32[]{:S(2)}, u32[]{:S(2)}) %all-to-all-start) | async-done | bytes 262176 | tf_op jit(solution)/shard_map/all_to_all | solution.py:22
  89.9 1.1 project.2
  91.1 14.0 %all-to-all-start.1 = ((bf16[32,32,128]{2,1,0:T(8,128)(2,1)}), bf16[32,32,128]{2,1,0:T(8,128)(2,1)S(1)}, u32[]{:S(2)}, u32[]{:S(2)}) async-start(bf16[32,32,128]{2,1,0:T(8,128)(2,1)} %bitcast.29), calls=%async_computation.1 | async-start | bytes 524288 | tf_op jit(solution)/shard_map/all_to_all | solution.py:47
  105.1 3.3 %collective-permute-start.3 = (bf16[144,512]{1,0:T(8,128)(2,1)S(1)}, bf16[144,512]{1,0:T(8,128)(2,1)S(1)}, u32[]{:S(2)}, u32[]{:S(2)}) collective-permute-start(bf16[144,512]{1,0:T(8,128)(2,1)S(1)} %get-tuple-element.42), channel_id=1, source_target_pairs={{0,8},{8,0},{16,24},{24,16},{1,9},{9,1},{17,25},{25,17},{2,10},{10... | collective-permute-start | bytes 442376 | tf_op jit(solution)/shard_map/ppermute | solution.py:30
  108.4 4.4 %collective-permute-start.4 = (bf16[144,512]{1,0:T(8,128)(2,1)S(1)}, bf16[144,512]{1,0:T(8,128)(2,1)S(1)}, u32[]{:S(2)}, u32[]{:S(2)}) collective-permute-start(bf16[144,512]{1,0:T(8,128)(2,1)S(1)} %get-tuple-element.43), channel_id=1, source_target_pairs={{0,16},{8,24},{16,0},{24,8},{1,17},{9,25},{17,1},{25,9},{2,18},{10... | collective-permute-start | bytes 442376 | tf_op jit(solution)/shard_map/ppermute | solution.py:30
  112.8 2.5 collective-permute-start.5
  115.4 2.2 collective-permute-done.3
  117.6 6.3 %collective-permute-done.4 = bf16[144,512]{1,0:T(8,128)(2,1)S(1)} collective-permute-done((bf16[144,512]{1,0:T(8,128)(2,1)S(1)}, bf16[144,512]{1,0:T(8,128)(2,1)S(1)}, u32[]{:S(2)}, u32[]{:S(2)}) %collective-permute-start.4) | collective-permute-done | bytes 147488 | tf_op jit(solution)/shard_map/ppermute | solution.py:30
  124.7 16.6 %all_to_all.40 = bf16[32,16,128]{2,1,0:T(8,128)(2,1)S(1)} all-to-all(bf16[32,16,128]{2,1,0:T(8,128)(2,1)S(1)} %bitcast.114), channel_id=1, replica_groups=mesh['grp'=2,'far'=8,'near'=4,'dp'=8] {'near','dp'}, dimensions={0} | all-to-all | bytes 262144 | tf_op jit(solution)/shard_map/all_to_all | solution.py:47
  141.2 2.0 live_out.1
  143.3 6.8 %all-to-all-start.3 = ((bf16[8,16,512]{2,1,0:T(8,128)(2,1)}), bf16[8,16,512]{2,1,0:T(8,128)(2,1)S(1)}, u32[]{:S(2)}, u32[]{:S(2)}) async-start(bf16[8,16,512]{2,1,0:T(8,128)(2,1)} %live_out.1), calls=%async_computation.3 | async-start | bytes 262144 | tf_op jit(solution)/shard_map/all_to_all | solution.py:47
  150.1 29.3 %all-to-all-done.3 = bf16[8,16,512]{2,1,0:T(8,128)(2,1)S(1)} async-done(((bf16[8,16,512]{2,1,0:T(8,128)(2,1)}), bf16[8,16,512]{2,1,0:T(8,128)(2,1)S(1)}, u32[]{:S(2)}, u32[]{:S(2)}) %all-to-all-start.3) | async-done | bytes 131104 | tf_op jit(solution)/shard_map/all_to_all | solution.py:47
  180.2 4.1 %all-to-all-start.4 = ((bf16[8,16,512]{2,1,0:T(8,128)(2,1)}), bf16[8,16,512]{2,1,0:T(8,128)(2,1)S(1)}, u32[]{:S(2)}, u32[]{:S(2)}) async-start(bf16[8,16,512]{2,1,0:T(8,128)(2,1)} %broadcast_in_dim.57), calls=%async_computation.4 | async-start | bytes 262144 | tf_op jit(solution)/shard_map/all_to_all | solution.py:22
  184.5 28.7 %all-to-all-done.4 = bf16[8,16,512]{2,1,0:T(8,128)(2,1)S(1)} async-done(((bf16[8,16,512]{2,1,0:T(8,128)(2,1)}), bf16[8,16,512]{2,1,0:T(8,128)(2,1)S(1)}, u32[]{:S(2)}, u32[]{:S(2)}) %all-to-all-start.4) | async-done | bytes 131104 | tf_op jit(solution)/shard_map/all_to_all | solution.py:22
  213.2 1.0 project.3
  214.2 15.4 %all_to_all.41 = bf16[32,32,128]{2,1,0:T(8,128)(2,1)S(1)} all-to-all(bf16[32,32,128]{2,1,0:T(8,128)(2,1)S(1)} %bitcast.111), channel_id=1, replica_groups=mesh['grp'=2,'far'=8,'near'=4,'dp'=8] {'near','dp'}, dimensions={0} | all-to-all | bytes 524288 | tf_op jit(solution)/shard_map/all_to_all | solution.py:47
  229.6 1.4 recur.3
  231.0 4.8 %all-to-all-start.6 = ((bf16[32,16,128]{2,1,0:T(8,128)(2,1)}), bf16[32,16,128]{2,1,0:T(8,128)(2,1)S(1)}, u32[]{:S(2)}, u32[]{:S(2)}) async-start(bf16[32,16,128]{2,1,0:T(8,128)(2,1)} %bitcast.41), calls=%async_computation.6 | async-start | bytes 262144 | tf_op jit(solution)/shard_map/all_to_all | solution.py:47
  236.0 7.9 %all-to-all-done.6 = bf16[32,16,128]{2,1,0:T(8,128)(2,1)S(1)} async-done(((bf16[32,16,128]{2,1,0:T(8,128)(2,1)}), bf16[32,16,128]{2,1,0:T(8,128)(2,1)S(1)}, u32[]{:S(2)}, u32[]{:S(2)}) %all-to-all-start.6) | async-done | bytes 131104 | tf_op jit(solution)/shard_map/all_to_all | solution.py:47
  243.9 1.3 out.1
  245.2 3.6 %all-to-all-start.7 = ((bf16[8,136,128]{2,1,0:T(8,128)(2,1)}), bf16[8,136,128]{2,1,0:T(8,128)(2,1)S(1)}, u32[]{:S(2)}, u32[]{:S(2)}) async-start(bf16[8,136,128]{2,1,0:T(8,128)(2,1)} %out.1), calls=%async_computation.7 | async-start | bytes 557056 | tf_op jit(solution)/shard_map/all_to_all | solution.py:47
  248.8 2.6 collective-permute-start.6
  251.4 3.0 %collective-permute-start.7 = (bf16[8,512]{1,0:T(8,128)(2,1)S(1)}, bf16[8,512]{1,0:T(8,128)(2,1)S(1)}, u32[]{:S(2)}, u32[]{:S(2)}) collective-permute-start(bf16[8,512]{1,0:T(8,128)(2,1)S(1)} %get-tuple-element.97), channel_id=1, source_target_pairs={{0,16},{8,24},{16,0},{24,8},{1,17},{9,25},{17,1},{25,9},{2,18},{10... | collective-permute-start | bytes 24584 | tf_op jit(solution)/shard_map/ppermute | solution.py:30
  254.4 4.6 %collective-permute-start.8 = (bf16[8,512]{1,0:T(8,128)(2,1)S(1)}, bf16[8,512]{1,0:T(8,128)(2,1)S(1)}, u32[]{:S(2)}, u32[]{:S(2)}) collective-permute-start(bf16[8,512]{1,0:T(8,128)(2,1)S(1)} %get-tuple-element.96), channel_id=1, source_target_pairs={{0,24},{8,16},{16,8},{24,0},{1,25},{9,17},{17,9},{25,1},{2,26},{10... | collective-permute-start | bytes 24584 | tf_op jit(solution)/shard_map/ppermute | solution.py:30
  259.1 7.9 %collective-permute-done.6 = bf16[8,512]{1,0:T(8,128)(2,1)S(1)} collective-permute-done((bf16[8,512]{1,0:T(8,128)(2,1)S(1)}, bf16[8,512]{1,0:T(8,128)(2,1)S(1)}, u32[]{:S(2)}, u32[]{:S(2)}) %collective-permute-start.6) | collective-permute-done | bytes 8224 | tf_op jit(solution)/shard_map/ppermute | solution.py:30
  267.1 23.9 %all-to-all-done.7 = bf16[8,136,128]{2,1,0:T(8,128)(2,1)S(1)} async-done(((bf16[8,136,128]{2,1,0:T(8,128)(2,1)}), bf16[8,136,128]{2,1,0:T(8,128)(2,1)S(1)}, u32[]{:S(2)}, u32[]{:S(2)}) %all-to-all-start.7) | async-done | bytes 278560 | tf_op jit(solution)/shard_map/all_to_all | solution.py:47
  (159 shorter events, 16.9 us)
Async XLA Ops:
  1.4 1.0 copy-start.2
  2.4 13.7 %copy-start.3 = (bf16[4,8,512]{2,1,0:T(8,128)(2,1)S(1)}, bf16[4,8,512]{2,1,0:T(8,128)(2,1)}, u32[]{:S(2)}) copy-start(bf16[4,8,512]{2,1,0:T(8,128)(2,1)} %param.16) | copy-start | bytes 98308
  2.5 68.3 %collective-permute-start = (bf16[128,512]{1,0:T(8,128)(2,1)S(1)}, bf16[128,512]{1,0:T(8,128)(2,1)S(1)}, u32[]{:S(2)}, u32[]{:S(2)}) collective-permute-start(bf16[128,512]{1,0:T(8,128)(2,1)S(1)} %pad_maximum_fusion.6), channel_id=1, source_target_pairs={{0,24},{8,16},{16,8},{24,0},{1,25},{9,17},{17,9},{25,1},{2,26},{10... | collective-permute-start | bytes 393224 | tf_op jit(solution)/shard_map/ppermute | solution.py:30
  11.6 59.2 %collective-permute-start.1 = (bf16[128,512]{1,0:T(8,128)(2,1)S(1)}, bf16[128,512]{1,0:T(8,128)(2,1)S(1)}, u32[]{:S(2)}, u32[]{:S(2)}) collective-permute-start(bf16[128,512]{1,0:T(8,128)(2,1)S(1)} %pad_maximum_fusion.6), channel_id=1, source_target_pairs={{0,16},{8,24},{16,0},{24,8},{1,17},{9,25},{17,1},{25,9},{2,18},{10... | collective-permute-start | bytes 393224 | tf_op jit(solution)/shard_map/ppermute | solution.py:30
  13.6 57.2 %collective-permute-start.2 = (bf16[128,512]{1,0:T(8,128)(2,1)S(1)}, bf16[128,512]{1,0:T(8,128)(2,1)S(1)}, u32[]{:S(2)}, u32[]{:S(2)}) collective-permute-start(bf16[128,512]{1,0:T(8,128)(2,1)S(1)} %pad_maximum_fusion.6), channel_id=1, source_target_pairs={{0,8},{8,0},{16,24},{24,16},{1,9},{9,1},{17,25},{25,17},{2,10},{10... | collective-permute-start | bytes 393224 | tf_op jit(solution)/shard_map/ppermute | solution.py:30
  16.8 72.8 %all-to-all-start = ((bf16[8,32,512]{2,1,0:T(8,128)(2,1)}), bf16[8,32,512]{2,1,0:T(8,128)(2,1)S(1)}, u32[]{:S(2)}, u32[]{:S(2)}) async-start(bf16[8,32,512]{2,1,0:T(8,128)(2,1)} %broadcast_in_dim.47), calls=%async_computation | async-start | bytes 524288 | tf_op jit(solution)/shard_map/all_to_all | solution.py:22
  57.6 0.7 copy-start.9
  62.2 1.1 copy-start.12
  62.2 1.2 copy-start.8
  62.2 1.3 copy-start.11
  62.2 1.7 copy-start.6
  62.2 1.6 copy-start.5
  65.5 0.8 copy-start.4
  66.4 0.7 copy-start.10
  66.4 2.7 copy-start.7
  70.1 0.7 copy-start.13
  91.1 32.8 %copy-start = (f32[2,16,256]{2,1,0:T(8,128)S(1)}, f32[2,16,256]{2,1,0:T(8,128)}, u32[]{:S(2)}) copy-start(f32[2,16,256]{2,1,0:T(8,128)} %re.3) | copy-start | bytes 98308
  91.1 32.8 %copy-start.1 = (f32[2,16,256]{2,1,0:T(8,128)S(1)}, f32[2,16,256]{2,1,0:T(8,128)}, u32[]{:S(2)}) copy-start(f32[2,16,256]{2,1,0:T(8,128)} %im.3) | copy-start | bytes 98308
  91.1 32.8 %all-to-all-start.1 = ((bf16[32,32,128]{2,1,0:T(8,128)(2,1)}), bf16[32,32,128]{2,1,0:T(8,128)(2,1)S(1)}, u32[]{:S(2)}, u32[]{:S(2)}) async-start(bf16[32,32,128]{2,1,0:T(8,128)(2,1)} %bitcast.29), calls=%async_computation.1 | async-start | bytes 524288 | tf_op jit(solution)/shard_map/all_to_all | solution.py:47
  105.1 12.5 %collective-permute-start.3 = (bf16[144,512]{1,0:T(8,128)(2,1)S(1)}, bf16[144,512]{1,0:T(8,128)(2,1)S(1)}, u32[]{:S(2)}, u32[]{:S(2)}) collective-permute-start(bf16[144,512]{1,0:T(8,128)(2,1)S(1)} %get-tuple-element.42), channel_id=1, source_target_pairs={{0,8},{8,0},{16,24},{24,16},{1,9},{9,1},{17,25},{25,17},{2,10},{10... | collective-permute-start | bytes 442376 | tf_op jit(solution)/shard_map/ppermute | solution.py:30
  108.4 15.5 %collective-permute-start.4 = (bf16[144,512]{1,0:T(8,128)(2,1)S(1)}, bf16[144,512]{1,0:T(8,128)(2,1)S(1)}, u32[]{:S(2)}, u32[]{:S(2)}) collective-permute-start(bf16[144,512]{1,0:T(8,128)(2,1)S(1)} %get-tuple-element.43), channel_id=1, source_target_pairs={{0,16},{8,24},{16,0},{24,8},{1,17},{9,25},{17,1},{25,9},{2,18},{10... | collective-permute-start | bytes 442376 | tf_op jit(solution)/shard_map/ppermute | solution.py:30
  112.8 11.0 %collective-permute-start.5 = (bf16[144,512]{1,0:T(8,128)(2,1)S(1)}, bf16[144,512]{1,0:T(8,128)(2,1)S(1)}, u32[]{:S(2)}, u32[]{:S(2)}) collective-permute-start(bf16[144,512]{1,0:T(8,128)(2,1)S(1)} %get-tuple-element.44), channel_id=1, source_target_pairs={{0,24},{8,16},{16,8},{24,0},{1,25},{9,17},{17,9},{25,1},{2,26},{10... | collective-permute-start | bytes 442376 | tf_op jit(solution)/shard_map/ppermute | solution.py:30
  143.3 36.1 %all-to-all-start.3 = ((bf16[8,16,512]{2,1,0:T(8,128)(2,1)}), bf16[8,16,512]{2,1,0:T(8,128)(2,1)S(1)}, u32[]{:S(2)}, u32[]{:S(2)}) async-start(bf16[8,16,512]{2,1,0:T(8,128)(2,1)} %live_out.1), calls=%async_computation.3 | async-start | bytes 262144 | tf_op jit(solution)/shard_map/all_to_all | solution.py:47
  180.2 33.0 %all-to-all-start.4 = ((bf16[8,16,512]{2,1,0:T(8,128)(2,1)}), bf16[8,16,512]{2,1,0:T(8,128)(2,1)S(1)}, u32[]{:S(2)}, u32[]{:S(2)}) async-start(bf16[8,16,512]{2,1,0:T(8,128)(2,1)} %broadcast_in_dim.57), calls=%async_computation.4 | async-start | bytes 262144 | tf_op jit(solution)/shard_map/all_to_all | solution.py:22
  231.0 12.8 %all-to-all-start.6 = ((bf16[32,16,128]{2,1,0:T(8,128)(2,1)}), bf16[32,16,128]{2,1,0:T(8,128)(2,1)S(1)}, u32[]{:S(2)}, u32[]{:S(2)}) async-start(bf16[32,16,128]{2,1,0:T(8,128)(2,1)} %bitcast.41), calls=%async_computation.6 | async-start | bytes 262144 | tf_op jit(solution)/shard_map/all_to_all | solution.py:47
  245.2 45.8 %all-to-all-start.7 = ((bf16[8,136,128]{2,1,0:T(8,128)(2,1)}), bf16[8,136,128]{2,1,0:T(8,128)(2,1)S(1)}, u32[]{:S(2)}, u32[]{:S(2)}) async-start(bf16[8,136,128]{2,1,0:T(8,128)(2,1)} %out.1), calls=%async_computation.7 | async-start | bytes 557056 | tf_op jit(solution)/shard_map/all_to_all | solution.py:47
  248.8 18.2 %collective-permute-start.6 = (bf16[8,512]{1,0:T(8,128)(2,1)S(1)}, bf16[8,512]{1,0:T(8,128)(2,1)S(1)}, u32[]{:S(2)}, u32[]{:S(2)}) collective-permute-start(bf16[8,512]{1,0:T(8,128)(2,1)S(1)} %get-tuple-element.98), channel_id=1, source_target_pairs={{0,8},{8,0},{16,24},{24,16},{1,9},{9,1},{17,25},{25,17},{2,10},{10... | collective-permute-start | bytes 24584 | tf_op jit(solution)/shard_map/ppermute | solution.py:30
  251.4 15.6 %collective-permute-start.7 = (bf16[8,512]{1,0:T(8,128)(2,1)S(1)}, bf16[8,512]{1,0:T(8,128)(2,1)S(1)}, u32[]{:S(2)}, u32[]{:S(2)}) collective-permute-start(bf16[8,512]{1,0:T(8,128)(2,1)S(1)} %get-tuple-element.97), channel_id=1, source_target_pairs={{0,16},{8,24},{16,0},{24,8},{1,17},{9,25},{17,1},{25,9},{2,18},{10... | collective-permute-start | bytes 24584 | tf_op jit(solution)/shard_map/ppermute | solution.py:30
  254.4 12.5 %collective-permute-start.8 = (bf16[8,512]{1,0:T(8,128)(2,1)S(1)}, bf16[8,512]{1,0:T(8,128)(2,1)S(1)}, u32[]{:S(2)}, u32[]{:S(2)}) collective-permute-start(bf16[8,512]{1,0:T(8,128)(2,1)S(1)} %get-tuple-element.96), channel_id=1, source_target_pairs={{0,24},{8,16},{16,8},{24,0},{1,25},{9,17},{17,9},{25,1},{2,26},{10... | collective-permute-start | bytes 24584 | tf_op jit(solution)/shard_map/ppermute | solution.py:30

commit v9 on v8

--- a/solution.py
+++ b/solution.py
@@ -6,6 +6,7 @@
 from jax.experimental import pallas as pl
 from jax.experimental.pallas import tpu as pltpu
 from jax.sharding import Mesh, PartitionSpec as P
+
 
 D = 4096
 CHANNELS = 2048
@@ -134,7 +135,7 @@
         sent[:, j] = out
 
 
-def call(kernel, out_shape, name, scratch_shapes=()):
+def call(kernel, out_shape, scratch_shapes=()):
     return pl.pallas_call(
         kernel,
         out_shape=out_shape,
@@ -143,7 +144,6 @@
             flops=200_000_000, bytes_accessed=1 << 20, transcendentals=1 << 14
         ),
         compiler_params=pltpu.CompilerParams(vmem_limit_bytes=16 << 20),
-        name=name,
     )
 
 
@@ -155,7 +155,6 @@
     return call(
         functools.partial(recur_kernel, depth, channels, rows // seqs),
         (jax.ShapeDtypeStruct((near, dp, own // 2, LANES), jnp.bfloat16), final, final),
-        "recur",
         [pltpu.VMEM((rows, 2 * width), jnp.bfloat16)],
     )(arrived, slot_of, *states, *weights, *done)
 
@@ -236,7 +235,7 @@
         pieces[f, width // LANES * own :] = last.astype(jnp.bfloat16)
 
 
-def per_device(
+def program(
     tokens,
     seq_lengths,
     state_re,
@@ -337,7 +336,8 @@
         scaled = w_out[d].astype(jnp.float32) * gain_out[d][:, None]
         return jnp.concatenate([w_in[d].T, scaled.astype(jnp.bfloat16)], axis=0)
 
-    weights_0 = by_place(traded([weights_of(0)] * near))
+    came = traded([weights_of(0)] * near)
+    weights_0 = by_place(came)
     gathered = from_everyone(start, "far")
     picks = (pick_kept, pick_back, pick_own)
     tables = (slot_of, row_of, row_of_half, picks, weights, weights_of(1))
@@ -345,21 +345,21 @@
     slot_of, row_of, row_of_half, picks, weights, own_1 = tables
     pick_kept, pick_back, pick_own = picks
     gathered = gathered.reshape(far * own, width)
-    project = call(functools.partial(in_kernel, channels), pieces_of, "project")
+    project = call(functools.partial(in_kernel, channels), pieces_of)
     pieces = project(gathered, weights_0, gain_in[0:1])
     handed = exact(pick_kept, gathered).reshape(near, block, width)
     parts = [jnp.concatenate([own_1, handed[d]], axis=0) for d in range(near)]
     pieces, parts = lax.optimization_barrier((pieces, parts))
-    arrived, came = lax.optimization_barrier((joined(pieces), traded(parts)))
-    before = sum(c[2 * channels :].astype(jnp.float32) for c in came)
-    weights_1 = by_place([c[: 2 * channels] for c in came])
+    arrived = joined(pieces)
+    came = traded(parts)
     sent, *done = recur(0, channels, arrived, slot_of, states, weights, ())
     pieces = call(
         functools.partial(live_out_kernel, channels, live_own),
         jax.ShapeDtypeStruct((far, block, width), jnp.bfloat16),
-        "live_out",
     )(joined(sent).reshape(near, -1, LANES), weights_0, row_of_half)
-    total = summed(pieces)
+    total, came = lax.optimization_barrier((summed(pieces), came))
+    before = sum(c[2 * channels :].astype(jnp.float32) for c in came)
+    weights_1 = by_place([c[: 2 * channels] for c in came])
     squares = lax.dynamic_slice_in_dim(total[live_own, : far * block], far_here * block, block)
     inv_out = lax.rsqrt(squares / CHANNELS + EPSILON)
     current = (before + total * inv_out[:, None]).astype(jnp.bfloat16)
@@ -373,7 +373,6 @@
     pieces = call(
         functools.partial(out_kernel, channels),
         jax.ShapeDtypeStruct((far, rows_out + 8, LANES), jnp.bfloat16),
-        "out",
     )(joined(sent).reshape(near, -1, LANES), weights_1)
     back = exact(pick_back, gathered).reshape(near, few, width)
     pieces, back = lax.optimization_barrier((pieces, back))
@@ -419,6 +418,7 @@
         P(None, ("grp", "dp"), tp),
         P(None, ("grp", "dp"), tp),
     )
+
     return jax.shard_map(
-        per_device, mesh=split, in_specs=in_specs, out_specs=out_specs, check_vma=False
-    )
+        program, mesh=split, in_specs=in_specs, out_specs=out_specs, check_vma=False
+    )

time: 293 us -> 290 us (0.990)
  blocking collectives: 32 us -> 53.7 us
  waiting for transfers between devices: 125 us -> 105 us
  starting transfers between devices: 108 us -> 104 us
    all_to_all x2 -> x3, blocking collectives: 32 us -> 53.7 us  [exchanged(): return lax.all_to_all(pieces, axis, 0, 0, tiled=True)]
    all_to_all x4 -> x3, starting transfers between devices: 29.3 us -> 15.2 us  [exchanged(): return lax.all_to_all(pieces, axis, 0, 0, tiled=True)]
    all_to_all x2, starting transfers between devices: 44.9 us -> 54.7 us  [from_everyone(): lax.all_to_all(jnp.broadcast_to(shard[None], (peers, *shard.shape)), axis...]
    all_to_all x4 -> x3, waiting for transfers between devices: 61.1 us -> 51.3 us  [exchanged(): return lax.all_to_all(pieces, axis, 0, 0, tiled=True)]
    ppermute x9, waiting for transfers between devices: 16.4 us -> 8.05 us  [traded(): lax.ppermute(parts[d], 'near', [(p, p ^ d) for p in range(peers)])]
  transfers between devices with their start and end apart: 15 -> 14, of which waited for: 8 -> 6; matrix products, arithmetic and copies ran while one was open for 4% -> 4% of each run, Pallas kernels for 0% -> 0%
where the time goes in v9:
time: 290 us; the launch traced here: 289 us
  waiting for transfers between devices  105 us (36%)
  starting transfers between devices  104 us (36%)
  blocking collectives  53.7 us (19%)
  local copies, waits for them, and re-layouts  13.5 us (5%)
  Pallas kernels  6.89 us (2%)
  other arithmetic  3.92 us (1%)
    all_to_all x2, starting transfers between devices, from_everyone(): lax.all_to_all(jnp.broadcast_to(shard[None], (peers, *shard.shape)), axis...  54.7 us
    all_to_all x3, blocking collectives, exchanged(): return lax.all_to_all(pieces, axis, 0, 0, tiled=True)  53.7 us
    all_to_all x3, waiting for transfers between devices, exchanged(): return lax.all_to_all(pieces, axis, 0, 0, tiled=True)  51.3 us
    all_to_all x2, waiting for transfers between devices, from_everyone(): lax.all_to_all(jnp.broadcast_to(shard[None], (peers, *shard.shape)), axis...  46.1 us
    ppermute x9, starting transfers between devices, traded(): lax.ppermute(parts[d], 'near', [(p, p ^ d) for p in range(peers)])  34 us
    all_to_all x3, starting transfers between devices, exchanged(): return lax.all_to_all(pieces, axis, 0, 0, tiled=True)  15.2 us
    ppermute x9, waiting for transfers between devices, traded(): lax.ppermute(parts[d], 'near', [(p, p ^ d) for p in range(peers)])  8.05 us
  transfers between devices with their start and end apart: 14, of which 6 were waited for; matrix products, arithmetic and copies ran while one was open for 4% of the time, Pallas kernels for 0%

profile of v9, /device:TPU:40, one launch (start us, length us, event | category | flops | bytes accessed | tf_op | source)
XLA Modules:
  0.0 289.2 jit_solution(11155155860731552581)
XLA Ops:
  0.6 0.8 slice_bitcast_fusion.5
  1.4 0.9 slice_bitcast_fusion
  2.5 9.1 %collective-permute-start = (bf16[128,512]{1,0:T(8,128)(2,1)S(1)}, bf16[128,512]{1,0:T(8,128)(2,1)S(1)}, u32[]{:S(2)}, u32[]{:S(2)}) collective-permute-start(bf16[128,512]{1,0:T(8,128)(2,1)S(1)} %pad_maximum_fusion.6), channel_id=1, source_target_pairs={{0,24},{8,16},{16,8},{24,0},{1,25},{9,17},{17,9},{25,1},{2,26},{10... | collective-permute-start | bytes 393224 | tf_op jit(solution)/shard_map/ppermute | solution.py:31
  11.6 2.0 collective-permute-start.1
  13.6 2.5 collective-permute-start.2
  16.1 0.7 broadcast_in_dim.47
  16.8 40.7 %all-to-all-start = ((bf16[8,32,512]{2,1,0:T(8,128)(2,1)}), bf16[8,32,512]{2,1,0:T(8,128)(2,1)S(1)}, u32[]{:S(2)}, u32[]{:S(2)}) async-start(bf16[8,32,512]{2,1,0:T(8,128)(2,1)} %broadcast_in_dim.47), calls=%async_computation | async-start | bytes 524288 | tf_op jit(solution)/shard_map/all_to_all | solution.py:23
  65.7 0.7 copy-done.4
  71.1 18.6 %all-to-all-done = bf16[8,32,512]{2,1,0:T(8,128)(2,1)S(1)} async-done(((bf16[8,32,512]{2,1,0:T(8,128)(2,1)}), bf16[8,32,512]{2,1,0:T(8,128)(2,1)S(1)}, u32[]{:S(2)}, u32[]{:S(2)}) %all-to-all-start) | async-done | bytes 262176 | tf_op jit(solution)/shard_map/all_to_all | solution.py:23
  90.4 24.0 %all_to_all.40 = bf16[32,32,128]{2,1,0:T(8,128)(2,1)S(1)} all-to-all(bf16[32,32,128]{2,1,0:T(8,128)(2,1)S(1)} %bitcast.110), channel_id=1, replica_groups=mesh['grp'=2,'far'=8,'near'=4,'dp'=8] {'near','dp'}, dimensions={0} | all-to-all | bytes 524288 | tf_op jit(solution)/shard_map/all_to_all | solution.py:48
  114.3 0.7 shard_map.176
  115.1 12.6 %all_to_all.41 = bf16[32,16,128]{2,1,0:T(8,128)(2,1)S(1)} all-to-all(bf16[32,16,128]{2,1,0:T(8,128)(2,1)S(1)} %bitcast.115), channel_id=1, replica_groups=mesh['grp'=2,'far'=8,'near'=4,'dp'=8] {'near','dp'}, dimensions={0} | all-to-all | bytes 262144 | tf_op jit(solution)/shard_map/all_to_all | solution.py:48
  127.7 2.0 shard_map.177
  129.8 6.8 %all-to-all-start.3 = ((bf16[8,16,512]{2,1,0:T(8,128)(2,1)}), bf16[8,16,512]{2,1,0:T(8,128)(2,1)S(1)}, u32[]{:S(2)}, u32[]{:S(2)}) async-start(bf16[8,16,512]{2,1,0:T(8,128)(2,1)} %shard_map.177), calls=%async_computation.3 | async-start | bytes 262144 | tf_op jit(solution)/shard_map/all_to_all | solution.py:48
  136.6 2.6 collective-permute-start.3
  139.1 3.0 %collective-permute-start.4 = (bf16[144,512]{1,0:T(8,128)(2,1)S(1)}, bf16[144,512]{1,0:T(8,128)(2,1)S(1)}, u32[]{:S(2)}, u32[]{:S(2)}) collective-permute-start(bf16[144,512]{1,0:T(8,128)(2,1)S(1)} %get-tuple-element.50), channel_id=1, source_target_pairs={{0,16},{8,24},{16,0},{24,8},{1,17},{9,25},{17,1},{25,9},{2,18},{10... | collective-permute-start | bytes 442376 | tf_op jit(solution)/shard_map/ppermute | solution.py:31
  142.2 4.6 %collective-permute-start.5 = (bf16[144,512]{1,0:T(8,128)(2,1)S(1)}, bf16[144,512]{1,0:T(8,128)(2,1)S(1)}, u32[]{:S(2)}, u32[]{:S(2)}) collective-permute-start(bf16[144,512]{1,0:T(8,128)(2,1)S(1)} %get-tuple-element.51), channel_id=1, source_target_pairs={{0,24},{8,16},{16,8},{24,0},{1,25},{9,17},{17,9},{25,1},{2,26},{10... | collective-permute-start | bytes 442376 | tf_op jit(solution)/shard_map/ppermute | solution.py:31
  146.8 19.6 %all-to-all-done.3 = bf16[8,16,512]{2,1,0:T(8,128)(2,1)S(1)} async-done(((bf16[8,16,512]{2,1,0:T(8,128)(2,1)}), bf16[8,16,512]{2,1,0:T(8,128)(2,1)S(1)}, u32[]{:S(2)}, u32[]{:S(2)}) %all-to-all-start.3) | async-done | bytes 131104 | tf_op jit(solution)/shard_map/all_to_all | solution.py:48
  167.3 14.0 %all-to-all-start.4 = ((bf16[8,16,512]{2,1,0:T(8,128)(2,1)}), bf16[8,16,512]{2,1,0:T(8,128)(2,1)S(1)}, u32[]{:S(2)}, u32[]{:S(2)}) async-start(bf16[8,16,512]{2,1,0:T(8,128)(2,1)} %broadcast_in_dim.57), calls=%async_computation.4 | async-start | bytes 262144 | tf_op jit(solution)/shard_map/all_to_all | solution.py:23
  181.4 27.5 %all-to-all-done.4 = bf16[8,16,512]{2,1,0:T(8,128)(2,1)S(1)} async-done(((bf16[8,16,512]{2,1,0:T(8,128)(2,1)}), bf16[8,16,512]{2,1,0:T(8,128)(2,1)S(1)}, u32[]{:S(2)}, u32[]{:S(2)}) %all-to-all-start.4) | async-done | bytes 131104 | tf_op jit(solution)/shard_map/all_to_all | solution.py:23
  208.9 1.0 shard_map.178
  209.9 17.1 %all_to_all.42 = bf16[32,32,128]{2,1,0:T(8,128)(2,1)S(1)} all-to-all(bf16[32,32,128]{2,1,0:T(8,128)(2,1)S(1)} %bitcast.112), channel_id=1, replica_groups=mesh['grp'=2,'far'=8,'near'=4,'dp'=8] {'near','dp'}, dimensions={0} | all-to-all | bytes 524288 | tf_op jit(solution)/shard_map/all_to_all | solution.py:48
  227.1 1.4 shard_map.179
  228.5 4.8 %all-to-all-start.6 = ((bf16[32,16,128]{2,1,0:T(8,128)(2,1)}), bf16[32,16,128]{2,1,0:T(8,128)(2,1)S(1)}, u32[]{:S(2)}, u32[]{:S(2)}) async-start(bf16[32,16,128]{2,1,0:T(8,128)(2,1)} %bitcast.41), calls=%async_computation.6 | async-start | bytes 262144 | tf_op jit(solution)/shard_map/all_to_all | solution.py:48
  233.4 7.9 %all-to-all-done.6 = bf16[32,16,128]{2,1,0:T(8,128)(2,1)S(1)} async-done(((bf16[32,16,128]{2,1,0:T(8,128)(2,1)}), bf16[32,16,128]{2,1,0:T(8,128)(2,1)S(1)}, u32[]{:S(2)}, u32[]{:S(2)}) %all-to-all-start.6) | async-done | bytes 131104 | tf_op jit(solution)/shard_map/all_to_all | solution.py:48
  241.3 1.3 shard_map.180
  242.6 3.6 %all-to-all-start.7 = ((bf16[8,136,128]{2,1,0:T(8,128)(2,1)}), bf16[8,136,128]{2,1,0:T(8,128)(2,1)S(1)}, u32[]{:S(2)}, u32[]{:S(2)}) async-start(bf16[8,136,128]{2,1,0:T(8,128)(2,1)} %shard_map.180), calls=%async_computation.7 | async-start | bytes 557056 | tf_op jit(solution)/shard_map/all_to_all | solution.py:48
  246.2 2.6 collective-permute-start.6
  248.8 3.0 %collective-permute-start.7 = (bf16[8,512]{1,0:T(8,128)(2,1)S(1)}, bf16[8,512]{1,0:T(8,128)(2,1)S(1)}, u32[]{:S(2)}, u32[]{:S(2)}) collective-permute-start(bf16[8,512]{1,0:T(8,128)(2,1)S(1)} %get-tuple-element.97), channel_id=1, source_target_pairs={{0,16},{8,24},{16,0},{24,8},{1,17},{9,25},{17,1},{25,9},{2,18},{10... | collective-permute-start | bytes 24584 | tf_op jit(solution)/shard_map/ppermute | solution.py:31
  251.9 4.6 %collective-permute-start.8 = (bf16[8,512]{1,0:T(8,128)(2,1)S(1)}, bf16[8,512]{1,0:T(8,128)(2,1)S(1)}, u32[]{:S(2)}, u32[]{:S(2)}) collective-permute-start(bf16[8,512]{1,0:T(8,128)(2,1)S(1)} %get-tuple-element.96), channel_id=1, source_target_pairs={{0,24},{8,16},{16,8},{24,0},{1,25},{9,17},{17,9},{25,1},{2,26},{10... | collective-permute-start | bytes 24584 | tf_op jit(solution)/shard_map/ppermute | solution.py:31
  256.5 8.0 %collective-permute-done.6 = bf16[8,512]{1,0:T(8,128)(2,1)S(1)} collective-permute-done((bf16[8,512]{1,0:T(8,128)(2,1)S(1)}, bf16[8,512]{1,0:T(8,128)(2,1)S(1)}, u32[]{:S(2)}, u32[]{:S(2)}) %collective-permute-start.6) | collective-permute-done | bytes 8224 | tf_op jit(solution)/shard_map/ppermute | solution.py:31
  264.7 23.8 %all-to-all-done.7 = bf16[8,136,128]{2,1,0:T(8,128)(2,1)S(1)} async-done(((bf16[8,136,128]{2,1,0:T(8,128)(2,1)}), bf16[8,136,128]{2,1,0:T(8,128)(2,1)S(1)}, u32[]{:S(2)}, u32[]{:S(2)}) %all-to-all-start.7) | async-done | bytes 278560 | tf_op jit(solution)/shard_map/all_to_all | solution.py:48
  (158 shorter events, 15.2 us)
Async XLA Ops:
  1.4 1.0 copy-start.2
  2.4 13.7 %copy-start.3 = (bf16[4,8,512]{2,1,0:T(8,128)(2,1)S(1)}, bf16[4,8,512]{2,1,0:T(8,128)(2,1)}, u32[]{:S(2)}) copy-start(bf16[4,8,512]{2,1,0:T(8,128)(2,1)} %param.16) | copy-start | bytes 98308
  2.5 68.3 %collective-permute-start = (bf16[128,512]{1,0:T(8,128)(2,1)S(1)}, bf16[128,512]{1,0:T(8,128)(2,1)S(1)}, u32[]{:S(2)}, u32[]{:S(2)}) collective-permute-start(bf16[128,512]{1,0:T(8,128)(2,1)S(1)} %pad_maximum_fusion.6), channel_id=1, source_target_pairs={{0,24},{8,16},{16,8},{24,0},{1,25},{9,17},{17,9},{25,1},{2,26},{10... | collective-permute-start | bytes 393224 | tf_op jit(solution)/shard_map/ppermute | solution.py:31
  11.6 59.2 %collective-permute-start.1 = (bf16[128,512]{1,0:T(8,128)(2,1)S(1)}, bf16[128,512]{1,0:T(8,128)(2,1)S(1)}, u32[]{:S(2)}, u32[]{:S(2)}) collective-permute-start(bf16[128,512]{1,0:T(8,128)(2,1)S(1)} %pad_maximum_fusion.6), channel_id=1, source_target_pairs={{0,16},{8,24},{16,0},{24,8},{1,17},{9,25},{17,1},{25,9},{2,18},{10... | collective-permute-start | bytes 393224 | tf_op jit(solution)/shard_map/ppermute | solution.py:31
  13.6 57.2 %collective-permute-start.2 = (bf16[128,512]{1,0:T(8,128)(2,1)S(1)}, bf16[128,512]{1,0:T(8,128)(2,1)S(1)}, u32[]{:S(2)}, u32[]{:S(2)}) collective-permute-start(bf16[128,512]{1,0:T(8,128)(2,1)S(1)} %pad_maximum_fusion.6), channel_id=1, source_target_pairs={{0,8},{8,0},{16,24},{24,16},{1,9},{9,1},{17,25},{25,17},{2,10},{10... | collective-permute-start | bytes 393224 | tf_op jit(solution)/shard_map/ppermute | solution.py:31
  16.8 72.8 %all-to-all-start = ((bf16[8,32,512]{2,1,0:T(8,128)(2,1)}), bf16[8,32,512]{2,1,0:T(8,128)(2,1)S(1)}, u32[]{:S(2)}, u32[]{:S(2)}) async-start(bf16[8,32,512]{2,1,0:T(8,128)(2,1)} %broadcast_in_dim.47), calls=%async_computation | async-start | bytes 524288 | tf_op jit(solution)/shard_map/all_to_all | solution.py:23
  57.6 0.7 copy-start.9
  62.2 1.1 copy-start.12
  62.2 1.2 copy-start.8
  62.2 1.3 copy-start.11
  62.2 1.7 copy-start.6
  62.2 1.6 copy-start.5
  65.5 0.8 copy-start.4
  66.4 0.7 copy-start.10
  66.4 2.7 copy-start.7
  70.1 0.7 copy-start.13
  90.4 24.0 %copy-start = (f32[2,16,256]{2,1,0:T(8,128)S(1)}, f32[2,16,256]{2,1,0:T(8,128)}, u32[]{:S(2)}) copy-start(f32[2,16,256]{2,1,0:T(8,128)} %re.3) | copy-start | bytes 98308
  90.4 24.0 %copy-start.1 = (f32[2,16,256]{2,1,0:T(8,128)S(1)}, f32[2,16,256]{2,1,0:T(8,128)}, u32[]{:S(2)}) copy-start(f32[2,16,256]{2,1,0:T(8,128)} %im.3) | copy-start | bytes 98308
  129.8 36.6 %all-to-all-start.3 = ((bf16[8,16,512]{2,1,0:T(8,128)(2,1)}), bf16[8,16,512]{2,1,0:T(8,128)(2,1)S(1)}, u32[]{:S(2)}, u32[]{:S(2)}) async-start(bf16[8,16,512]{2,1,0:T(8,128)(2,1)} %shard_map.177), calls=%async_computation.3 | async-start | bytes 262144 | tf_op jit(solution)/shard_map/all_to_all | solution.py:48
  136.6 29.8 %collective-permute-start.3 = (bf16[144,512]{1,0:T(8,128)(2,1)S(1)}, bf16[144,512]{1,0:T(8,128)(2,1)S(1)}, u32[]{:S(2)}, u32[]{:S(2)}) collective-permute-start(bf16[144,512]{1,0:T(8,128)(2,1)S(1)} %get-tuple-element.49), channel_id=1, source_target_pairs={{0,8},{8,0},{16,24},{24,16},{1,9},{9,1},{17,25},{25,17},{2,10},{10... | collective-permute-start | bytes 442376 | tf_op jit(solution)/shard_map/ppermute | solution.py:31
  139.1 27.3 %collective-permute-start.4 = (bf16[144,512]{1,0:T(8,128)(2,1)S(1)}, bf16[144,512]{1,0:T(8,128)(2,1)S(1)}, u32[]{:S(2)}, u32[]{:S(2)}) collective-permute-start(bf16[144,512]{1,0:T(8,128)(2,1)S(1)} %get-tuple-element.50), channel_id=1, source_target_pairs={{0,16},{8,24},{16,0},{24,8},{1,17},{9,25},{17,1},{25,9},{2,18},{10... | collective-permute-start | bytes 442376 | tf_op jit(solution)/shard_map/ppermute | solution.py:31
  142.2 24.2 %collective-permute-start.5 = (bf16[144,512]{1,0:T(8,128)(2,1)S(1)}, bf16[144,512]{1,0:T(8,128)(2,1)S(1)}, u32[]{:S(2)}, u32[]{:S(2)}) collective-permute-start(bf16[144,512]{1,0:T(8,128)(2,1)S(1)} %get-tuple-element.51), channel_id=1, source_target_pairs={{0,24},{8,16},{16,8},{24,0},{1,25},{9,17},{17,9},{25,1},{2,26},{10... | collective-permute-start | bytes 442376 | tf_op jit(solution)/shard_map/ppermute | solution.py:31
  167.3 41.7 %all-to-all-start.4 = ((bf16[8,16,512]{2,1,0:T(8,128)(2,1)}), bf16[8,16,512]{2,1,0:T(8,128)(2,1)S(1)}, u32[]{:S(2)}, u32[]{:S(2)}) async-start(bf16[8,16,512]{2,1,0:T(8,128)(2,1)} %broadcast_in_dim.57), calls=%async_computation.4 | async-start | bytes 262144 | tf_op jit(solution)/shard_map/all_to_all | solution.py:23
  228.5 12.8 %all-to-all-start.6 = ((bf16[32,16,128]{2,1,0:T(8,128)(2,1)}), bf16[32,16,128]{2,1,0:T(8,128)(2,1)S(1)}, u32[]{:S(2)}, u32[]{:S(2)}) async-start(bf16[32,16,128]{2,1,0:T(8,128)(2,1)} %bitcast.41), calls=%async_computation.6 | async-start | bytes 262144 | tf_op jit(solution)/shard_map/all_to_all | solution.py:48
  242.6 45.9 %all-to-all-start.7 = ((bf16[8,136,128]{2,1,0:T(8,128)(2,1)}), bf16[8,136,128]{2,1,0:T(8,128)(2,1)S(1)}, u32[]{:S(2)}, u32[]{:S(2)}) async-start(bf16[8,136,128]{2,1,0:T(8,128)(2,1)} %shard_map.180), calls=%async_computation.7 | async-start | bytes 557056 | tf_op jit(solution)/shard_map/all_to_all | solution.py:48
  246.2 18.3 %collective-permute-start.6 = (bf16[8,512]{1,0:T(8,128)(2,1)S(1)}, bf16[8,512]{1,0:T(8,128)(2,1)S(1)}, u32[]{:S(2)}, u32[]{:S(2)}) collective-permute-start(bf16[8,512]{1,0:T(8,128)(2,1)S(1)} %get-tuple-element.98), channel_id=1, source_target_pairs={{0,8},{8,0},{16,24},{24,16},{1,9},{9,1},{17,25},{25,17},{2,10},{10... | collective-permute-start | bytes 24584 | tf_op jit(solution)/shard_map/ppermute | solution.py:31
  248.8 15.7 %collective-permute-start.7 = (bf16[8,512]{1,0:T(8,128)(2,1)S(1)}, bf16[8,512]{1,0:T(8,128)(2,1)S(1)}, u32[]{:S(2)}, u32[]{:S(2)}) collective-permute-start(bf16[8,512]{1,0:T(8,128)(2,1)S(1)} %get-tuple-element.97), channel_id=1, source_target_pairs={{0,16},{8,24},{16,0},{24,8},{1,17},{9,25},{17,1},{25,9},{2,18},{10... | collective-permute-start | bytes 24584 | tf_op jit(solution)/shard_map/ppermute | solution.py:31
  251.9 12.7 %collective-permute-start.8 = (bf16[8,512]{1,0:T(8,128)(2,1)S(1)}, bf16[8,512]{1,0:T(8,128)(2,1)S(1)}, u32[]{:S(2)}, u32[]{:S(2)}) collective-permute-start(bf16[8,512]{1,0:T(8,128)(2,1)S(1)} %get-tuple-element.96), channel_id=1, source_target_pairs={{0,24},{8,16},{16,8},{24,0},{1,25},{9,17},{17,9},{25,1},{2,26},{10... | collective-permute-start | bytes 24584 | tf_op jit(solution)/shard_map/ppermute | solution.py:31

commit v10 on v9

--- a/solution.py
+++ b/solution.py
@@ -191,7 +191,7 @@
         pieces[n] = out.reshape(dp, own, LANES)
 
 
-def live_out_kernel(channels, live_own, arrived, both, row_of, pieces):
+def live_out_kernel(live_own, arrived, w_out, row_of, pieces):
     near, slots, _ = arrived.shape
     far, rows, width = pieces.shape
     at = lax.broadcasted_iota(jnp.int32, (far * rows, slots), 0)
@@ -200,7 +200,7 @@
         pick = (at == row_of[half : half + 1]).astype(jnp.float32).astype(jnp.bfloat16)
         for n in range(near):
             live = product(pick, arrived[n], ((1,), (0,))).astype(jnp.bfloat16)
-            partial += product(live, with_zeros(both[n, channels:], half == 1), ((1,), (0,)))
+            partial += product(live, with_zeros(w_out[n], half == 1), ((1,), (0,)))
             squares += squared(live, half)
     squares = jnp.concatenate(
         [squares[:1], jnp.zeros((1, width - far * rows), jnp.float32)], axis=1
@@ -303,69 +303,77 @@
     place_home = place.reshape(far, near, own)
     held = lax.dynamic_slice_in_dim(place_home, here, 1, 1).reshape(-1)
     pick_kept = same(kept, held)
+    in_all_lanes = [(0, 0), (0, LANES - channels)]
+    weights = recurrence_weights(
+        decay_rate, frequency, log_step, in_re, in_im, readout_real, readout_imaginary
+    ) + (jnp.pad(skip_scale, in_all_lanes),)
+    pieces_of = jax.ShapeDtypeStruct((near, dp, own, LANES), jnp.bfloat16)
+
+    def joined(pieces):
+        flat = pieces.reshape(near * dp, -1, LANES)
+        return exchanged(flat, joint).reshape(pieces.shape)
+
+    def summed(pieces):
+        return jnp.sum(exchanged(pieces, "far").astype(jnp.float32), axis=0)
+
+    def weights_of(d):
+        scaled = w_out[d].astype(jnp.float32) * gain_out[d][:, None]
+        return jnp.concatenate([w_in[d].T, scaled.astype(jnp.bfloat16)], axis=0)
+
+    own_0, own_1 = weights_of(0), weights_of(1)
+    came = traded([own_0[:channels]] * near)
+    near_in = by_place(came)
+    gathered = from_everyone(start, "far")
+    tables = (slot_of, row_of, row_of_half, pick_kept, weights, own_0, own_1)
+    gathered, near_in, tables = lax.optimization_barrier((gathered, near_in, tables))
+    slot_of, row_of, row_of_half, pick_kept, weights, own_0, own_1 = tables
+    gathered = gathered.reshape(far * own, width)
+    project = call(functools.partial(in_kernel, channels), pieces_of)
+    pieces = project(gathered, near_in, gain_in[0:1])
+    handed = exact(pick_kept, gathered).reshape(near, block, width)
+    parts = [
+        jnp.concatenate([own_0[channels:], own_1, handed[d]], axis=0) for d in range(near)
+    ]
+    pieces, parts = lax.optimization_barrier((pieces, parts))
+    arrived = joined(pieces)
+    came = traded(parts)
+    sent, *done = recur(0, channels, arrived, slot_of, states, weights, ())
+    near_out = by_place([c[:channels] for c in came])
+    pieces = call(
+        functools.partial(live_out_kernel, live_own),
+        jax.ShapeDtypeStruct((far, block, width), jnp.bfloat16),
+    )(joined(sent).reshape(near, -1, LANES), near_out, row_of_half)
+    total, came = lax.optimization_barrier((summed(pieces), came))
+    before = sum(c[3 * channels :].astype(jnp.float32) for c in came)
+    weights_1 = by_place([c[channels : 3 * channels] for c in came])
+    squares = lax.dynamic_slice_in_dim(total[live_own, : far * block], far_here * block, block)
+    inv_out = lax.rsqrt(squares / CHANNELS + EPSILON)
+    current = (before + total * inv_out[:, None]).astype(jnp.bfloat16)
+    current = jnp.where((int_range(block) < live_own)[:, None], current, 0)
+
+    late_lengths, current = lax.optimization_barrier((seq_lengths, current))
+    late_ends = jnp.cumsum(late_lengths)
+    late_starts = late_ends - late_lengths
     home_starts = lax.dynamic_slice_in_dim(
-        starts[::seq_local].reshape(far, near), far_here, 1, 0
+        late_starts[::seq_local].reshape(far, near), far_here, 1, 0
     ).reshape(-1)
     home_ends = lax.dynamic_slice_in_dim(
-        ends[seq_local - 1 :: seq_local].reshape(far, near), far_here, 1, 0
+        late_ends[seq_local - 1 :: seq_local].reshape(far, near), far_here, 1, 0
     ).reshape(-1)
     number = first_of(home_starts[peer], here)[:, None] + int_range(few)
     back = jnp.where(
         number * near + here < home_ends[peer][:, None], row_of_number(number), -1
     ).reshape(-1)
     pick_back = same(back, int_range(far * block))
-    place_own = lax.dynamic_slice_in_dim(held.reshape(far, own), far_here, 1, 0).reshape(-1)
+    late_place = jnp.where(step < late_lengths[:, None], late_starts[:, None] + step, -1)
+    rank = far_here * near + here
+    place_own = lax.dynamic_slice_in_dim(late_place, rank * seq_local, seq_local, 0).reshape(-1)
     column = place_own % near
     source = (column ^ here) * few + place_own // near
     source = source - first_of(lax.dynamic_slice_in_dim(home_starts, here, 1), column)
     pick_own = same(jnp.where(place_own >= 0, source, -1), int_range(near * few))
-    in_all_lanes = [(0, 0), (0, LANES - channels)]
-    weights = recurrence_weights(
-        decay_rate, frequency, log_step, in_re, in_im, readout_real, readout_imaginary
-    ) + (jnp.pad(skip_scale, in_all_lanes),)
-    pieces_of = jax.ShapeDtypeStruct((near, dp, own, LANES), jnp.bfloat16)
-
-    def joined(pieces):
-        flat = pieces.reshape(near * dp, -1, LANES)
-        return exchanged(flat, joint).reshape(pieces.shape)
-
-    def summed(pieces):
-        return jnp.sum(exchanged(pieces, "far").astype(jnp.float32), axis=0)
-
-    def weights_of(d):
-        scaled = w_out[d].astype(jnp.float32) * gain_out[d][:, None]
-        return jnp.concatenate([w_in[d].T, scaled.astype(jnp.bfloat16)], axis=0)
-
-    came = traded([weights_of(0)] * near)
-    weights_0 = by_place(came)
-    gathered = from_everyone(start, "far")
-    picks = (pick_kept, pick_back, pick_own)
-    tables = (slot_of, row_of, row_of_half, picks, weights, weights_of(1))
-    gathered, weights_0, tables = lax.optimization_barrier((gathered, weights_0, tables))
-    slot_of, row_of, row_of_half, picks, weights, own_1 = tables
-    pick_kept, pick_back, pick_own = picks
-    gathered = gathered.reshape(far * own, width)
-    project = call(functools.partial(in_kernel, channels), pieces_of)
-    pieces = project(gathered, weights_0, gain_in[0:1])
-    handed = exact(pick_kept, gathered).reshape(near, block, width)
-    parts = [jnp.concatenate([own_1, handed[d]], axis=0) for d in range(near)]
-    pieces, parts = lax.optimization_barrier((pieces, parts))
-    arrived = joined(pieces)
-    came = traded(parts)
-    sent, *done = recur(0, channels, arrived, slot_of, states, weights, ())
-    pieces = call(
-        functools.partial(live_out_kernel, channels, live_own),
-        jax.ShapeDtypeStruct((far, block, width), jnp.bfloat16),
-    )(joined(sent).reshape(near, -1, LANES), weights_0, row_of_half)
-    total, came = lax.optimization_barrier((summed(pieces), came))
-    before = sum(c[2 * channels :].astype(jnp.float32) for c in came)
-    weights_1 = by_place([c[: 2 * channels] for c in came])
-    squares = lax.dynamic_slice_in_dim(total[live_own, : far * block], far_here * block, block)
-    inv_out = lax.rsqrt(squares / CHANNELS + EPSILON)
-    current = (before + total * inv_out[:, None]).astype(jnp.bfloat16)
-    current = jnp.where((int_range(block) < live_own)[:, None], current, 0)
-
     gathered = from_everyone(current, "far")
+    gathered, pick_back, pick_own = lax.optimization_barrier((gathered, pick_back, pick_own))
     gathered = gathered.reshape(far * block, width)
     pieces = project(gathered, weights_1, gain_in[1:2], row_of)
     sent, *done = recur(1, channels, joined(pieces), slot_of, states, weights, done)

time: 290 us -> 298 us (1.028)
  waiting for transfers between devices: 105 us -> 125 us
  blocking collectives: 53.7 us -> 42.1 us
  starting transfers between devices: 104 us -> 99.6 us
    ppermute x9, waiting for transfers between devices: 8.05 us -> 22.5 us  [traded(): lax.ppermute(parts[d], 'near', [(p, p ^ d) for p in range(peers)])]
    all_to_all x3 -> x2, blocking collectives: 53.7 us -> 42.1 us  [exchanged(): return lax.all_to_all(pieces, axis, 0, 0, tiled=True)]
    all_to_all x2, starting transfers between devices: 54.7 us -> 46.2 us  [from_everyone(): lax.all_to_all(jnp.broadcast_to(shard[None], (peers, *shard.shape)), axis...]
    all_to_all x3 -> x4, waiting for transfers between devices: 51.3 us -> 59.1 us  [exchanged(): return lax.all_to_all(pieces, axis, 0, 0, tiled=True)]
    all_to_all x3 -> x4, starting transfers between devices: 15.2 us -> 20 us  [exchanged(): return lax.all_to_all(pieces, axis, 0, 0, tiled=True)]
  transfers between devices with their start and end apart: 14 -> 15, of which waited for: 6 -> 9; matrix products, arithmetic and copies ran while one was open for 4% -> 4% of each run, Pallas kernels for 0% -> 0%
where the time goes in v10:
time: 298 us; the launch traced here: 297 us
  waiting for transfers between devices  125 us (42%)
  starting transfers between devices  99.6 us (33%)
  blocking collectives  42.1 us (14%)
  local copies, waits for them, and re-layouts  16 us (5%)
  Pallas kernels  7.52 us (3%)
  other arithmetic  4.34 us (1%)
    all_to_all x4, waiting for transfers between devices, exchanged(): return lax.all_to_all(pieces, axis, 0, 0, tiled=True)  59.1 us
    all_to_all x2, starting transfers between devices, from_everyone(): lax.all_to_all(jnp.broadcast_to(shard[None], (peers, *shard.shape)), axis...  46.2 us
    all_to_all x2, waiting for transfers between devices, from_everyone(): lax.all_to_all(jnp.broadcast_to(shard[None], (peers, *shard.shape)), axis...  43.7 us
    all_to_all x2, blocking collectives, exchanged(): return lax.all_to_all(pieces, axis, 0, 0, tiled=True)  42.1 us
    ppermute x9, starting transfers between devices, traded(): lax.ppermute(parts[d], 'near', [(p, p ^ d) for p in range(peers)])  33.4 us
    ppermute x9, waiting for transfers between devices, traded(): lax.ppermute(parts[d], 'near', [(p, p ^ d) for p in range(peers)])  22.5 us
    all_to_all x4, starting transfers between devices, exchanged(): return lax.all_to_all(pieces, axis, 0, 0, tiled=True)  20 us
  transfers between devices with their start and end apart: 15, of which 9 were waited for; matrix products, arithmetic and copies ran while one was open for 4% of the time, Pallas kernels for 0%

profile of v10, /device:TPU:40, one launch (start us, length us, event | category | flops | bytes accessed | tf_op | source)
XLA Modules:
  0.0 296.8 jit_solution(8429557717791101183)
XLA Ops:
  0.6 0.9 slice_bitcast_fusion
  1.5 9.1 %collective-permute-start = (bf16[64,512]{1,0:T(8,128)(2,1)S(1)}, bf16[64,512]{1,0:T(8,128)(2,1)S(1)}, u32[]{:S(2)}, u32[]{:S(2)}) collective-permute-start(bf16[64,512]{1,0:T(8,128)(2,1)S(1)} %get-tuple-element.96), channel_id=1, source_target_pairs={{0,24},{8,16},{16,8},{24,0},{1,25},{9,17},{17,9},{25,1},{2,26},{10... | collective-permute-start | bytes 196616 | tf_op jit(solution)/shard_map/ppermute | solution.py:31
  10.7 2.0 collective-permute-start.1
  12.6 2.5 collective-permute-start.2
  15.9 40.7 %all-to-all-start = ((bf16[8,32,512]{2,1,0:T(8,128)(2,1)}), bf16[8,32,512]{2,1,0:T(8,128)(2,1)S(1)}, u32[]{:S(2)}, u32[]{:S(2)}) async-start(bf16[8,32,512]{2,1,0:T(8,128)(2,1)} %broadcast_in_dim.49), calls=%async_computation | async-start | bytes 524288 | tf_op jit(solution)/shard_map/all_to_all | solution.py:23
  61.6 0.8 copy-done.9
  69.3 19.3 %all-to-all-done = bf16[8,32,512]{2,1,0:T(8,128)(2,1)S(1)} async-done(((bf16[8,32,512]{2,1,0:T(8,128)(2,1)}), bf16[8,32,512]{2,1,0:T(8,128)(2,1)S(1)}, u32[]{:S(2)}, u32[]{:S(2)}) %all-to-all-start) | async-done | bytes 262176 | tf_op jit(solution)/shard_map/all_to_all | solution.py:23
  89.9 24.0 %all_to_all.40 = bf16[32,32,128]{2,1,0:T(8,128)(2,1)S(1)} all-to-all(bf16[32,32,128]{2,1,0:T(8,128)(2,1)S(1)} %bitcast.120), channel_id=1, replica_groups=mesh['grp'=2,'far'=8,'near'=4,'dp'=8] {'near','dp'}, dimensions={0} | all-to-all | bytes 524288 | tf_op jit(solution)/shard_map/all_to_all | solution.py:48
  113.8 1.4 shard_map.176
  115.2 4.8 %all-to-all-start.2 = ((bf16[32,16,128]{2,1,0:T(8,128)(2,1)}), bf16[32,16,128]{2,1,0:T(8,128)(2,1)S(1)}, u32[]{:S(2)}, u32[]{:S(2)}) async-start(bf16[32,16,128]{2,1,0:T(8,128)(2,1)} %bitcast.27), calls=%async_computation.2 | async-start | bytes 262144 | tf_op jit(solution)/shard_map/all_to_all | solution.py:48
  120.0 4.2 %collective-permute-start.4 = (bf16[208,512]{1,0:T(8,128)(2,1)S(1)}, bf16[208,512]{1,0:T(8,128)(2,1)S(1)}, u32[]{:S(2)}, u32[]{:S(2)}) collective-permute-start(bf16[208,512]{1,0:T(8,128)(2,1)S(1)} %get-tuple-element.53), channel_id=1, source_target_pairs={{0,16},{8,24},{16,0},{24,8},{1,17},{9,25},{17,1},{25,9},{2,18},{10... | collective-permute-start | bytes 638984 | tf_op jit(solution)/shard_map/ppermute | solution.py:31
  124.2 3.4 %collective-permute-start.3 = (bf16[208,512]{1,0:T(8,128)(2,1)S(1)}, bf16[208,512]{1,0:T(8,128)(2,1)S(1)}, u32[]{:S(2)}, u32[]{:S(2)}) collective-permute-start(bf16[208,512]{1,0:T(8,128)(2,1)S(1)} %get-tuple-element.52), channel_id=1, source_target_pairs={{0,24},{8,16},{16,8},{24,0},{1,25},{9,17},{17,9},{25,1},{2,26},{10... | collective-permute-start | bytes 638984 | tf_op jit(solution)/shard_map/ppermute | solution.py:31
  127.6 2.1 collective-permute-start.5
  129.7 10.4 %collective-permute-done.4 = bf16[208,512]{1,0:T(8,128)(2,1)S(1)} collective-permute-done((bf16[208,512]{1,0:T(8,128)(2,1)S(1)}, bf16[208,512]{1,0:T(8,128)(2,1)S(1)}, u32[]{:S(2)}, u32[]{:S(2)}) %collective-permute-start.4) | collective-permute-done | bytes 213024 | tf_op jit(solution)/shard_map/ppermute | solution.py:31
  140.1 4.2 %collective-permute-done.5 = bf16[208,512]{1,0:T(8,128)(2,1)S(1)} collective-permute-done((bf16[208,512]{1,0:T(8,128)(2,1)S(1)}, bf16[208,512]{1,0:T(8,128)(2,1)S(1)}, u32[]{:S(2)}, u32[]{:S(2)}) %collective-permute-start.5) | collective-permute-done | bytes 213024 | tf_op jit(solution)/shard_map/ppermute | solution.py:31
  144.4 2.0 shard_map.177
  146.4 6.8 %all-to-all-start.3 = ((bf16[8,16,512]{2,1,0:T(8,128)(2,1)}), bf16[8,16,512]{2,1,0:T(8,128)(2,1)S(1)}, u32[]{:S(2)}, u32[]{:S(2)}) async-start(bf16[8,16,512]{2,1,0:T(8,128)(2,1)} %shard_map.177), calls=%async_computation.3 | async-start | bytes 262144 | tf_op jit(solution)/shard_map/all_to_all | solution.py:48
  153.2 27.7 %all-to-all-done.3 = bf16[8,16,512]{2,1,0:T(8,128)(2,1)S(1)} async-done(((bf16[8,16,512]{2,1,0:T(8,128)(2,1)}), bf16[8,16,512]{2,1,0:T(8,128)(2,1)S(1)}, u32[]{:S(2)}, u32[]{:S(2)}) %all-to-all-start.3) | async-done | bytes 131104 | tf_op jit(solution)/shard_map/all_to_all | solution.py:48
  182.7 5.4 %all-to-all-start.4 = ((bf16[8,16,512]{2,1,0:T(8,128)(2,1)}), bf16[8,16,512]{2,1,0:T(8,128)(2,1)S(1)}, u32[]{:S(2)}, u32[]{:S(2)}) async-start(bf16[8,16,512]{2,1,0:T(8,128)(2,1)} %broadcast_in_dim.58), calls=%async_computation.4 | async-start | bytes 262144 | tf_op jit(solution)/shard_map/all_to_all | solution.py:23
  191.5 24.4 %all-to-all-done.4 = bf16[8,16,512]{2,1,0:T(8,128)(2,1)S(1)} async-done(((bf16[8,16,512]{2,1,0:T(8,128)(2,1)}), bf16[8,16,512]{2,1,0:T(8,128)(2,1)S(1)}, u32[]{:S(2)}, u32[]{:S(2)}) %all-to-all-start.4) | async-done | bytes 131104 | tf_op jit(solution)/shard_map/all_to_all | solution.py:23
  215.9 1.0 shard_map.178
  216.9 18.2 %all_to_all.41 = bf16[32,32,128]{2,1,0:T(8,128)(2,1)S(1)} all-to-all(bf16[32,32,128]{2,1,0:T(8,128)(2,1)S(1)} %bitcast.123), channel_id=1, replica_groups=mesh['grp'=2,'far'=8,'near'=4,'dp'=8] {'near','dp'}, dimensions={0} | all-to-all | bytes 524288 | tf_op jit(solution)/shard_map/all_to_all | solution.py:48
  235.1 1.4 shard_map.179
  236.5 4.8 %all-to-all-start.6 = ((bf16[32,16,128]{2,1,0:T(8,128)(2,1)}), bf16[32,16,128]{2,1,0:T(8,128)(2,1)S(1)}, u32[]{:S(2)}, u32[]{:S(2)}) async-start(bf16[32,16,128]{2,1,0:T(8,128)(2,1)} %bitcast.46), calls=%async_computation.6 | async-start | bytes 262144 | tf_op jit(solution)/shard_map/all_to_all | solution.py:48
  241.4 7.9 %all-to-all-done.6 = bf16[32,16,128]{2,1,0:T(8,128)(2,1)S(1)} async-done(((bf16[32,16,128]{2,1,0:T(8,128)(2,1)}), bf16[32,16,128]{2,1,0:T(8,128)(2,1)S(1)}, u32[]{:S(2)}, u32[]{:S(2)}) %all-to-all-start.6) | async-done | bytes 131104 | tf_op jit(solution)/shard_map/all_to_all | solution.py:48
  249.4 1.3 shard_map.180
  250.6 3.6 %all-to-all-start.7 = ((bf16[8,136,128]{2,1,0:T(8,128)(2,1)}), bf16[8,136,128]{2,1,0:T(8,128)(2,1)S(1)}, u32[]{:S(2)}, u32[]{:S(2)}) async-start(bf16[8,136,128]{2,1,0:T(8,128)(2,1)} %shard_map.180), calls=%async_computation.7 | async-start | bytes 557056 | tf_op jit(solution)/shard_map/all_to_all | solution.py:48
  254.3 3.1 %collective-permute-start.8 = (bf16[8,512]{1,0:T(8,128)(2,1)S(1)}, bf16[8,512]{1,0:T(8,128)(2,1)S(1)}, u32[]{:S(2)}, u32[]{:S(2)}) collective-permute-start(bf16[8,512]{1,0:T(8,128)(2,1)S(1)} %get-tuple-element.108), channel_id=1, source_target_pairs={{0,24},{8,16},{16,8},{24,0},{1,25},{9,17},{17,9},{25,1},{2,26},{10... | collective-permute-start | bytes 24584 | tf_op jit(solution)/shard_map/ppermute | solution.py:31
  257.4 2.9 collective-permute-start.7
  260.3 4.2 %collective-permute-start.6 = (bf16[8,512]{1,0:T(8,128)(2,1)S(1)}, bf16[8,512]{1,0:T(8,128)(2,1)S(1)}, u32[]{:S(2)}, u32[]{:S(2)}) collective-permute-start(bf16[8,512]{1,0:T(8,128)(2,1)S(1)} %get-tuple-element.110), channel_id=1, source_target_pairs={{0,8},{8,0},{16,24},{24,16},{1,9},{9,1},{17,25},{25,17},{2,10},{10... | collective-permute-start | bytes 24584 | tf_op jit(solution)/shard_map/ppermute | solution.py:31
  265.0 7.4 %collective-permute-done.6 = bf16[8,512]{1,0:T(8,128)(2,1)S(1)} collective-permute-done((bf16[8,512]{1,0:T(8,128)(2,1)S(1)}, bf16[8,512]{1,0:T(8,128)(2,1)S(1)}, u32[]{:S(2)}, u32[]{:S(2)}) %collective-permute-start.6) | collective-permute-done | bytes 8224 | tf_op jit(solution)/shard_map/ppermute | solution.py:31
  272.5 23.5 %all-to-all-done.7 = bf16[8,136,128]{2,1,0:T(8,128)(2,1)S(1)} async-done(((bf16[8,136,128]{2,1,0:T(8,128)(2,1)}), bf16[8,136,128]{2,1,0:T(8,128)(2,1)S(1)}, u32[]{:S(2)}, u32[]{:S(2)}) %all-to-all-start.7) | async-done | bytes 278560 | tf_op jit(solution)/shard_map/all_to_all | solution.py:48
  (178 shorter events, 19.9 us)
Async XLA Ops:
  0.6 14.5 %copy-start.5 = (bf16[4,8,512]{2,1,0:T(8,128)(2,1)S(1)}, bf16[4,8,512]{2,1,0:T(8,128)(2,1)}, u32[]{:S(2)}) copy-start(bf16[4,8,512]{2,1,0:T(8,128)(2,1)} %param.16) | copy-start | bytes 98308
  1.5 67.7 %collective-permute-start = (bf16[64,512]{1,0:T(8,128)(2,1)S(1)}, bf16[64,512]{1,0:T(8,128)(2,1)S(1)}, u32[]{:S(2)}, u32[]{:S(2)}) collective-permute-start(bf16[64,512]{1,0:T(8,128)(2,1)S(1)} %get-tuple-element.96), channel_id=1, source_target_pairs={{0,24},{8,16},{16,8},{24,0},{1,25},{9,17},{17,9},{25,1},{2,26},{10... | collective-permute-start | bytes 196616 | tf_op jit(solution)/shard_map/ppermute | solution.py:31
  10.7 58.5 %collective-permute-start.1 = (bf16[64,512]{1,0:T(8,128)(2,1)S(1)}, bf16[64,512]{1,0:T(8,128)(2,1)S(1)}, u32[]{:S(2)}, u32[]{:S(2)}) collective-permute-start(bf16[64,512]{1,0:T(8,128)(2,1)S(1)} %get-tuple-element.96), channel_id=1, source_target_pairs={{0,16},{8,24},{16,0},{24,8},{1,17},{9,25},{17,1},{25,9},{2,18},{10... | collective-permute-start | bytes 196616 | tf_op jit(solution)/shard_map/ppermute | solution.py:31
  12.6 56.6 %collective-permute-start.2 = (bf16[64,512]{1,0:T(8,128)(2,1)S(1)}, bf16[64,512]{1,0:T(8,128)(2,1)S(1)}, u32[]{:S(2)}, u32[]{:S(2)}) collective-permute-start(bf16[64,512]{1,0:T(8,128)(2,1)S(1)} %get-tuple-element.96), channel_id=1, source_target_pairs={{0,8},{8,0},{16,24},{24,16},{1,9},{9,1},{17,25},{25,17},{2,10},{10... | collective-permute-start | bytes 196616 | tf_op jit(solution)/shard_map/ppermute | solution.py:31
  15.9 72.8 %all-to-all-start = ((bf16[8,32,512]{2,1,0:T(8,128)(2,1)}), bf16[8,32,512]{2,1,0:T(8,128)(2,1)S(1)}, u32[]{:S(2)}, u32[]{:S(2)}) async-start(bf16[8,32,512]{2,1,0:T(8,128)(2,1)} %broadcast_in_dim.49), calls=%async_computation | async-start | bytes 524288 | tf_op jit(solution)/shard_map/all_to_all | solution.py:23
  58.7 0.7 copy-start.14
  58.7 0.8 copy-start.10
  58.7 0.9 copy-start.13
  58.8 1.2 copy-start.7
  58.8 1.2 copy-start.8
  60.8 0.8 copy-start.6
  61.6 0.8 copy-start.9
  63.4 0.7 copy-start.15
  64.2 0.9 copy-start.4
  66.9 0.7 copy-start.16
  67.6 21.3 %copy-start.2 = (bf16[128,512]{1,0:T(8,128)(2,1)}, bf16[128,512]{1,0:T(8,128)(2,1)S(1)}, u32[]{:S(2)}) copy-start(bf16[128,512]{1,0:T(8,128)(2,1)S(1)} %pad_maximum_fusion.8) | copy-start | bytes 393220
  67.6 1.6 copy-start.3
  68.4 0.7 copy-start.12
  88.9 0.8 slice-start
  89.8 24.0 %copy-start = (f32[2,16,256]{2,1,0:T(8,128)S(1)}, f32[2,16,256]{2,1,0:T(8,128)}, u32[]{:S(2)}) copy-start(f32[2,16,256]{2,1,0:T(8,128)} %re.3) | copy-start | bytes 98308
  89.9 24.0 %copy-start.1 = (f32[2,16,256]{2,1,0:T(8,128)S(1)}, f32[2,16,256]{2,1,0:T(8,128)}, u32[]{:S(2)}) copy-start(f32[2,16,256]{2,1,0:T(8,128)} %im.3) | copy-start | bytes 98308
  115.2 29.1 %all-to-all-start.2 = ((bf16[32,16,128]{2,1,0:T(8,128)(2,1)}), bf16[32,16,128]{2,1,0:T(8,128)(2,1)S(1)}, u32[]{:S(2)}, u32[]{:S(2)}) async-start(bf16[32,16,128]{2,1,0:T(8,128)(2,1)} %bitcast.27), calls=%async_computation.2 | async-start | bytes 262144 | tf_op jit(solution)/shard_map/all_to_all | solution.py:48
  120.0 20.0 %collective-permute-start.4 = (bf16[208,512]{1,0:T(8,128)(2,1)S(1)}, bf16[208,512]{1,0:T(8,128)(2,1)S(1)}, u32[]{:S(2)}, u32[]{:S(2)}) collective-permute-start(bf16[208,512]{1,0:T(8,128)(2,1)S(1)} %get-tuple-element.53), channel_id=1, source_target_pairs={{0,16},{8,24},{16,0},{24,8},{1,17},{9,25},{17,1},{25,9},{2,18},{10... | collective-permute-start | bytes 638984 | tf_op jit(solution)/shard_map/ppermute | solution.py:31
  124.2 15.9 %collective-permute-start.3 = (bf16[208,512]{1,0:T(8,128)(2,1)S(1)}, bf16[208,512]{1,0:T(8,128)(2,1)S(1)}, u32[]{:S(2)}, u32[]{:S(2)}) collective-permute-start(bf16[208,512]{1,0:T(8,128)(2,1)S(1)} %get-tuple-element.52), channel_id=1, source_target_pairs={{0,24},{8,16},{16,8},{24,0},{1,25},{9,17},{17,9},{25,1},{2,26},{10... | collective-permute-start | bytes 638984 | tf_op jit(solution)/shard_map/ppermute | solution.py:31
  127.6 16.7 %collective-permute-start.5 = (bf16[208,512]{1,0:T(8,128)(2,1)S(1)}, bf16[208,512]{1,0:T(8,128)(2,1)S(1)}, u32[]{:S(2)}, u32[]{:S(2)}) collective-permute-start(bf16[208,512]{1,0:T(8,128)(2,1)S(1)} %get-tuple-element.54), channel_id=1, source_target_pairs={{0,8},{8,0},{16,24},{24,16},{1,9},{9,1},{17,25},{25,17},{2,10},{10... | collective-permute-start | bytes 638984 | tf_op jit(solution)/shard_map/ppermute | solution.py:31
  146.4 34.6 %all-to-all-start.3 = ((bf16[8,16,512]{2,1,0:T(8,128)(2,1)}), bf16[8,16,512]{2,1,0:T(8,128)(2,1)S(1)}, u32[]{:S(2)}, u32[]{:S(2)}) async-start(bf16[8,16,512]{2,1,0:T(8,128)(2,1)} %shard_map.177), calls=%async_computation.3 | async-start | bytes 262144 | tf_op jit(solution)/shard_map/all_to_all | solution.py:48
  182.7 33.3 %all-to-all-start.4 = ((bf16[8,16,512]{2,1,0:T(8,128)(2,1)}), bf16[8,16,512]{2,1,0:T(8,128)(2,1)S(1)}, u32[]{:S(2)}, u32[]{:S(2)}) async-start(bf16[8,16,512]{2,1,0:T(8,128)(2,1)} %broadcast_in_dim.58), calls=%async_computation.4 | async-start | bytes 262144 | tf_op jit(solution)/shard_map/all_to_all | solution.py:23
  236.5 12.8 %all-to-all-start.6 = ((bf16[32,16,128]{2,1,0:T(8,128)(2,1)}), bf16[32,16,128]{2,1,0:T(8,128)(2,1)S(1)}, u32[]{:S(2)}, u32[]{:S(2)}) async-start(bf16[32,16,128]{2,1,0:T(8,128)(2,1)} %bitcast.46), calls=%async_computation.6 | async-start | bytes 262144 | tf_op jit(solution)/shard_map/all_to_all | solution.py:48
  250.6 45.4 %all-to-all-start.7 = ((bf16[8,136,128]{2,1,0:T(8,128)(2,1)}), bf16[8,136,128]{2,1,0:T(8,128)(2,1)S(1)}, u32[]{:S(2)}, u32[]{:S(2)}) async-start(bf16[8,136,128]{2,1,0:T(8,128)(2,1)} %shard_map.180), calls=%async_computation.7 | async-start | bytes 557056 | tf_op jit(solution)/shard_map/all_to_all | solution.py:48
  254.3 10.2 %collective-permute-start.8 = (bf16[8,512]{1,0:T(8,128)(2,1)S(1)}, bf16[8,512]{1,0:T(8,128)(2,1)S(1)}, u32[]{:S(2)}, u32[]{:S(2)}) collective-permute-start(bf16[8,512]{1,0:T(8,128)(2,1)S(1)} %get-tuple-element.108), channel_id=1, source_target_pairs={{0,24},{8,16},{16,8},{24,0},{1,25},{9,17},{17,9},{25,1},{2,26},{10... | collective-permute-start | bytes 24584 | tf_op jit(solution)/shard_map/ppermute | solution.py:31
  257.4 7.6 %collective-permute-start.7 = (bf16[8,512]{1,0:T(8,128)(2,1)S(1)}, bf16[8,512]{1,0:T(8,128)(2,1)S(1)}, u32[]{:S(2)}, u32[]{:S(2)}) collective-permute-start(bf16[8,512]{1,0:T(8,128)(2,1)S(1)} %get-tuple-element.109), channel_id=1, source_target_pairs={{0,16},{8,24},{16,0},{24,8},{1,17},{9,25},{17,1},{25,9},{2,18},{10... | collective-permute-start | bytes 24584 | tf_op jit(solution)/shard_map/ppermute | solution.py:31
  260.3 12.1 %collective-permute-start.6 = (bf16[8,512]{1,0:T(8,128)(2,1)S(1)}, bf16[8,512]{1,0:T(8,128)(2,1)S(1)}, u32[]{:S(2)}, u32[]{:S(2)}) collective-permute-start(bf16[8,512]{1,0:T(8,128)(2,1)S(1)} %get-tuple-element.110), channel_id=1, source_target_pairs={{0,8},{8,0},{16,24},{24,16},{1,9},{9,1},{17,25},{25,17},{2,10},{10... | collective-permute-start | bytes 24584 | tf_op jit(solution)/shard_map/ppermute | solution.py:31
  (1 other events, 0.7 us)

commit v11 on v9

--- a/solution.py
+++ b/solution.py
@@ -369,17 +369,18 @@
     gathered = gathered.reshape(far * block, width)
     pieces = project(gathered, weights_1, gain_in[1:2], row_of)
     sent, *done = recur(1, channels, joined(pieces), slot_of, states, weights, done)
+    back = exact(pick_back, gathered).reshape(near, few, width)
+    sent, back = lax.optimization_barrier((sent, back))
     rows_out = width // LANES * own
+    arrived = joined(sent).reshape(near, -1, LANES)
+    back = traded([back[d] for d in range(near)])
     pieces = call(
         functools.partial(out_kernel, channels),
         jax.ShapeDtypeStruct((far, rows_out + 8, LANES), jnp.bfloat16),
-    )(joined(sent).reshape(near, -1, LANES), weights_1)
-    back = exact(pick_back, gathered).reshape(near, few, width)
-    pieces, back = lax.optimization_barrier((pieces, back))
-    total = summed(pieces)
-    back = jnp.stack(traded([back[d] for d in range(near)])).reshape(near * few, width)
+    )(arrived, weights_1)
+    total, back = lax.optimization_barrier((summed(pieces), back))
+    back = jnp.stack(back).reshape(near * few, width)
     after = jnp.dot(pick_own, back, preferred_element_type=jnp.float32)
-    total, after = lax.optimization_barrier((total, after))
     mixed = jnp.concatenate(
         [total[i * own : (i + 1) * own] for i in range(width // LANES)], axis=-1
     )

time: 290 us -> 291 us (level)
  blocking collectives: 53.7 us -> 49.2 us
  waiting for transfers between devices: 105 us -> 108 us
    all_to_all x3, waiting for transfers between devices: 51.3 us -> 61.6 us  [exchanged(): return lax.all_to_all(pieces, axis, 0, 0, tiled=True)]
    ppermute x9, waiting for transfers between devices: 8.05 us -> 0.02 us  [traded(): lax.ppermute(parts[d], 'near', [(p, p ^ d) for p in range(peers)])]
    all_to_all x3, blocking collectives: 53.7 us -> 49.2 us  [exchanged(): return lax.all_to_all(pieces, axis, 0, 0, tiled=True)]
  transfers between devices with their start and end apart: 14 -> 14, of which waited for: 6 -> 5; matrix products, arithmetic and copies ran while one was open for 4% -> 4% of each run, Pallas kernels for 0% -> 0%
where the time goes in v11:
time: 291 us; the launch traced here: 290 us
  waiting for transfers between devices  108 us (37%)
  starting transfers between devices  106 us (36%)
  blocking collectives  49.2 us (17%)
  local copies, waits for them, and re-layouts  13.5 us (5%)
  Pallas kernels  7.35 us (3%)
  other arithmetic  3.22 us (1%)
    all_to_all x3, waiting for transfers between devices, exchanged(): return lax.all_to_all(pieces, axis, 0, 0, tiled=True)  61.6 us
    all_to_all x2, starting transfers between devices, from_everyone(): lax.all_to_all(jnp.broadcast_to(shard[None], (peers, *shard.shape)), axis...  54.7 us
    all_to_all x3, blocking collectives, exchanged(): return lax.all_to_all(pieces, axis, 0, 0, tiled=True)  49.2 us
    all_to_all x2, waiting for transfers between devices, from_everyone(): lax.all_to_all(jnp.broadcast_to(shard[None], (peers, *shard.shape)), axis...  46.1 us
    ppermute x9, starting transfers between devices, traded(): lax.ppermute(parts[d], 'near', [(p, p ^ d) for p in range(peers)])  34 us
    all_to_all x3, starting transfers between devices, exchanged(): return lax.all_to_all(pieces, axis, 0, 0, tiled=True)  17.6 us
  transfers between devices with their start and end apart: 14, of which 5 were waited for; matrix products, arithmetic and copies ran while one was open for 4% of the time, Pallas kernels for 0%

profile of v11, /device:TPU:40, one launch (start us, length us, event | category | flops | bytes accessed | tf_op | source)
XLA Modules:
  0.0 289.7 jit_solution(8308120464150924569)
XLA Ops:
  0.6 0.8 slice_bitcast_fusion.6
  1.4 0.9 slice_bitcast_fusion
  2.5 9.1 %collective-permute-start = (bf16[128,512]{1,0:T(8,128)(2,1)S(1)}, bf16[128,512]{1,0:T(8,128)(2,1)S(1)}, u32[]{:S(2)}, u32[]{:S(2)}) collective-permute-start(bf16[128,512]{1,0:T(8,128)(2,1)S(1)} %pad_maximum_fusion.6), channel_id=1, source_target_pairs={{0,24},{8,16},{16,8},{24,0},{1,25},{9,17},{17,9},{25,1},{2,26},{10... | collective-permute-start | bytes 393224 | tf_op jit(solution)/shard_map/ppermute | solution.py:31
  11.6 2.0 collective-permute-start.1
  13.6 2.5 collective-permute-start.2
  16.1 0.7 broadcast_in_dim.46
  16.8 40.7 %all-to-all-start = ((bf16[8,32,512]{2,1,0:T(8,128)(2,1)}), bf16[8,32,512]{2,1,0:T(8,128)(2,1)S(1)}, u32[]{:S(2)}, u32[]{:S(2)}) async-start(bf16[8,32,512]{2,1,0:T(8,128)(2,1)} %broadcast_in_dim.46), calls=%async_computation | async-start | bytes 524288 | tf_op jit(solution)/shard_map/all_to_all | solution.py:23
  65.7 0.7 copy-done.3
  71.1 18.6 %all-to-all-done = bf16[8,32,512]{2,1,0:T(8,128)(2,1)S(1)} async-done(((bf16[8,32,512]{2,1,0:T(8,128)(2,1)}), bf16[8,32,512]{2,1,0:T(8,128)(2,1)S(1)}, u32[]{:S(2)}, u32[]{:S(2)}) %all-to-all-start) | async-done | bytes 262176 | tf_op jit(solution)/shard_map/all_to_all | solution.py:23
  90.4 24.0 %all_to_all.40 = bf16[32,32,128]{2,1,0:T(8,128)(2,1)S(1)} all-to-all(bf16[32,32,128]{2,1,0:T(8,128)(2,1)S(1)} %bitcast.113), channel_id=1, replica_groups=mesh['grp'=2,'far'=8,'near'=4,'dp'=8] {'near','dp'}, dimensions={0} | all-to-all | bytes 524288 | tf_op jit(solution)/shard_map/all_to_all | solution.py:48
  114.3 0.7 shard_map.176
  115.1 12.6 %all_to_all.41 = bf16[32,16,128]{2,1,0:T(8,128)(2,1)S(1)} all-to-all(bf16[32,16,128]{2,1,0:T(8,128)(2,1)S(1)} %bitcast.118), channel_id=1, replica_groups=mesh['grp'=2,'far'=8,'near'=4,'dp'=8] {'near','dp'}, dimensions={0} | all-to-all | bytes 262144 | tf_op jit(solution)/shard_map/all_to_all | solution.py:48
  127.7 2.0 shard_map.177
  129.8 6.8 %all-to-all-start.3 = ((bf16[8,16,512]{2,1,0:T(8,128)(2,1)}), bf16[8,16,512]{2,1,0:T(8,128)(2,1)S(1)}, u32[]{:S(2)}, u32[]{:S(2)}) async-start(bf16[8,16,512]{2,1,0:T(8,128)(2,1)} %shard_map.177), calls=%async_computation.3 | async-start | bytes 262144 | tf_op jit(solution)/shard_map/all_to_all | solution.py:48
  136.6 2.6 collective-permute-start.3
  139.1 3.0 %collective-permute-start.4 = (bf16[144,512]{1,0:T(8,128)(2,1)S(1)}, bf16[144,512]{1,0:T(8,128)(2,1)S(1)}, u32[]{:S(2)}, u32[]{:S(2)}) collective-permute-start(bf16[144,512]{1,0:T(8,128)(2,1)S(1)} %get-tuple-element.54), channel_id=1, source_target_pairs={{0,16},{8,24},{16,0},{24,8},{1,17},{9,25},{17,1},{25,9},{2,18},{10... | collective-permute-start | bytes 442376 | tf_op jit(solution)/shard_map/ppermute | solution.py:31
  142.2 4.6 %collective-permute-start.5 = (bf16[144,512]{1,0:T(8,128)(2,1)S(1)}, bf16[144,512]{1,0:T(8,128)(2,1)S(1)}, u32[]{:S(2)}, u32[]{:S(2)}) collective-permute-start(bf16[144,512]{1,0:T(8,128)(2,1)S(1)} %get-tuple-element.55), channel_id=1, source_target_pairs={{0,24},{8,16},{16,8},{24,0},{1,25},{9,17},{17,9},{25,1},{2,26},{10... | collective-permute-start | bytes 442376 | tf_op jit(solution)/shard_map/ppermute | solution.py:31
  146.8 19.6 %all-to-all-done.3 = bf16[8,16,512]{2,1,0:T(8,128)(2,1)S(1)} async-done(((bf16[8,16,512]{2,1,0:T(8,128)(2,1)}), bf16[8,16,512]{2,1,0:T(8,128)(2,1)S(1)}, u32[]{:S(2)}, u32[]{:S(2)}) %all-to-all-start.3) | async-done | bytes 131104 | tf_op jit(solution)/shard_map/all_to_all | solution.py:48
  167.3 14.0 %all-to-all-start.4 = ((bf16[8,16,512]{2,1,0:T(8,128)(2,1)}), bf16[8,16,512]{2,1,0:T(8,128)(2,1)S(1)}, u32[]{:S(2)}, u32[]{:S(2)}) async-start(bf16[8,16,512]{2,1,0:T(8,128)(2,1)} %broadcast_in_dim.57), calls=%async_computation.4 | async-start | bytes 262144 | tf_op jit(solution)/shard_map/all_to_all | solution.py:23
  181.4 27.5 %all-to-all-done.4 = bf16[8,16,512]{2,1,0:T(8,128)(2,1)S(1)} async-done(((bf16[8,16,512]{2,1,0:T(8,128)(2,1)}), bf16[8,16,512]{2,1,0:T(8,128)(2,1)S(1)}, u32[]{:S(2)}, u32[]{:S(2)}) %all-to-all-start.4) | async-done | bytes 131104 | tf_op jit(solution)/shard_map/all_to_all | solution.py:23
  208.9 1.7 shard_map.178
  210.6 7.2 %all-to-all-start.5 = ((bf16[32,32,128]{2,1,0:T(8,128)(2,1)}), bf16[32,32,128]{2,1,0:T(8,128)(2,1)S(1)}, u32[]{:S(2)}, u32[]{:S(2)}) async-start(bf16[32,32,128]{2,1,0:T(8,128)(2,1)} %bitcast.39), calls=%async_computation.5 | async-start | bytes 524288 | tf_op jit(solution)/shard_map/all_to_all | solution.py:48
  217.9 10.0 %all-to-all-done.5 = bf16[32,32,128]{2,1,0:T(8,128)(2,1)S(1)} async-done(((bf16[32,32,128]{2,1,0:T(8,128)(2,1)}), bf16[32,32,128]{2,1,0:T(8,128)(2,1)S(1)}, u32[]{:S(2)}, u32[]{:S(2)}) %all-to-all-start.5) | async-done | bytes 262176 | tf_op jit(solution)/shard_map/all_to_all | solution.py:48
  227.9 1.2 shard_map.179
  229.1 12.6 %all_to_all.42 = bf16[32,16,128]{2,1,0:T(8,128)(2,1)S(1)} all-to-all(bf16[32,16,128]{2,1,0:T(8,128)(2,1)S(1)} %bitcast.117), channel_id=1, replica_groups=mesh['grp'=2,'far'=8,'near'=4,'dp'=8] {'near','dp'}, dimensions={0} | all-to-all | bytes 262144 | tf_op jit(solution)/shard_map/all_to_all | solution.py:48
  241.7 1.3 shard_map.180
  243.0 3.6 %all-to-all-start.7 = ((bf16[8,136,128]{2,1,0:T(8,128)(2,1)}), bf16[8,136,128]{2,1,0:T(8,128)(2,1)S(1)}, u32[]{:S(2)}, u32[]{:S(2)}) async-start(bf16[8,136,128]{2,1,0:T(8,128)(2,1)} %shard_map.180), calls=%async_computation.7 | async-start | bytes 557056 | tf_op jit(solution)/shard_map/all_to_all | solution.py:48
  246.7 2.6 collective-permute-start.6
  249.2 3.0 %collective-permute-start.7 = (bf16[8,512]{1,0:T(8,128)(2,1)S(1)}, bf16[8,512]{1,0:T(8,128)(2,1)S(1)}, u32[]{:S(2)}, u32[]{:S(2)}) collective-permute-start(bf16[8,512]{1,0:T(8,128)(2,1)S(1)} %get-tuple-element.102), channel_id=1, source_target_pairs={{0,16},{8,24},{16,0},{24,8},{1,17},{9,25},{17,1},{25,9},{2,18},{10... | collective-permute-start | bytes 24584 | tf_op jit(solution)/shard_map/ppermute | solution.py:31
  252.3 4.6 %collective-permute-start.8 = (bf16[8,512]{1,0:T(8,128)(2,1)S(1)}, bf16[8,512]{1,0:T(8,128)(2,1)S(1)}, u32[]{:S(2)}, u32[]{:S(2)}) collective-permute-start(bf16[8,512]{1,0:T(8,128)(2,1)S(1)} %get-tuple-element.101), channel_id=1, source_target_pairs={{0,24},{8,16},{16,8},{24,0},{1,25},{9,17},{17,9},{25,1},{2,26},{10... | collective-permute-start | bytes 24584 | tf_op jit(solution)/shard_map/ppermute | solution.py:31
  256.9 32.0 %all-to-all-done.7 = bf16[8,136,128]{2,1,0:T(8,128)(2,1)S(1)} async-done(((bf16[8,136,128]{2,1,0:T(8,128)(2,1)}), bf16[8,136,128]{2,1,0:T(8,128)(2,1)S(1)}, u32[]{:S(2)}, u32[]{:S(2)}) %all-to-all-start.7) | async-done | bytes 278560 | tf_op jit(solution)/shard_map/all_to_all | solution.py:48
  289.0 0.8 fusion.3
  (157 shorter events, 14.4 us)
Async XLA Ops:
  1.4 1.0 copy-start.2
  2.4 13.7 %copy-start.7 = (bf16[4,8,512]{2,1,0:T(8,128)(2,1)S(1)}, bf16[4,8,512]{2,1,0:T(8,128)(2,1)}, u32[]{:S(2)}) copy-start(bf16[4,8,512]{2,1,0:T(8,128)(2,1)} %param.16) | copy-start | bytes 98308
  2.5 68.3 %collective-permute-start = (bf16[128,512]{1,0:T(8,128)(2,1)S(1)}, bf16[128,512]{1,0:T(8,128)(2,1)S(1)}, u32[]{:S(2)}, u32[]{:S(2)}) collective-permute-start(bf16[128,512]{1,0:T(8,128)(2,1)S(1)} %pad_maximum_fusion.6), channel_id=1, source_target_pairs={{0,24},{8,16},{16,8},{24,0},{1,25},{9,17},{17,9},{25,1},{2,26},{10... | collective-permute-start | bytes 393224 | tf_op jit(solution)/shard_map/ppermute | solution.py:31
  11.6 59.2 %collective-permute-start.1 = (bf16[128,512]{1,0:T(8,128)(2,1)S(1)}, bf16[128,512]{1,0:T(8,128)(2,1)S(1)}, u32[]{:S(2)}, u32[]{:S(2)}) collective-permute-start(bf16[128,512]{1,0:T(8,128)(2,1)S(1)} %pad_maximum_fusion.6), channel_id=1, source_target_pairs={{0,16},{8,24},{16,0},{24,8},{1,17},{9,25},{17,1},{25,9},{2,18},{10... | collective-permute-start | bytes 393224 | tf_op jit(solution)/shard_map/ppermute | solution.py:31
  13.6 57.2 %collective-permute-start.2 = (bf16[128,512]{1,0:T(8,128)(2,1)S(1)}, bf16[128,512]{1,0:T(8,128)(2,1)S(1)}, u32[]{:S(2)}, u32[]{:S(2)}) collective-permute-start(bf16[128,512]{1,0:T(8,128)(2,1)S(1)} %pad_maximum_fusion.6), channel_id=1, source_target_pairs={{0,8},{8,0},{16,24},{24,16},{1,9},{9,1},{17,25},{25,17},{2,10},{10... | collective-permute-start | bytes 393224 | tf_op jit(solution)/shard_map/ppermute | solution.py:31
  16.8 72.8 %all-to-all-start = ((bf16[8,32,512]{2,1,0:T(8,128)(2,1)}), bf16[8,32,512]{2,1,0:T(8,128)(2,1)S(1)}, u32[]{:S(2)}, u32[]{:S(2)}) async-start(bf16[8,32,512]{2,1,0:T(8,128)(2,1)} %broadcast_in_dim.46), calls=%async_computation | async-start | bytes 524288 | tf_op jit(solution)/shard_map/all_to_all | solution.py:23
  57.6 0.7 copy-start.9
  62.2 1.1 copy-start.12
  62.2 1.2 copy-start.8
  62.2 1.3 copy-start.11
  62.2 1.7 copy-start.5
  62.2 1.6 copy-start.4
  65.5 0.8 copy-start.3
  66.4 0.7 copy-start.10
  66.4 2.7 copy-start.6
  70.1 0.7 copy-start.13
  90.4 24.0 %copy-start = (f32[2,16,256]{2,1,0:T(8,128)S(1)}, f32[2,16,256]{2,1,0:T(8,128)}, u32[]{:S(2)}) copy-start(f32[2,16,256]{2,1,0:T(8,128)} %re.3) | copy-start | bytes 98308
  90.4 24.0 %copy-start.1 = (f32[2,16,256]{2,1,0:T(8,128)S(1)}, f32[2,16,256]{2,1,0:T(8,128)}, u32[]{:S(2)}) copy-start(f32[2,16,256]{2,1,0:T(8,128)} %im.3) | copy-start | bytes 98308
  129.8 36.6 %all-to-all-start.3 = ((bf16[8,16,512]{2,1,0:T(8,128)(2,1)}), bf16[8,16,512]{2,1,0:T(8,128)(2,1)S(1)}, u32[]{:S(2)}, u32[]{:S(2)}) async-start(bf16[8,16,512]{2,1,0:T(8,128)(2,1)} %shard_map.177), calls=%async_computation.3 | async-start | bytes 262144 | tf_op jit(solution)/shard_map/all_to_all | solution.py:48
  136.6 29.8 %collective-permute-start.3 = (bf16[144,512]{1,0:T(8,128)(2,1)S(1)}, bf16[144,512]{1,0:T(8,128)(2,1)S(1)}, u32[]{:S(2)}, u32[]{:S(2)}) collective-permute-start(bf16[144,512]{1,0:T(8,128)(2,1)S(1)} %get-tuple-element.53), channel_id=1, source_target_pairs={{0,8},{8,0},{16,24},{24,16},{1,9},{9,1},{17,25},{25,17},{2,10},{10... | collective-permute-start | bytes 442376 | tf_op jit(solution)/shard_map/ppermute | solution.py:31
  139.1 27.3 %collective-permute-start.4 = (bf16[144,512]{1,0:T(8,128)(2,1)S(1)}, bf16[144,512]{1,0:T(8,128)(2,1)S(1)}, u32[]{:S(2)}, u32[]{:S(2)}) collective-permute-start(bf16[144,512]{1,0:T(8,128)(2,1)S(1)} %get-tuple-element.54), channel_id=1, source_target_pairs={{0,16},{8,24},{16,0},{24,8},{1,17},{9,25},{17,1},{25,9},{2,18},{10... | collective-permute-start | bytes 442376 | tf_op jit(solution)/shard_map/ppermute | solution.py:31
  142.2 24.2 %collective-permute-start.5 = (bf16[144,512]{1,0:T(8,128)(2,1)S(1)}, bf16[144,512]{1,0:T(8,128)(2,1)S(1)}, u32[]{:S(2)}, u32[]{:S(2)}) collective-permute-start(bf16[144,512]{1,0:T(8,128)(2,1)S(1)} %get-tuple-element.55), channel_id=1, source_target_pairs={{0,24},{8,16},{16,8},{24,0},{1,25},{9,17},{17,9},{25,1},{2,26},{10... | collective-permute-start | bytes 442376 | tf_op jit(solution)/shard_map/ppermute | solution.py:31
  167.3 41.7 %all-to-all-start.4 = ((bf16[8,16,512]{2,1,0:T(8,128)(2,1)}), bf16[8,16,512]{2,1,0:T(8,128)(2,1)S(1)}, u32[]{:S(2)}, u32[]{:S(2)}) async-start(bf16[8,16,512]{2,1,0:T(8,128)(2,1)} %broadcast_in_dim.57), calls=%async_computation.4 | async-start | bytes 262144 | tf_op jit(solution)/shard_map/all_to_all | solution.py:23
  210.6 17.3 %all-to-all-start.5 = ((bf16[32,32,128]{2,1,0:T(8,128)(2,1)}), bf16[32,32,128]{2,1,0:T(8,128)(2,1)S(1)}, u32[]{:S(2)}, u32[]{:S(2)}) async-start(bf16[32,32,128]{2,1,0:T(8,128)(2,1)} %bitcast.39), calls=%async_computation.5 | async-start | bytes 524288 | tf_op jit(solution)/shard_map/all_to_all | solution.py:48
  243.0 45.9 %all-to-all-start.7 = ((bf16[8,136,128]{2,1,0:T(8,128)(2,1)}), bf16[8,136,128]{2,1,0:T(8,128)(2,1)S(1)}, u32[]{:S(2)}, u32[]{:S(2)}) async-start(bf16[8,136,128]{2,1,0:T(8,128)(2,1)} %shard_map.180), calls=%async_computation.7 | async-start | bytes 557056 | tf_op jit(solution)/shard_map/all_to_all | solution.py:48
  246.7 42.2 %collective-permute-start.6 = (bf16[8,512]{1,0:T(8,128)(2,1)S(1)}, bf16[8,512]{1,0:T(8,128)(2,1)S(1)}, u32[]{:S(2)}, u32[]{:S(2)}) collective-permute-start(bf16[8,512]{1,0:T(8,128)(2,1)S(1)} %get-tuple-element.103), channel_id=1, source_target_pairs={{0,8},{8,0},{16,24},{24,16},{1,9},{9,1},{17,25},{25,17},{2,10},{10... | collective-permute-start | bytes 24584 | tf_op jit(solution)/shard_map/ppermute | solution.py:31
  249.2 39.7 %collective-permute-start.7 = (bf16[8,512]{1,0:T(8,128)(2,1)S(1)}, bf16[8,512]{1,0:T(8,128)(2,1)S(1)}, u32[]{:S(2)}, u32[]{:S(2)}) collective-permute-start(bf16[8,512]{1,0:T(8,128)(2,1)S(1)} %get-tuple-element.102), channel_id=1, source_target_pairs={{0,16},{8,24},{16,0},{24,8},{1,17},{9,25},{17,1},{25,9},{2,18},{10... | collective-permute-start | bytes 24584 | tf_op jit(solution)/shard_map/ppermute | solution.py:31
  252.3 36.6 %collective-permute-start.8 = (bf16[8,512]{1,0:T(8,128)(2,1)S(1)}, bf16[8,512]{1,0:T(8,128)(2,1)S(1)}, u32[]{:S(2)}, u32[]{:S(2)}) collective-permute-start(bf16[8,512]{1,0:T(8,128)(2,1)S(1)} %get-tuple-element.101), channel_id=1, source_target_pairs={{0,24},{8,16},{16,8},{24,0},{1,25},{9,17},{17,9},{25,1},{2,26},{10... | collective-permute-start | bytes 24584 | tf_op jit(solution)/shard_map/ppermute | solution.py:31
